TPU v7x, 32 devices: a whole 2x2x4 slice. The times are simulated.
32 devices in a mesh: sp: 4 (over y, x), tp: 8 (over z, core).
Axes of the slice: x: 2, y: 2, z: 4, core: 2. Of those that a mesh axis runs over, the one named last changes fastest.
Arguments:
- resid: bfloat16 [2048, 2048], P(('sp', 'tp')), may hold values from -6 to 6
- query_a: bfloat16 [2048, 16, 128], P('sp', 'tp'), may hold values from -16 to 16
- key_a: bfloat16 [2048, 16, 128], P('sp', 'tp'), may hold values from -16 to 16
- value_a: bfloat16 [2048, 16, 128], P('sp', 'tp'), may hold values from -6 to 6
- query_b: bfloat16 [2048, 16, 64], P('sp', 'tp'), may hold values from -16 to 16
- key_b: bfloat16 [2048, 16, 64], P('sp', 'tp'), may hold values from -16 to 16
- value_b: bfloat16 [2048, 16, 64], P('sp', 'tp'), may hold values from -6 to 6
- mix_a: float32 [16], P('tp'), may hold values from 0.3 to 0.8
- mix_b: float32 [16], P('tp'), may hold values from 0.3 to 0.8
- head_gain_a: float32 [128], replicated, may hold values from 0.1 to 1.9
- head_gain_b: float32 [64], replicated, may hold values from 0.1 to 1.9
- proj_a: bfloat16 [2048, 2048], P('tp'), may hold values from -0.109375 to 0.109375
- proj_b: bfloat16 [1024, 2048], P('tp'), may hold values from -0.109375 to 0.109375
- norm_gain: float32 [2048], replicated, may hold values from 0.1 to 1.9
- route_ids: int32 [2048, 2], P(('sp', 'tp')), may hold values from 0 to 3, all different within a row; in each aligned block of 64 rows (0 to 63, 64 to 127, ...) at most 48 rows name the same one
- route_weights: float32 [2048, 2], P(('sp', 'tp')), may hold values from 0.2 to 1
- expert_gate: bfloat16 [4, 2048, 6144], P('sp', None, 'tp'), may hold values from -0.125 to 0.125
- expert_up: bfloat16 [4, 2048, 6144], P('sp', None, 'tp'), may hold values from -0.125 to 0.125
- expert_down: bfloat16 [4, 6144, 2048], P('sp', 'tp'), may hold values from -0.078125 to 0.078125
Outputs:
- out: bfloat16 [2048, 2048], P(('sp', 'tp'))
Inputs may be any that keep to these rules, and one draw needn't show every extreme that they name: `route_ids`: each row names 2 different experts. Within the rows of one device (aligned blocks of 64 rows) no expert is named by more than 48 rows, and in every draw some device's block names some expert exactly 48 times.
All inputs are finite; a program needn't handle non-finite values.
Results may differ from a plain program's by a relative error of at most 0.02.
Values may be sent and summed in bfloat16 or wider, within the bound.
No kernel may reach another device: no remote copies, remote signals or barrier semaphores. Data moves between devices by JAX's collectives and lax.ppermute only.
A program may use at most 128 MiB of HBM per device.

v0:
```python
import math

import jax
import jax.numpy as jnp
from jax import lax
from jax.experimental import pallas as pl
from jax.experimental.pallas import tpu as pltpu
from jax.sharding import Mesh, PartitionSpec as P


EPS = 1e-06
NEG = -1e30
HEAD_SCALE = 1.0 - (0.8 - 0.6 * math.exp(-0.3))
KEY_STEP = 512


def partner(value, axis, apart):
    return lax.ppermute(value, axis, [(i, i ^ 1 << apart) for i in range(lax.axis_size(axis))])


def rms_scaled(values, gain):
    return values * lax.rsqrt(jnp.mean(values * values, axis=-1, keepdims=True) + EPS) * gain


def slot_numbers(route_rows, experts, capacity):
    count, top_count = route_rows.shape
    flat = route_rows.reshape(count * top_count)
    onehot = (flat[:, None] == jnp.arange(experts, dtype=jnp.int32)[None, :]).astype(jnp.int32)
    ranks = jnp.sum((jnp.cumsum(onehot, axis=0) - onehot) * onehot, axis=1)
    return (flat * capacity + ranks).reshape(count, top_count)


def empty_map(count, heads, width):
    return (
        jnp.zeros((count, heads, width), jnp.float32),
        jnp.full((heads, count), NEG, jnp.float32),
        jnp.zeros((heads, count), jnp.float32),
    )


def empty_group(query, value):
    return (
        empty_map(query.shape[0], query.shape[1], value.shape[2]),
        empty_map(query.shape[0], query.shape[1], value.shape[2]),
    )


def map_update(state, query, keys, values, allowed, scale):
    weighted, maximum, sums = state
    scores = jnp.einsum("qhd,khd->hqk", query, keys, preferred_element_type=jnp.float32) * scale
    scores = jnp.where(allowed[None], scores, NEG)
    fresh = jnp.maximum(maximum, jnp.max(scores, axis=2))
    weights = jnp.where(allowed[None], jnp.exp(scores - fresh[:, :, None]), 0.0)
    factor = jnp.exp(maximum - fresh)
    sums = sums * factor + jnp.sum(weights, axis=2)
    added = jnp.einsum(
        "hqk,khv->qhv", weights.astype(jnp.bfloat16), values, preferred_element_type=jnp.float32
    )
    weighted = weighted * jnp.transpose(factor)[:, :, None] + added
    return (weighted, fresh, sums)


def group_update(states, query, keys, values, allowed):
    width = query.shape[2] // 2
    scale = 1.0 / math.sqrt(width)
    return tuple(
        (
            map_update(
                states[which],
                query[:, :, which * width : (which + 1) * width],
                keys[:, :, which * width : (which + 1) * width],
                values,
                allowed,
                scale,
            )
            for which in range(2)
        )
    )


def set_update(carry, queries, pieces):
    rows_a, rows_b, query_pos = queries
    piece_key_a, piece_value_a, piece_key_b, piece_value_b = pieces
    length = piece_key_a.shape[0]
    step = math.gcd(length, KEY_STEP)
    latest = query_pos[-1]

    def inner(index, states):
        first = index * step

        def compute(current):
            keys_a = lax.dynamic_slice_in_dim(piece_key_a, first, step, 0)
            values_a = lax.dynamic_slice_in_dim(piece_value_a, first, step, 0)
            keys_b = lax.dynamic_slice_in_dim(piece_key_b, first, step, 0)
            values_b = lax.dynamic_slice_in_dim(piece_value_b, first, step, 0)
            key_pos = first + jnp.arange(step, dtype=jnp.int32)
            allowed = key_pos[None, :] <= query_pos[:, None]
            return (
                group_update(current[0], rows_a, keys_a, values_a, allowed),
                group_update(current[1], rows_b, keys_b, values_b, allowed),
            )

        return lax.cond(first <= latest, compute, lambda current: current, states)

    return lax.fori_loop(0, length // step, inner, carry)


def finish_group(states, mix, gain):
    outputs = [state[0] / jnp.transpose(state[2])[:, :, None] for state in states]
    mixed = outputs[0] - mix[None, :, None] * outputs[1]
    normed = rms_scaled(mixed, gain) * HEAD_SCALE
    return normed.astype(jnp.bfloat16).reshape(mixed.shape[0], -1)


def gathered_device(
    resid,
    query_a,
    key_a,
    value_a,
    query_b,
    key_b,
    value_b,
    mix_a,
    mix_b,
    head_gain_a,
    head_gain_b,
    proj_a,
    proj_b,
    norm_gain,
    route_ids,
    route_weights,
    expert_gate,
    expert_up,
    expert_down,
):
    seq_rows = query_a.shape[0]
    sp_ways = lax.axis_size("sp")
    place = lax.axis_index("sp")
    positions = place * seq_rows + jnp.arange(seq_rows, dtype=jnp.int32)
    levels = sp_ways.bit_length() - 1
    half = seq_rows // 2
    moved = jnp.concatenate(
        [query_a[half:].reshape(half, -1), query_b[half:].reshape(half, -1)], axis=1
    )
    for bit in range(levels):
        moved = partner(moved, "sp", bit)
    split_at = query_a.shape[1] * query_a.shape[2]
    far_a = moved[:, :split_at].reshape(half, query_a.shape[1], query_a.shape[2])
    far_b = moved[:, split_at:].reshape(half, query_b.shape[1], query_b.shape[2])
    far_pos = (sp_ways - 1 - place) * seq_rows + half + jnp.arange(half, dtype=jnp.int32)
    query_sets = ((query_a[:half], query_b[:half], positions[:half]), (far_a, far_b, far_pos))

    def fold_keys(carry, pieces):
        return tuple(
            (set_update(states, queries, pieces) for states, queries in zip(carry, query_sets))
        )

    initial = tuple(
        (
            (empty_group(queries[0], value_a), empty_group(queries[1], value_b))
            for queries in query_sets
        )
    )
    results = fold_keys(
        initial,
        (
            lax.all_gather(key_a, "sp", axis=0, tiled=True),
            lax.all_gather(value_a, "sp", axis=0, tiled=True),
            lax.all_gather(key_b, "sp", axis=0, tiled=True),
            lax.all_gather(value_b, "sp", axis=0, tiled=True),
        ),
    )
    finished = [
        (finish_group(states[0], mix_a, head_gain_a), finish_group(states[1], mix_b, head_gain_b))
        for states in results
    ]
    returned = jnp.concatenate([finished[1][0], finished[1][1]], axis=1)
    for bit in range(levels):
        returned = partner(returned, "sp", bit)
    width_a = finished[0][0].shape[1]
    heads_out_a = jnp.concatenate([finished[0][0], returned[:, :width_a]], axis=0)
    heads_out_b = jnp.concatenate([finished[0][1], returned[:, width_a:]], axis=0)
    width = resid.shape[1]
    tok_rows = resid.shape[0]
    top_count = route_ids.shape[1]
    capacity = 3 * top_count * tok_rows // (2 * sp_ways)
    own_slots = slot_numbers(route_ids, sp_ways, capacity)
    term = jnp.dot(heads_out_a, proj_a, preferred_element_type=jnp.float32)
    term = term + jnp.dot(heads_out_b, proj_b, preferred_element_type=jnp.float32)
    mixed = resid.astype(jnp.float32) + lax.psum_scatter(
        lax.optimization_barrier(term.astype(jnp.bfloat16))
        .astype(jnp.float32)
        .astype(jnp.bfloat16),
        "tp",
        scatter_dimension=0,
        tiled=True,
    ).astype(jnp.float32)
    normed = rms_scaled(mixed, norm_gain).astype(jnp.bfloat16)
    lookup = jnp.arange(sp_ways * capacity, dtype=jnp.int32)[:, None]
    spread = jnp.zeros((sp_ways * capacity, tok_rows), jnp.float32)
    for which in range(top_count):
        spread = spread + (own_slots[:, which][None, :] == lookup).astype(jnp.float32)
    outgoing = jnp.dot(
        spread.astype(jnp.bfloat16), normed, preferred_element_type=jnp.float32
    ).astype(jnp.bfloat16)
    arrived = lax.all_to_all(
        outgoing.reshape(sp_ways, capacity, width), "sp", split_axis=0, concat_axis=0, tiled=True
    )
    piece = lax.all_gather(arrived.reshape(sp_ways * capacity, width), "tp", axis=0, tiled=True)
    gate = jnp.dot(piece, expert_gate[0], preferred_element_type=jnp.float32)
    upward = jnp.dot(piece, expert_up[0], preferred_element_type=jnp.float32)
    hidden = (jax.nn.silu(gate) * upward).astype(jnp.bfloat16)
    term = jnp.dot(hidden, expert_down[0], preferred_element_type=jnp.float32)
    summed = lax.psum_scatter(
        lax.optimization_barrier(term.astype(jnp.bfloat16))
        .astype(jnp.float32)
        .astype(jnp.bfloat16),
        "tp",
        scatter_dimension=0,
        tiled=True,
    )
    finished_rows = summed.reshape(sp_ways, capacity, width)
    back = lax.all_to_all(finished_rows, "sp", split_axis=0, concat_axis=0, tiled=True)
    picked = jnp.take(back.reshape(sp_ways * capacity, width), own_slots.reshape(-1), axis=0)
    picked = picked.reshape(tok_rows, top_count, width)
    output = mixed + jnp.sum(route_weights[:, :, None] * picked.astype(jnp.float32), axis=1)
    return output.astype(jnp.bfloat16)


def attend_kernel(scalars, own, gain, *refs, step, width, maps, block):
    pieces, (out, scores, packed) = refs[:-3], refs[-3:]
    place = pl.program_id(0)
    coef = scalars[0]

    @pl.when(place == 0)
    def _():
        for far, piece in enumerate(pieces):
            packed[own[0] ^ far] = piece[...]

    queries = [jnp.transpose(packed[place, 2 * which * maps : (2 * which + 1) * maps, :]) for which in range(2)]

    def fold(values, combine):
        parts = [values[:, at * width : (at + 1) * width] for at in range(step // width)]
        while len(parts) > 1:
            parts = [combine(*parts[at : at + 2]) for at in range(0, len(parts), 2)]
        return parts[0]

    def raw(which, index):
        keys = packed[index, (2 * which + 1) * maps : (2 * which + 2) * maps, :]
        return jnp.dot(queries[which], keys, preferred_element_type=jnp.float32)

    row = lax.broadcasted_iota(jnp.int32, (step, step), 0)
    column = lax.broadcasted_iota(jnp.int32, (step, step), 1)
    highest = []
    for which in range(2):
        diagonal = jnp.where(column <= row, raw(which, place), NEG)
        scores[which, place] = diagonal
        highest.append(fold(diagonal, jnp.maximum))

    def first_pass(index, carry):
        found = []
        for which in range(2):
            values = raw(which, index)
            scores[which, index] = values
            found.append(jnp.maximum(carry[which], fold(values, jnp.maximum)))
        return tuple(found)

    highest = lax.fori_loop(0, place, first_pass, tuple(highest))
    tops = [jnp.max(found, axis=1, keepdims=True) * coef for found in highest]

    def second_pass(index, carry):
        values = packed[index, 4 * maps : 4 * maps + width, :]
        found = []
        for which in range(2):
            total, mixed = carry[which]
            weights = jnp.exp2(scores[which, index] * coef - tops[which])
            total = total + fold(weights, jnp.add)
            mixed = mixed + lax.dot_general(
                weights.astype(jnp.bfloat16),
                values,
                (((1,), (1,)), ((), ())),
                preferred_element_type=jnp.float32,
            )
            found.append((total, mixed))
        return tuple(found)

    empty = jnp.zeros((step, width), jnp.float32)
    found = lax.fori_loop(0, place + 1, second_pass, ((empty, empty), (empty, empty)))
    outputs = [mixed / jnp.sum(total, axis=1, keepdims=True) for total, mixed in found]
    mixed = outputs[0] - scalars[1] * outputs[1]
    square = jnp.sum(mixed * mixed, axis=1, keepdims=True) * scalars[2]
    normed = (mixed * lax.rsqrt(square + EPS) * gain[...]).astype(jnp.bfloat16)
    cores = out.shape[1]
    for at in range(step // block):
        begin = at // cores * block
        out[0, at % cores, begin : begin + block] = normed[at * block : (at + 1) * block]


def widen(values, width):
    missing = width - values.shape[-1]
    return jnp.pad(values, [(0, 0)] * (values.ndim - 1) + [(0, missing)]) if missing else values


def fast_memory(limit_mib):
    return pltpu.CompilerParams(vmem_limit_bytes=limit_mib << 20)


def mirrored(value, axis, apart):
    return lax.ppermute(value, axis, [(i, i ^ apart) for i in range(lax.axis_size(axis))])


def mirrored_all(values, axis):
    found = {far: mirrored(values[far], axis, far) for far in reversed(range(1, len(values)))}
    return [values[0]] + [found[far] for far in range(1, len(values))]


def whole_call(body, outs, *operands, scalars=(), flops=0, scratch=(), limit=8):
    vmem = pl.BlockSpec(memory_space=pltpu.VMEM)
    return pl.pallas_call(
        body,
        in_specs=[pl.BlockSpec(memory_space=pltpu.SMEM)] * len(scalars) + [vmem] * len(operands),
        out_specs=[vmem] * len(outs),
        out_shape=[pltpu.VMEM(shape, dtype) for shape, dtype in outs],
        scratch_shapes=scratch,
        compiler_params=fast_memory(limit),
        cost_estimate=pl.CostEstimate(flops=flops, bytes_accessed=0, transcendentals=0),
    )(*scalars, *[pltpu.with_memory_space_constraint(operand, pltpu.VMEM) for operand in operands])


def exchanged_heads(query_a, key_a, value_a, query_b, key_b, value_b, mix_a, mix_b, head_gain_a, head_gain_b, block):
    seq_rows, heads_a, _ = query_a.shape
    ways = lax.axis_size("sp")
    cores = lax.axis_size("c")
    place = lax.axis_index("sp")
    groups = ((query_a, key_a, value_a), (query_b, key_b, value_b))
    width = -(-max(group[2].shape[2] for group in groups) // 128) * 128
    maps = -(-max(group[0].shape[2] // 2 for group in groups) // 16) * 16

    def filled(array, size):
        return jnp.pad(array, ((0, 0), (0, size - array.shape[1]), (0, 0)))

    turned = lax.optimization_barrier([[jnp.transpose(array, (1, 2, 0)) for array in group] for group in groups])
    outgoing = []
    for query, key, value in turned:
        half = query.shape[1] // 2
        split = [array[:, first : first + half] for first in (0, half) for array in (query, key)]
        outgoing.append(jnp.concatenate([filled(array, maps) for array in split] + [filled(value, width)], axis=1))
    outgoing = jnp.concatenate(outgoing, axis=0)
    pieces = [lax.dynamic_index_in_dim(outgoing, place ^ far, 0, False) for far in range(ways)]
    pieces = mirrored_all(pieces, "sp")
    first = place < heads_a
    gain = jnp.where(first, widen(head_gain_a, width), widen(head_gain_b, width)) * HEAD_SCALE
    coef_a, coef_b = [math.log2(math.e) / math.sqrt(group[0].shape[2] // 2) for group in groups]
    scalars = jnp.stack(
        [
            jnp.where(first, coef_a, coef_b).astype(jnp.float32),
            lax.dynamic_index_in_dim(jnp.concatenate([mix_a, mix_b]), place, 0, False),
            jnp.where(first, 1.0 / value_a.shape[2], 1.0 / value_b.shape[2]).astype(jnp.float32),
        ]
    )
    pairs = (ways * seq_rows) * (ways + 1) * seq_rows
    shape = (ways, cores, seq_rows // cores, width)
    smem = pl.BlockSpec(memory_space=pltpu.SMEM)
    mixed = pl.pallas_call(
        lambda *refs: attend_kernel(*refs, step=seq_rows, width=width, maps=maps, block=block),
        grid=(ways,),
        in_specs=[smem, smem, pl.BlockSpec((1, width), lambda index: (0, 0))]
        + [pl.BlockSpec(piece.shape, lambda index: (0, 0)) for piece in pieces],
        out_specs=pl.BlockSpec((1,) + shape[1:], lambda index: (index, 0, 0, 0)),
        out_shape=pltpu.HBM(shape, jnp.bfloat16),
        scratch_shapes=[
            pltpu.VMEM((2, ways, seq_rows, seq_rows), jnp.float32),
            pltpu.VMEM((ways,) + pieces[0].shape, jnp.bfloat16),
        ],
        compiler_params=pltpu.CompilerParams(dimension_semantics=("arbitrary",), vmem_limit_bytes=24 << 20),
        cost_estimate=pl.CostEstimate(flops=2 * pairs * (maps + width), bytes_accessed=0, transcendentals=pairs),
        name="attend",
    )(scalars, place[None].astype(jnp.int32), gain[None, :], *pieces)
    flat = mixed.reshape((ways * cores,) + shape[2:])
    return lax.all_to_all(flat, ("sp", "c"), split_axis=0, concat_axis=0, tiled=True).reshape(shape)


def project(heads, proj_a, proj_b, lines, block, heads_a):
    ways, cores, rows, _ = heads.shape
    model = proj_a.shape[1]
    weights = []
    for apart in range(cores):
        weights += [proj_a, proj_b] if apart == 0 else [mirrored(proj_a, "c", apart), mirrored(proj_b, "c", apart)]
    where = jnp.stack([lax.axis_index("c"), lax.axis_index("z")]).astype(jnp.int32)
    step = math.gcd(model, 512)
    narrow = proj_b.shape[0] // (ways - heads_a)
    wide = proj_a.shape[0] // heads_a

    def body(at, heads_ref, *refs):
        sets, outs = refs[: 2 * cores], refs[2 * cores :]
        pairs = []
        for apart in range(cores):
            core = at[0] ^ apart

            def taken(head, used):
                found = [heads_ref[head, core, pl.ds((at[1] ^ far) * block, block), :] for far in range(lines)]
                return jnp.concatenate(found, axis=0)[:, :used]

            left_a = jnp.concatenate([taken(head, wide) for head in range(heads_a)], axis=1)
            left_b = jnp.concatenate([taken(head, narrow) for head in range(heads_a, ways)], axis=1)
            pairs += [(left_a, sets[2 * apart]), (left_b, sets[2 * apart + 1])]
        for first in range(0, model, step):
            span = slice(first, first + step)
            total = None
            for left, right in pairs:
                piece = jnp.dot(left, right[:, span], preferred_element_type=jnp.float32)
                total = piece if total is None else total + piece
            for far in range(lines):
                outs[far][:, span] = total[far * block : (far + 1) * block].astype(jnp.bfloat16)

    return whole_call(
        body,
        [((block, model), jnp.bfloat16)] * lines,
        heads,
        *weights,
        scalars=(where,),
        flops=2 * rows * model * (proj_a.shape[0] + proj_b.shape[0]) * cores,
    )


def expert_hidden(rows_ref, gate_ref, up_ref, held, first, count):
    hidden = gate_ref.shape[1]
    tile = math.gcd(hidden, 256)
    for at in range(hidden // tile):
        span = slice(at * tile, (at + 1) * tile)
        gate = jnp.dot(rows_ref[pl.ds(first, count), :], gate_ref[:, span], preferred_element_type=jnp.float32)
        upward = jnp.dot(rows_ref[pl.ds(first, count), :], up_ref[:, span], preferred_element_type=jnp.float32)
        held[:, span] = (jax.nn.silu(gate) * upward).astype(jnp.bfloat16)


def expert_down(held, down_ref, out_ref, first, count):
    model = down_ref.shape[1]
    tile = math.gcd(model, 512)
    for at in range(model // tile):
        span = slice(at * tile, (at + 1) * tile)
        total = jnp.dot(held, down_ref[:, span], preferred_element_type=jnp.float32)
        out_ref[pl.ds(first, count), span] = total.astype(jnp.bfloat16)


def expert_call(rows, weights, out_cols, after=()):
    count = rows.shape[0]
    hidden = weights[-1].shape[0] if len(weights) != 2 else weights[0].shape[1]
    tile = max(size for size in range(16, 257, 16) if count % size == 0)
    flops = 2 * count * sum(weight.size for weight in weights)

    def body(rows_ref, *refs):
        weight_refs, (out_ref, held) = refs[: len(weights)], refs[-2:]

        def step(index, carry):
            first = index * tile
            if len(weights) > 1:
                expert_hidden(rows_ref, *weight_refs[:2], held, first, tile)
            if len(weights) == 2:
                out_ref[pl.ds(first, tile), :] = held[...]
            else:
                left = held[...] if len(weights) == 3 else rows_ref[pl.ds(first, tile), :]
                expert_down(left, weight_refs[-1], out_ref, first, tile)
            return carry

        lax.fori_loop(0, count // tile, step, 0)

    (out,) = whole_call(
        body,
        [((count, out_cols), jnp.bfloat16)],
        rows,
        *weights,
        *after,
        flops=flops,
        scratch=[pltpu.VMEM((tile, hidden), jnp.bfloat16)],
    )
    return out


def exchanged_device(
    resid,
    query_a,
    key_a,
    value_a,
    query_b,
    key_b,
    value_b,
    mix_a,
    mix_b,
    head_gain_a,
    head_gain_b,
    proj_a,
    proj_b,
    norm_gain,
    route_ids,
    route_weights,
    expert_gate,
    expert_up,
    down_w,
):
    ways, lines, cores = (lax.axis_size(axis) for axis in ("sp", "z", "c"))
    place = lax.axis_index("sp")
    tok_rows, width = resid.shape
    top_count = route_ids.shape[1]
    capacity = 3 * top_count * tok_rows // (2 * ways)
    slots_all = ways * capacity
    low = jnp.bfloat16
    head_cols, back_cols = (width * part // 16 // 128 * 128 for part in (6, 5))
    tail_cols, rest_cols = width - head_cols, width - back_cols

    heads = exchanged_heads(
        query_a, key_a, value_a, query_b, key_b, value_b, mix_a, mix_b, head_gain_a, head_gain_b, tok_rows
    )

    slots = slot_numbers(route_ids ^ place, ways, capacity)
    routes = jnp.concatenate([jnp.transpose(slots).astype(jnp.float32), jnp.transpose(route_weights)], axis=0)
    line_routes = mirrored_all([routes] * lines, "z")

    def hits(routes_ref, which):
        lookup = lax.broadcasted_iota(jnp.int32, (slots_all, tok_rows), 0)
        return routes_ref[which : which + 1, :].astype(jnp.int32) == lookup

    def spread_rows(routes_ref, tokens):
        spread = sum(hits(routes_ref, which).astype(jnp.float32) for which in range(top_count)).astype(low)
        return jnp.dot(spread, tokens, preferred_element_type=jnp.float32).astype(low)

    def blend_rows(routes_ref, block):
        weights = sum(
            jnp.where(hits(routes_ref, which), routes_ref[top_count + which : top_count + which + 1, :], 0.0)
            for which in range(top_count)
        )
        upper = weights.astype(low)
        total = None
        for part in (upper, (weights - upper.astype(jnp.float32)).astype(low)):
            piece = lax.dot_general(part, block, (((0,), (0,)), ((), ())), preferred_element_type=jnp.float32)
            total = piece if total is None else total + piece
        return total

    parts = project(heads, proj_a, proj_b, lines, tok_rows, query_a.shape[1])
    parts = mirrored_all(parts, "z")

    def norm_body(*refs):
        part_refs, (resid_ref, gain_ref, routes_ref), outs = refs[:lines], refs[lines : lines + 3], refs[lines + 3 :]
        mixed = resid_ref[...].astype(jnp.float32)
        for part in part_refs:
            mixed = mixed + part[...].astype(jnp.float32)
        outs[0][...] = mixed
        normed = rms_scaled(mixed, gain_ref[...]).astype(low)
        outs[1][...] = normed[:, head_cols:]
        picked = spread_rows(routes_ref, normed[:, :head_cols])
        for far in range(ways):
            outs[2 + far][...] = picked[far * capacity : (far + 1) * capacity]

    mixed, tail, *heads_out = whole_call(
        norm_body,
        [((tok_rows, width), jnp.float32), ((tok_rows, tail_cols), low)] + [((capacity, head_cols), low)] * ways,
        *parts,
        resid,
        norm_gain[None, :],
        routes,
    )
    tails = mirrored_all([tail] * lines, "z")
    heads_in = mirrored_all(heads_out, "sp")
    groups = {"near": list(range(ways - 1)), "far": [ways - 1]}
    head_blocks = {}
    for group, members in groups.items():
        block = heads_in[members[0]]
        if len(members) > 1:
            block = jnp.concatenate([heads_in[far] for far in members], axis=0)
        head_blocks[group] = mirrored_all([block] * lines, "z")

    weights = (expert_gate[0], expert_up[0], down_w[0])

    def spread_body(*refs):
        tail_refs, routes_refs, outs = refs[:lines], refs[lines : 2 * lines], refs[-ways:]
        for line in range(lines):
            picked = spread_rows(routes_refs[line], tail_refs[line][...])
            for far in range(ways):
                outs[far][line * capacity : (line + 1) * capacity] = picked[far * capacity : (far + 1) * capacity]

    tail_blocks = list(
        whole_call(
            spread_body,
            [((lines * capacity, tail_cols), low)] * ways,
            *tails,
            *line_routes,
            head_blocks["near"][0],
            *weights[:2],
        )
    )
    for members in groups.values():
        for far in members:
            if far > 0:
                tail_blocks[far] = mirrored(tail_blocks[far], "sp", far)

    def join(group, *after):
        members = groups[group]

        def body(*refs):
            head_refs, tail_refs, out = refs[:lines], refs[lines : lines + len(members)], refs[-1]
            for line in range(lines):
                for at in range(len(members)):
                    first = (line * len(members) + at) * capacity
                    out[first : first + capacity, :head_cols] = head_refs[line][at * capacity : (at + 1) * capacity]
                    out[first : first + capacity, head_cols:] = tail_refs[at][line * capacity : (line + 1) * capacity]

        (rows,) = whole_call(
            body,
            [((lines * len(members) * capacity, width), low)],
            *head_blocks[group],
            *[tail_blocks[far] for far in members],
            *after,
        )
        return rows

    def pair(group, own_part, other_parts):
        members = groups[group]

        def body(*refs):
            part_refs, outs = refs[:cores], refs[cores:]
            for line in range(lines):
                for at in range(len(members)):
                    first = (line * len(members) + at) * capacity
                    total = part_refs[0][first : first + capacity].astype(jnp.float32)
                    for part in part_refs[1:]:
                        total = total + part[first : first + capacity].astype(jnp.float32)
                    total = total.astype(low)
                    outs[line][at * capacity : (at + 1) * capacity] = total[:, :back_cols]
                    outs[lines + at][line * capacity : (line + 1) * capacity] = total[:, back_cols:]

        count = len(members)
        return whole_call(
            body,
            [((count * capacity, back_cols), low)] * lines + [((lines * capacity, rest_cols), low)] * count,
            own_part,
            *other_parts,
        )

    assert cores == 2
    tail_back, head_back, before = {}, {}, ()
    for group, members in groups.items():
        rows = join(group, *before)
        other_rows = mirrored(rows, "c", 1)
        hidden = expert_call(rows, weights[:2], weights[0].shape[1])
        after = (hidden,) + tuple(head_back[done][0] for done in head_back)
        other_part = expert_call(other_rows, weights, width, after)
        own_part = expert_call(hidden, weights[2:], width)
        back = pair(group, own_part, [mirrored(other_part, "c", 1)])
        for at, far in reversed(list(enumerate(members))):
            tail_back[far] = mirrored(back[lines + at], "sp", far) if far else back[lines + at]
        head_back[group] = mirrored_all(back[:lines], "z")
        before = (other_part,)
    tail_back = [tail_back[far] for far in range(ways)]

    def blend_body(*refs):
        tail_refs, routes_refs, outs = refs[:ways], refs[ways : ways + lines], refs[ways + lines :]
        for line in range(lines):
            block = jnp.concatenate([ref[line * capacity : (line + 1) * capacity] for ref in tail_refs], axis=0)
            outs[line][...] = blend_rows(routes_refs[line], block).astype(low)

    tail_sums = whole_call(blend_body, [((tok_rows, rest_cols), low)] * lines, *tail_back, *line_routes)
    tail_sums = mirrored_all(tail_sums, "z")

    def total_body(*refs):
        at = 0
        for members in groups.values():
            part_refs = refs[at : at + lines]
            at += lines
            total = sum(part[...].astype(jnp.float32) for part in part_refs).astype(low)
            for index, far in enumerate(members):
                refs[far - ways][...] = total[index * capacity : (index + 1) * capacity]

    head_sums = whole_call(
        total_body, [((capacity, back_cols), low)] * ways, *[block for group in groups for block in head_back[group]]
    )
    head_sums = mirrored_all(head_sums, "sp")

    def final_body(mixed_ref, routes_ref, *refs):
        head_refs, tail_refs, (out,) = refs[:ways], refs[ways : ways + lines], refs[ways + lines :]
        block = jnp.concatenate([ref[...] for ref in head_refs], axis=0)
        total = mixed_ref[:, :back_cols] + blend_rows(routes_ref, block)
        out[:, :back_cols] = total.astype(low)
        total = mixed_ref[:, back_cols:]
        for ref in tail_refs:
            total = total + ref[...].astype(jnp.float32)
        out[:, back_cols:] = total.astype(low)

    (output,) = whole_call(final_body, [((tok_rows, width), low)], mixed, routes, *head_sums, *tail_sums)
    return output


def placements(tp):
    both = ("sp",) + tp
    return (
        (
            P(both, None),
            P("sp", tp, None),
            P("sp", tp, None),
            P("sp", tp, None),
            P("sp", tp, None),
            P("sp", tp, None),
            P("sp", tp, None),
            P(tp),
            P(tp),
            P(),
            P(),
            P(tp, None),
            P(tp, None),
            P(),
            P(both, None),
            P(both, None),
            P("sp", None, tp),
            P("sp", None, tp),
            P("sp", tp, None),
        ),
        P(both, None),
    )


def solution(mesh):
    sp_ways, tp_ways = (mesh.shape[axis] for axis in ("sp", "tp"))
    cores = 2

    def program(*arrays):
        resid, query_a, query_b, route_ids = arrays[0], arrays[1], arrays[4], arrays[14]
        block = resid.shape[0] // (sp_ways * tp_ways)
        heads = (query_a.shape[1] + query_b.shape[1]) // tp_ways
        capacity = 3 * route_ids.shape[1] * block // (2 * sp_ways)
        fits = heads == sp_ways and capacity % 16 == 0 and block % 16 == 0 and resid.shape[1] % 2048 == 0
        if fits:
            devices = mesh.devices.reshape(sp_ways, tp_ways // cores, cores)
            inner, axes = Mesh(devices, ("sp", "z", "c")), ("z", "c")

            def body(*parts):
                return exchanged_device(*parts)

        else:
            inner, axes, body = mesh, ("tp",), gathered_device
        given, returned = placements(axes)
        mapped = jax.shard_map(body, mesh=inner, in_specs=given, out_specs=returned, check_vma=False)
        return mapped(*arrays)

    return program
```

profile of v0, /device:TPU:0, one launch (start us, length us, event | category | flops | bytes accessed | tf_op | source)
XLA Modules:
  0.0 218.0 jit_solution(14563968926501625161)
XLA Ops:
  4.5 3.1 %collective-permute-start = (bf16[384,512]{1,0:T(8,128)(2,1)S(1)}, bf16[384,512]{1,0:T(8,128)(2,1)S(1)}, u32[]{:S(2)}, u32[]{:S(2)}) collective-permute-start(bf16[384,512]{1,0:T(8,128)(2,1)S(1)} %get-tuple-element.87), channel_id=1, source_target_pairs={{0,8},{8,0},{16,24},{24,16},{1,9},{9,1},{17,25},{25,17},{2,10},{10... | collective-permute-start | bytes 1179656 | tf_op jit(solution)/shard_map/ppermute | solution.py:309
  7.6 1.5 collective-permute-start.1
  11.1 6.5 %collective-permute-done.refs_4_ = bf16[384,512]{1,0:T(8,128)(2,1)S(1)} collective-permute-done((bf16[384,512]{1,0:T(8,128)(2,1)S(1)}, bf16[384,512]{1,0:T(8,128)(2,1)S(1)}, u32[]{:S(2)}, u32[]{:S(2)}) %collective-permute-start) | collective-permute-done | bytes 393248 | tf_op jit(solution)/shard_map/ppermute | solution.py:309
  17.6 9.0 %collective-permute-done.1.refs_5_ = bf16[384,512]{1,0:T(8,128)(2,1)S(1)} collective-permute-done((bf16[384,512]{1,0:T(8,128)(2,1)S(1)}, bf16[384,512]{1,0:T(8,128)(2,1)S(1)}, u32[]{:S(2)}, u32[]{:S(2)}) %collective-permute-start.1) | collective-permute-done | bytes 393248 | tf_op jit(solution)/shard_map/ppermute | solution.py:309
  26.6 15.1 %attend.1 = bf16[4,2,256,128]{3,2,1,0:T(8,128)(2,1)} custom-call(f32[3]{0:T(128)S(1)} %pad_maximum_fusion.2.refs_0_, s32[1]{0:T(128)} %bitcast.4.refs_1_, f32[1,128]{1,0:T(1,128)S(1)} %fusion.10.refs_2_, bf16[384,512]{1,0:T(8,128)(2,1)S(1)} %get-tuple-element.86.refs_3_, bf16[384,512]{1,0:T(8,128)(2,1)S(1)} %collective-permute-done.refs_4_, ...), custom_call_target="tpu_custom_call" | custom-call | flops 2013265920 | tf_op jit(solution)/shard_map/attend/pallas_call | solution.py:364
  41.7 4.4 %all-to-all-start = ((bf16[8,256,128]{2,1,0:T(8,128)(2,1)}), bf16[8,256,128]{2,1,0:T(8,128)(2,1)}, u32[]{:S(2)}, u32[]{:S(2)}) async-start(bf16[8,256,128]{2,1,0:T(8,128)(2,1)} %bitcast.50), calls=%async_computation | async-start | bytes 1048576 | tf_op jit(solution)/shard_map/all_to_all | solution.py:380
  47.1 8.7 %all-to-all-done = bf16[8,256,128]{2,1,0:T(8,128)(2,1)} async-done(((bf16[8,256,128]{2,1,0:T(8,128)(2,1)}), bf16[8,256,128]{2,1,0:T(8,128)(2,1)}, u32[]{:S(2)}, u32[]{:S(2)}) %all-to-all-start) | async-done | bytes 524320 | tf_op jit(solution)/shard_map/all_to_all | solution.py:380
  55.8 3.4 %shard_map.181 = (bf16[64,2048]{1,0:T(8,128)(2,1)S(1)}, bf16[64,2048]{1,0:T(8,128)(2,1)S(1)}, bf16[64,2048]{1,0:T(8,128)(2,1)S(1)}, bf16[64,2048]{1,0:T(8,128)(2,1)S(1)}) custom-call(s32[2]{0:T(128)S(1)} %pad_add_fusion.at, bf16[4,2,256,128]{3,2,1,0:T(8,128)(2,1)} %bitcast.17.heads_ref, bf16[256,2048]{1,0:T(8,128)(2,1)} %refs_0_.1, ...), custom_call_target="tpu_custom_call" | custom-call | flops 805306368 | tf_op jit(solution)/shard_map/pallas_call | solution.py:319
  59.3 1.7 collective-permute-start.5
  60.9 2.6 %collective-permute-start.6 = (bf16[64,2048]{1,0:T(8,128)(2,1)S(1)}, bf16[64,2048]{1,0:T(8,128)(2,1)S(1)}, u32[]{:S(2)}, u32[]{:S(2)}) collective-permute-start(bf16[64,2048]{1,0:T(8,128)(2,1)S(1)} %get-tuple-element.53), channel_id=1, source_target_pairs={{0,4},{2,6},{4,0},{6,2},{1,5},{3,7},{5,1},{7,3},{8,12},{10,14},{12... | collective-permute-start | bytes 786440 | tf_op jit(solution)/shard_map/ppermute | solution.py:309
  65.1 3.7 %collective-permute-done.5.refs_1_ = bf16[64,2048]{1,0:T(8,128)(2,1)S(1)} collective-permute-done((bf16[64,2048]{1,0:T(8,128)(2,1)S(1)}, bf16[64,2048]{1,0:T(8,128)(2,1)S(1)}, u32[]{:S(2)}, u32[]{:S(2)}) %collective-permute-start.5) | collective-permute-done | bytes 262176 | tf_op jit(solution)/shard_map/ppermute | solution.py:309
  68.8 12.6 %collective-permute-done.6.refs_2_ = bf16[64,2048]{1,0:T(8,128)(2,1)S(1)} collective-permute-done((bf16[64,2048]{1,0:T(8,128)(2,1)S(1)}, bf16[64,2048]{1,0:T(8,128)(2,1)S(1)}, u32[]{:S(2)}, u32[]{:S(2)}) %collective-permute-start.6) | collective-permute-done | bytes 262176 | tf_op jit(solution)/shard_map/ppermute | solution.py:309
  81.9 3.4 %collective-permute-start.13 = (bf16[64,1280]{1,0:T(8,128)(2,1)S(1)}, bf16[64,1280]{1,0:T(8,128)(2,1)S(1)}, u32[]{:S(2)}, u32[]{:S(2)}) collective-permute-start(bf16[64,1280]{1,0:T(8,128)(2,1)S(1)} %get-tuple-element.59.refs_0_), channel_id=1, source_target_pairs={{0,2},{2,0},{4,6},{6,4},{1,3},{3,1},{5,7},{7,5},{8,10},{10,8},{12,... | collective-permute-start | bytes 491528 | tf_op jit(solution)/shard_map/ppermute | solution.py:309
  86.4 1.4 collective-permute-start.15
  87.8 3.0 %collective-permute-start.8 = (bf16[48,768]{1,0:T(8,128)(2,1)S(1)}, bf16[48,768]{1,0:T(8,128)(2,1)S(1)}, u32[]{:S(2)}, u32[]{:S(2)}) collective-permute-start(bf16[48,768]{1,0:T(8,128)(2,1)S(1)} %get-tuple-element.57), channel_id=1, source_target_pairs={{0,8},{8,0},{16,24},{24,16},{1,9},{9,1},{17,25},{25,17},{2,10},{10... | collective-permute-start | bytes 221192 | tf_op jit(solution)/shard_map/ppermute | solution.py:309
  90.9 2.3 %collective-permute-done.8 = bf16[48,768]{1,0:T(8,128)(2,1)S(1)} collective-permute-done((bf16[48,768]{1,0:T(8,128)(2,1)S(1)}, bf16[48,768]{1,0:T(8,128)(2,1)S(1)}, u32[]{:S(2)}, u32[]{:S(2)}) %collective-permute-start.8) | collective-permute-done | bytes 73760 | tf_op jit(solution)/shard_map/ppermute | solution.py:309
  93.6 2.1 collective-permute-start.17
  95.7 1.9 collective-permute-done.9
  97.5 2.4 %collective-permute-start.18 = (f32[4,64]{1,0:T(4,128)S(1)}, f32[4,64]{1,0:T(4,128)S(1)}, u32[]{:S(2)}, u32[]{:S(2)}) collective-permute-start(f32[4,64]{1,0:T(4,128)S(1)} %pad_maximum_fusion.refs_6_.refs_4_.routes_ref), channel_id=1, source_target_pairs={{0,6},{2,4},{4,2},{6,0},{1,7},{3,5},{5,3},{7,1},{8,14},{10,12},{12... | collective-permute-start | bytes 3080 | tf_op jit(solution)/shard_map/ppermute | solution.py:309
  100.1 2.8 %collective-permute-done.18.refs_7_ = f32[4,64]{1,0:T(4,128)S(1)} collective-permute-done((f32[4,64]{1,0:T(4,128)S(1)}, f32[4,64]{1,0:T(4,128)S(1)}, u32[]{:S(2)}, u32[]{:S(2)}) %collective-permute-start.18) | collective-permute-done | bytes 1056 | tf_op jit(solution)/shard_map/ppermute | solution.py:309
  103.6 2.1 collective-permute-start.19
  106.3 2.8 %collective-permute-start.11 = (bf16[144,768]{1,0:T(8,128)(2,1)S(1)}, bf16[144,768]{1,0:T(8,128)(2,1)S(1)}, u32[]{:S(2)}, u32[]{:S(2)}) collective-permute-start(bf16[144,768]{1,0:T(8,128)(2,1)S(1)} %constant_dynamic-update-slice_fusion.1.refs_8_.refs_0_), channel_id=1, source_target_pairs={{0,4},{2,6},{4,0},{6,2},{1,5},{3,7},{5,1},{7,3},{8,12},{10,14},{12... | collective-permute-start | bytes 663560 | tf_op jit(solution)/shard_map/ppermute | solution.py:309
  109.1 1.4 collective-permute-start.12
  110.5 3.6 %collective-permute-done.10.refs_1_ = bf16[144,768]{1,0:T(8,128)(2,1)S(1)} collective-permute-done((bf16[144,768]{1,0:T(8,128)(2,1)S(1)}, bf16[144,768]{1,0:T(8,128)(2,1)S(1)}, u32[]{:S(2)}, u32[]{:S(2)}) %collective-permute-start.10) | collective-permute-done | bytes 221216 | tf_op jit(solution)/shard_map/ppermute | solution.py:309
  114.1 9.9 %collective-permute-done.11.refs_2_ = bf16[144,768]{1,0:T(8,128)(2,1)S(1)} collective-permute-done((bf16[144,768]{1,0:T(8,128)(2,1)S(1)}, bf16[144,768]{1,0:T(8,128)(2,1)S(1)}, u32[]{:S(2)}, u32[]{:S(2)}) %collective-permute-start.11) | collective-permute-done | bytes 221216 | tf_op jit(solution)/shard_map/ppermute | solution.py:309
  124.3 4.4 %shard_map.185.rows_ref.refs_3_ = bf16[576,768]{1,0:T(8,128)(2,1)S(1)} custom-call(bf16[576,2048]{1,0:T(8,128)(2,1)S(1)} %shard_map.184.rows_ref, bf16[2048,768]{1,0:T(8,128)(2,1)S(1)} %bitcast.31, bf16[2048,768]{1,0:T(8,128)(2,1)S(1)} %bitcast.36), custom_call_target="tpu_custom_call" | custom-call | flops 3623878656 | tf_op jit(solution)/shard_map/pallas_call | solution.py:319
  128.8 6.1 %shard_map.187.refs_5_ = bf16[576,2048]{1,0:T(8,128)(2,1)S(1)} custom-call(bf16[576,2048]{1,0:T(8,128)(2,1)S(1)} %collective-permute-done.21.rows_ref, bf16[2048,768]{1,0:T(8,128)(2,1)S(1)} %bitcast.32, bf16[2048,768]{1,0:T(8,128)(2,1)S(1)} %bitcast.37, bf16[768,2048]{1,0:T(8,128)(2,1)S(1)} %bitcast.40, bf16[576,768]{1,0:T(8,128)(2,1)S(1)} %shard_map.185.rows_ref.refs_3_), custom_call_target="tpu_custom_call" | custom-call | flops 5435817984 | tf_op jit(solution)/shard_map/pallas_call | solution.py:319
  135.4 1.5 collective-permute-start.30
  137.0 1.4 collective-permute-start.26
  138.3 12.8 %collective-permute-done.26.refs_0_ = bf16[48,768]{1,0:T(8,128)(2,1)S(1)} collective-permute-done((bf16[48,768]{1,0:T(8,128)(2,1)S(1)}, bf16[48,768]{1,0:T(8,128)(2,1)S(1)}, u32[]{:S(2)}, u32[]{:S(2)}) %collective-permute-start.26) | collective-permute-done | bytes 73760 | tf_op jit(solution)/shard_map/ppermute | solution.py:309
  151.2 2.9 %collective-permute-start.27 = (bf16[48,768]{1,0:T(8,128)(2,1)S(1)}, bf16[48,768]{1,0:T(8,128)(2,1)S(1)}, u32[]{:S(2)}, u32[]{:S(2)}) collective-permute-start(bf16[48,768]{1,0:T(8,128)(2,1)S(1)} %collective-permute-done.26.refs_0_), channel_id=1, source_target_pairs={{0,2},{2,0},{4,6},{6,4},{1,3},{3,1},{5,7},{7,5},{8,10},{10,8},{12,... | collective-permute-start | bytes 221192 | tf_op jit(solution)/shard_map/ppermute | solution.py:309
  154.1 1.5 collective-permute-start.28
  155.6 1.5 collective-permute-start.29
  157.0 5.4 %collective-permute-done.28.refs_2_ = bf16[48,768]{1,0:T(8,128)(2,1)S(1)} collective-permute-done((bf16[48,768]{1,0:T(8,128)(2,1)S(1)}, bf16[48,768]{1,0:T(8,128)(2,1)S(1)}, u32[]{:S(2)}, u32[]{:S(2)}) %collective-permute-start.28) | collective-permute-done | bytes 73760 | tf_op jit(solution)/shard_map/ppermute | solution.py:309
  162.5 2.6 %shard_map.186.refs_0_ = bf16[576,2048]{1,0:T(8,128)(2,1)S(1)} custom-call(bf16[576,768]{1,0:T(8,128)(2,1)S(1)} %shard_map.185.rows_ref.refs_3_, bf16[768,2048]{1,0:T(8,128)(2,1)S(1)} %bitcast.41), custom_call_target="tpu_custom_call" | custom-call | flops 1811939328 | tf_op jit(solution)/shard_map/pallas_call | solution.py:319
  165.1 1.5 shard_map.190.rows_ref.refs_3_
  167.2 2.1 shard_map.192
  171.4 1.5 collective-permute-start.40
  173.0 1.4 collective-permute-start.41
  175.8 1.6 collective-permute-start.24
  177.4 6.0 %collective-permute-done.23.refs_1_ = bf16[144,640]{1,0:T(8,128)(2,1)S(1)} collective-permute-done((bf16[144,640]{1,0:T(8,128)(2,1)S(1)}, bf16[144,640]{1,0:T(8,128)(2,1)S(1)}, u32[]{:S(2)}, u32[]{:S(2)}) %collective-permute-start.23) | collective-permute-done | bytes 184352 | tf_op jit(solution)/shard_map/ppermute | solution.py:309
  183.4 1.8 collective-permute-start.25
  186.3 10.7 %collective-permute-done.40.refs_2_ = bf16[192,1408]{1,0:T(8,128)(2,1)S(1)} collective-permute-done((bf16[192,1408]{1,0:T(8,128)(2,1)S(1)}, bf16[192,1408]{1,0:T(8,128)(2,1)S(1)}, u32[]{:S(2)}, u32[]{:S(2)}) %collective-permute-start.40) | collective-permute-done | bytes 540704 | tf_op jit(solution)/shard_map/ppermute | solution.py:309
  197.0 2.4 %collective-permute-start.34 = (bf16[48,640]{1,0:T(8,128)(2,1)S(1)}, bf16[48,640]{1,0:T(8,128)(2,1)S(1)}, u32[]{:S(2)}, u32[]{:S(2)}) collective-permute-start(bf16[48,640]{1,0:T(8,128)(2,1)S(1)} %get-tuple-element.71), channel_id=1, source_target_pairs={{0,4},{2,6},{4,0},{6,2},{1,5},{3,7},{5,1},{7,3},{8,12},{10,14},{12... | collective-permute-start | bytes 184328 | tf_op jit(solution)/shard_map/ppermute | solution.py:309
  201.9 3.0 %collective-permute-start.43 = (bf16[64,1408]{1,0:T(8,128)(2,1)S(1)}, bf16[64,1408]{1,0:T(8,128)(2,1)S(1)}, u32[]{:S(2)}, u32[]{:S(2)}) collective-permute-start(bf16[64,1408]{1,0:T(8,128)(2,1)S(1)} %get-tuple-element.83), channel_id=1, source_target_pairs={{0,4},{2,6},{4,0},{6,2},{1,5},{3,7},{5,1},{7,3},{8,12},{10,14},{12... | collective-permute-start | bytes 540680 | tf_op jit(solution)/shard_map/ppermute | solution.py:309
  207.8 1.7 collective-permute-start.37
  210.7 2.5 %collective-permute-start.38 = (bf16[48,640]{1,0:T(8,128)(2,1)S(1)}, bf16[48,640]{1,0:T(8,128)(2,1)S(1)}, u32[]{:S(2)}, u32[]{:S(2)}) collective-permute-start(bf16[48,640]{1,0:T(8,128)(2,1)S(1)} %get-tuple-element.76), channel_id=1, source_target_pairs={{0,24},{8,16},{16,8},{24,0},{1,25},{9,17},{17,9},{25,1},{2,26},{10... | collective-permute-start | bytes 184328 | tf_op jit(solution)/shard_map/ppermute | solution.py:309
  213.2 2.6 %collective-permute-done.38.refs_3_ = bf16[48,640]{1,0:T(8,128)(2,1)S(1)} collective-permute-done((bf16[48,640]{1,0:T(8,128)(2,1)S(1)}, bf16[48,640]{1,0:T(8,128)(2,1)S(1)}, u32[]{:S(2)}, u32[]{:S(2)}) %collective-permute-start.38) | collective-permute-done | bytes 61472 | tf_op jit(solution)/shard_map/ppermute | solution.py:309
  (123 shorter events, 27.1 us)
Async XLA Ops:
  4.5 13.1 %collective-permute-start = (bf16[384,512]{1,0:T(8,128)(2,1)S(1)}, bf16[384,512]{1,0:T(8,128)(2,1)S(1)}, u32[]{:S(2)}, u32[]{:S(2)}) collective-permute-start(bf16[384,512]{1,0:T(8,128)(2,1)S(1)} %get-tuple-element.87), channel_id=1, source_target_pairs={{0,8},{8,0},{16,24},{24,16},{1,9},{9,1},{17,25},{25,17},{2,10},{10... | collective-permute-start | bytes 1179656 | tf_op jit(solution)/shard_map/ppermute | solution.py:309
  7.6 19.0 %collective-permute-start.1 = (bf16[384,512]{1,0:T(8,128)(2,1)S(1)}, bf16[384,512]{1,0:T(8,128)(2,1)S(1)}, u32[]{:S(2)}, u32[]{:S(2)}) collective-permute-start(bf16[384,512]{1,0:T(8,128)(2,1)S(1)} %get-tuple-element.88), channel_id=1, source_target_pairs={{0,16},{8,24},{16,0},{24,8},{1,17},{9,25},{17,1},{25,9},{2,18},{10... | collective-permute-start | bytes 1179656 | tf_op jit(solution)/shard_map/ppermute | solution.py:309
  9.1 17.5 %collective-permute-start.2 = (bf16[384,512]{1,0:T(8,128)(2,1)S(1)}, bf16[384,512]{1,0:T(8,128)(2,1)S(1)}, u32[]{:S(2)}, u32[]{:S(2)}) collective-permute-start(bf16[384,512]{1,0:T(8,128)(2,1)S(1)} %get-tuple-element.85), channel_id=1, source_target_pairs={{0,24},{8,16},{16,8},{24,0},{1,25},{9,17},{17,9},{25,1},{2,26},{10... | collective-permute-start | bytes 1179656 | tf_op jit(solution)/shard_map/ppermute | solution.py:309
  9.1 46.7 %collective-permute-start.3 = (bf16[256,2048]{1,0:T(8,128)(2,1)}, bf16[256,2048]{1,0:T(8,128)(2,1)}, u32[]{:S(2)}, u32[]{:S(2)}) collective-permute-start(bf16[256,2048]{1,0:T(8,128)(2,1)} %refs_0_.1), channel_id=1, source_target_pairs={{0,1},{1,0},{2,3},{3,2},{4,5},{5,4},{6,7},{7,6},{8,9},{9,8},{10,11... | collective-permute-start | bytes 3145736 | tf_op jit(solution)/shard_map/ppermute | solution.py:309
  9.1 38.0 %collective-permute-start.4 = (bf16[128,2048]{1,0:T(8,128)(2,1)}, bf16[128,2048]{1,0:T(8,128)(2,1)}, u32[]{:S(2)}, u32[]{:S(2)}) collective-permute-start(bf16[128,2048]{1,0:T(8,128)(2,1)} %refs_1_.1), channel_id=1, source_target_pairs={{0,1},{1,0},{2,3},{3,2},{4,5},{5,4},{6,7},{7,6},{8,9},{9,8},{10,11... | collective-permute-start | bytes 1572872 | tf_op jit(solution)/shard_map/ppermute | solution.py:309
  41.7 61.3 %copy-start.1 = (bf16[1,2048,768]{2,1,0:T(8,128)(2,1)S(1)}, bf16[1,2048,768]{2,1,0:T(8,128)(2,1)}, u32[]{:S(2)}) copy-start(bf16[1,2048,768]{2,1,0:T(8,128)(2,1)} %param.36) | copy-start | bytes 9437188
  41.7 14.1 %all-to-all-start = ((bf16[8,256,128]{2,1,0:T(8,128)(2,1)}), bf16[8,256,128]{2,1,0:T(8,128)(2,1)}, u32[]{:S(2)}, u32[]{:S(2)}) async-start(bf16[8,256,128]{2,1,0:T(8,128)(2,1)} %bitcast.50), calls=%async_computation | async-start | bytes 1048576 | tf_op jit(solution)/shard_map/all_to_all | solution.py:380
  55.8 47.1 %copy-start = (bf16[1,2048,768]{2,1,0:T(8,128)(2,1)S(1)}, bf16[1,2048,768]{2,1,0:T(8,128)(2,1)}, u32[]{:S(2)}) copy-start(bf16[1,2048,768]{2,1,0:T(8,128)(2,1)} %param.35) | copy-start | bytes 9437188
  59.3 9.5 %collective-permute-start.5 = (bf16[64,2048]{1,0:T(8,128)(2,1)S(1)}, bf16[64,2048]{1,0:T(8,128)(2,1)S(1)}, u32[]{:S(2)}, u32[]{:S(2)}) collective-permute-start(bf16[64,2048]{1,0:T(8,128)(2,1)S(1)} %get-tuple-element.52), channel_id=1, source_target_pairs={{0,2},{2,0},{4,6},{6,4},{1,3},{3,1},{5,7},{7,5},{8,10},{10,8},{12,... | collective-permute-start | bytes 786440 | tf_op jit(solution)/shard_map/ppermute | solution.py:309
  60.9 20.5 %collective-permute-start.6 = (bf16[64,2048]{1,0:T(8,128)(2,1)S(1)}, bf16[64,2048]{1,0:T(8,128)(2,1)S(1)}, u32[]{:S(2)}, u32[]{:S(2)}) collective-permute-start(bf16[64,2048]{1,0:T(8,128)(2,1)S(1)} %get-tuple-element.53), channel_id=1, source_target_pairs={{0,4},{2,6},{4,0},{6,2},{1,5},{3,7},{5,1},{7,3},{8,12},{10,14},{12... | collective-permute-start | bytes 786440 | tf_op jit(solution)/shard_map/ppermute | solution.py:309
  63.5 17.9 %collective-permute-start.7 = (bf16[64,2048]{1,0:T(8,128)(2,1)S(1)}, bf16[64,2048]{1,0:T(8,128)(2,1)S(1)}, u32[]{:S(2)}, u32[]{:S(2)}) collective-permute-start(bf16[64,2048]{1,0:T(8,128)(2,1)S(1)} %get-tuple-element.54), channel_id=1, source_target_pairs={{0,6},{2,4},{4,2},{6,0},{1,7},{3,5},{5,3},{7,1},{8,14},{10,12},{12... | collective-permute-start | bytes 786440 | tf_op jit(solution)/shard_map/ppermute | solution.py:309
  64.4 29.2 %collective-permute-start.16 = (f32[4,64]{1,0:T(4,128)S(1)}, f32[4,64]{1,0:T(4,128)S(1)}, u32[]{:S(2)}, u32[]{:S(2)}) collective-permute-start(f32[4,64]{1,0:T(4,128)S(1)} %pad_maximum_fusion.refs_6_.refs_4_.routes_ref), channel_id=1, source_target_pairs={{0,2},{2,0},{4,6},{6,4},{1,3},{3,1},{5,7},{7,5},{8,10},{10,8},{12,... | collective-permute-start | bytes 3080 | tf_op jit(solution)/shard_map/ppermute | solution.py:309
  81.9 21.0 %collective-permute-start.13 = (bf16[64,1280]{1,0:T(8,128)(2,1)S(1)}, bf16[64,1280]{1,0:T(8,128)(2,1)S(1)}, u32[]{:S(2)}, u32[]{:S(2)}) collective-permute-start(bf16[64,1280]{1,0:T(8,128)(2,1)S(1)} %get-tuple-element.59.refs_0_), channel_id=1, source_target_pairs={{0,2},{2,0},{4,6},{6,4},{1,3},{3,1},{5,7},{7,5},{8,10},{10,8},{12,... | collective-permute-start | bytes 491528 | tf_op jit(solution)/shard_map/ppermute | solution.py:309
  85.4 17.6 %collective-permute-start.14 = (bf16[64,1280]{1,0:T(8,128)(2,1)S(1)}, bf16[64,1280]{1,0:T(8,128)(2,1)S(1)}, u32[]{:S(2)}, u32[]{:S(2)}) collective-permute-start(bf16[64,1280]{1,0:T(8,128)(2,1)S(1)} %get-tuple-element.59.refs_0_), channel_id=1, source_target_pairs={{0,4},{2,6},{4,0},{6,2},{1,5},{3,7},{5,1},{7,3},{8,12},{10,14},{12... | collective-permute-start | bytes 491528 | tf_op jit(solution)/shard_map/ppermute | solution.py:309
  86.4 16.5 %collective-permute-start.15 = (bf16[64,1280]{1,0:T(8,128)(2,1)S(1)}, bf16[64,1280]{1,0:T(8,128)(2,1)S(1)}, u32[]{:S(2)}, u32[]{:S(2)}) collective-permute-start(bf16[64,1280]{1,0:T(8,128)(2,1)S(1)} %get-tuple-element.59.refs_0_), channel_id=1, source_target_pairs={{0,6},{2,4},{4,2},{6,0},{1,7},{3,5},{5,3},{7,1},{8,14},{10,12},{12... | collective-permute-start | bytes 491528 | tf_op jit(solution)/shard_map/ppermute | solution.py:309
  87.8 5.4 %collective-permute-start.8 = (bf16[48,768]{1,0:T(8,128)(2,1)S(1)}, bf16[48,768]{1,0:T(8,128)(2,1)S(1)}, u32[]{:S(2)}, u32[]{:S(2)}) collective-permute-start(bf16[48,768]{1,0:T(8,128)(2,1)S(1)} %get-tuple-element.57), channel_id=1, source_target_pairs={{0,8},{8,0},{16,24},{24,16},{1,9},{9,1},{17,25},{25,17},{2,10},{10... | collective-permute-start | bytes 221192 | tf_op jit(solution)/shard_map/ppermute | solution.py:309
  93.2 4.4 %collective-permute-start.9 = (bf16[48,768]{1,0:T(8,128)(2,1)S(1)}, bf16[48,768]{1,0:T(8,128)(2,1)S(1)}, u32[]{:S(2)}, u32[]{:S(2)}) collective-permute-start(bf16[48,768]{1,0:T(8,128)(2,1)S(1)} %get-tuple-element.58), channel_id=1, source_target_pairs={{0,16},{8,24},{16,0},{24,8},{1,17},{9,25},{17,1},{25,9},{2,18},{10... | collective-permute-start | bytes 221192 | tf_op jit(solution)/shard_map/ppermute | solution.py:309
  93.6 6.6 %collective-permute-start.17 = (f32[4,64]{1,0:T(4,128)S(1)}, f32[4,64]{1,0:T(4,128)S(1)}, u32[]{:S(2)}, u32[]{:S(2)}) collective-permute-start(f32[4,64]{1,0:T(4,128)S(1)} %pad_maximum_fusion.refs_6_.refs_4_.routes_ref), channel_id=1, source_target_pairs={{0,4},{2,6},{4,0},{6,2},{1,5},{3,7},{5,1},{7,3},{8,12},{10,14},{12... | collective-permute-start | bytes 3080 | tf_op jit(solution)/shard_map/ppermute | solution.py:309
  97.5 5.4 %collective-permute-start.18 = (f32[4,64]{1,0:T(4,128)S(1)}, f32[4,64]{1,0:T(4,128)S(1)}, u32[]{:S(2)}, u32[]{:S(2)}) collective-permute-start(f32[4,64]{1,0:T(4,128)S(1)} %pad_maximum_fusion.refs_6_.refs_4_.routes_ref), channel_id=1, source_target_pairs={{0,6},{2,4},{4,2},{6,0},{1,7},{3,5},{5,3},{7,1},{8,14},{10,12},{12... | collective-permute-start | bytes 3080 | tf_op jit(solution)/shard_map/ppermute | solution.py:309
  103.6 20.4 %collective-permute-start.19 = (bf16[192,1280]{1,0:T(8,128)(2,1)S(1)}, bf16[192,1280]{1,0:T(8,128)(2,1)S(1)}, u32[]{:S(2)}, u32[]{:S(2)}) collective-permute-start(bf16[192,1280]{1,0:T(8,128)(2,1)S(1)} %get-tuple-element.61), channel_id=1, source_target_pairs={{0,8},{8,0},{16,24},{24,16},{1,9},{9,1},{17,25},{25,17},{2,10},{10... | collective-permute-start | bytes 1474568 | tf_op jit(solution)/shard_map/ppermute | solution.py:309
  105.7 18.3 %collective-permute-start.20 = (bf16[192,1280]{1,0:T(8,128)(2,1)S(1)}, bf16[192,1280]{1,0:T(8,128)(2,1)S(1)}, u32[]{:S(2)}, u32[]{:S(2)}) collective-permute-start(bf16[192,1280]{1,0:T(8,128)(2,1)S(1)} %get-tuple-element.62), channel_id=1, source_target_pairs={{0,16},{8,24},{16,0},{24,8},{1,17},{9,25},{17,1},{25,9},{2,18},{10... | collective-permute-start | bytes 1474568 | tf_op jit(solution)/shard_map/ppermute | solution.py:309
  106.1 8.0 %collective-permute-start.10 = (bf16[144,768]{1,0:T(8,128)(2,1)S(1)}, bf16[144,768]{1,0:T(8,128)(2,1)S(1)}, u32[]{:S(2)}, u32[]{:S(2)}) collective-permute-start(bf16[144,768]{1,0:T(8,128)(2,1)S(1)} %constant_dynamic-update-slice_fusion.1.refs_8_.refs_0_), channel_id=1, source_target_pairs={{0,2},{2,0},{4,6},{6,4},{1,3},{3,1},{5,7},{7,5},{8,10},{10,8},{12,... | collective-permute-start | bytes 663560 | tf_op jit(solution)/shard_map/ppermute | solution.py:309
  106.3 17.8 %collective-permute-start.11 = (bf16[144,768]{1,0:T(8,128)(2,1)S(1)}, bf16[144,768]{1,0:T(8,128)(2,1)S(1)}, u32[]{:S(2)}, u32[]{:S(2)}) collective-permute-start(bf16[144,768]{1,0:T(8,128)(2,1)S(1)} %constant_dynamic-update-slice_fusion.1.refs_8_.refs_0_), channel_id=1, source_target_pairs={{0,4},{2,6},{4,0},{6,2},{1,5},{3,7},{5,1},{7,3},{8,12},{10,14},{12... | collective-permute-start | bytes 663560 | tf_op jit(solution)/shard_map/ppermute | solution.py:309
  109.1 15.0 %collective-permute-start.12 = (bf16[144,768]{1,0:T(8,128)(2,1)S(1)}, bf16[144,768]{1,0:T(8,128)(2,1)S(1)}, u32[]{:S(2)}, u32[]{:S(2)}) collective-permute-start(bf16[144,768]{1,0:T(8,128)(2,1)S(1)} %constant_dynamic-update-slice_fusion.1.refs_8_.refs_0_), channel_id=1, source_target_pairs={{0,6},{2,4},{4,2},{6,0},{1,7},{3,5},{5,3},{7,1},{8,14},{10,12},{12... | collective-permute-start | bytes 663560 | tf_op jit(solution)/shard_map/ppermute | solution.py:309
  124.2 4.6 %collective-permute-start.21 = (bf16[576,2048]{1,0:T(8,128)(2,1)S(1)}, bf16[576,2048]{1,0:T(8,128)(2,1)S(1)}, u32[]{:S(2)}, u32[]{:S(2)}) collective-permute-start(bf16[576,2048]{1,0:T(8,128)(2,1)S(1)} %shard_map.184.rows_ref), channel_id=1, source_target_pairs={{0,1},{1,0},{2,3},{3,2},{4,5},{5,4},{6,7},{7,6},{8,9},{9,8},{10,11... | collective-permute-start | bytes 7077896 | tf_op jit(solution)/shard_map/ppermute | solution.py:309
  135.0 31.6 %collective-permute-start.22 = (bf16[576,2048]{1,0:T(8,128)(2,1)S(1)}, bf16[576,2048]{1,0:T(8,128)(2,1)S(1)}, u32[]{:S(2)}, u32[]{:S(2)}) collective-permute-start(bf16[576,2048]{1,0:T(8,128)(2,1)S(1)} %shard_map.187.refs_5_), channel_id=1, source_target_pairs={{0,1},{1,0},{2,3},{3,2},{4,5},{5,4},{6,7},{7,6},{8,9},{9,8},{10,11... | collective-permute-start | bytes 7077896 | tf_op jit(solution)/shard_map/ppermute | solution.py:309
  135.4 27.0 %collective-permute-start.30 = (bf16[192,1280]{1,0:T(8,128)(2,1)S(1)}, bf16[192,1280]{1,0:T(8,128)(2,1)S(1)}, u32[]{:S(2)}, u32[]{:S(2)}) collective-permute-start(bf16[192,1280]{1,0:T(8,128)(2,1)S(1)} %get-tuple-element.68), channel_id=1, source_target_pairs={{0,24},{8,16},{16,8},{24,0},{1,25},{9,17},{17,9},{25,1},{2,26},{10... | collective-permute-start | bytes 1474568 | tf_op jit(solution)/shard_map/ppermute | solution.py:309
  137.0 14.2 %collective-permute-start.26 = (bf16[48,768]{1,0:T(8,128)(2,1)S(1)}, bf16[48,768]{1,0:T(8,128)(2,1)S(1)}, u32[]{:S(2)}, u32[]{:S(2)}) collective-permute-start(bf16[48,768]{1,0:T(8,128)(2,1)S(1)} %get-tuple-element.67), channel_id=1, source_target_pairs={{0,24},{8,16},{16,8},{24,0},{1,25},{9,17},{17,9},{25,1},{2,26},{10... | collective-permute-start | bytes 221192 | tf_op jit(solution)/shard_map/ppermute | solution.py:309
  151.2 5.9 %collective-permute-start.27 = (bf16[48,768]{1,0:T(8,128)(2,1)S(1)}, bf16[48,768]{1,0:T(8,128)(2,1)S(1)}, u32[]{:S(2)}, u32[]{:S(2)}) collective-permute-start(bf16[48,768]{1,0:T(8,128)(2,1)S(1)} %collective-permute-done.26.refs_0_), channel_id=1, source_target_pairs={{0,2},{2,0},{4,6},{6,4},{1,3},{3,1},{5,7},{7,5},{8,10},{10,8},{12,... | collective-permute-start | bytes 221192 | tf_op jit(solution)/shard_map/ppermute | solution.py:309
  154.1 8.3 %collective-permute-start.28 = (bf16[48,768]{1,0:T(8,128)(2,1)S(1)}, bf16[48,768]{1,0:T(8,128)(2,1)S(1)}, u32[]{:S(2)}, u32[]{:S(2)}) collective-permute-start(bf16[48,768]{1,0:T(8,128)(2,1)S(1)} %collective-permute-done.26.refs_0_), channel_id=1, source_target_pairs={{0,4},{2,6},{4,0},{6,2},{1,5},{3,7},{5,1},{7,3},{8,12},{10,14},{12... | collective-permute-start | bytes 221192 | tf_op jit(solution)/shard_map/ppermute | solution.py:309
  155.6 6.8 %collective-permute-start.29 = (bf16[48,768]{1,0:T(8,128)(2,1)S(1)}, bf16[48,768]{1,0:T(8,128)(2,1)S(1)}, u32[]{:S(2)}, u32[]{:S(2)}) collective-permute-start(bf16[48,768]{1,0:T(8,128)(2,1)S(1)} %collective-permute-done.26.refs_0_), channel_id=1, source_target_pairs={{0,6},{2,4},{4,2},{6,0},{1,7},{3,5},{5,3},{7,1},{8,14},{10,12},{12... | collective-permute-start | bytes 221192 | tf_op jit(solution)/shard_map/ppermute | solution.py:309
  162.5 4.7 %collective-permute-start.31 = (bf16[192,2048]{1,0:T(8,128)(2,1)S(1)}, bf16[192,2048]{1,0:T(8,128)(2,1)S(1)}, u32[]{:S(2)}, u32[]{:S(2)}) collective-permute-start(bf16[192,2048]{1,0:T(8,128)(2,1)S(1)} %shard_map.189.rows_ref), channel_id=1, source_target_pairs={{0,1},{1,0},{2,3},{3,2},{4,5},{5,4},{6,7},{7,6},{8,9},{9,8},{10,11... | collective-permute-start | bytes 2359304 | tf_op jit(solution)/shard_map/ppermute | solution.py:309
  169.3 3.6 %collective-permute-start.32 = (bf16[192,2048]{1,0:T(8,128)(2,1)S(1)}, bf16[192,2048]{1,0:T(8,128)(2,1)S(1)}, u32[]{:S(2)}, u32[]{:S(2)}) collective-permute-start(bf16[192,2048]{1,0:T(8,128)(2,1)S(1)} %shard_map.192), channel_id=1, source_target_pairs={{0,1},{1,0},{2,3},{3,2},{4,5},{5,4},{6,7},{7,6},{8,9},{9,8},{10,11... | collective-permute-start | bytes 2359304 | tf_op jit(solution)/shard_map/ppermute | solution.py:309
  169.8 15.5 %collective-permute-start.39 = (bf16[192,1408]{1,0:T(8,128)(2,1)S(1)}, bf16[192,1408]{1,0:T(8,128)(2,1)S(1)}, u32[]{:S(2)}, u32[]{:S(2)}) collective-permute-start(bf16[192,1408]{1,0:T(8,128)(2,1)S(1)} %get-tuple-element.78), channel_id=1, source_target_pairs={{0,8},{8,0},{16,24},{24,16},{1,9},{9,1},{17,25},{25,17},{2,10},{10... | collective-permute-start | bytes 1622024 | tf_op jit(solution)/shard_map/ppermute | solution.py:309
  171.4 25.6 %collective-permute-start.40 = (bf16[192,1408]{1,0:T(8,128)(2,1)S(1)}, bf16[192,1408]{1,0:T(8,128)(2,1)S(1)}, u32[]{:S(2)}, u32[]{:S(2)}) collective-permute-start(bf16[192,1408]{1,0:T(8,128)(2,1)S(1)} %get-tuple-element.79), channel_id=1, source_target_pairs={{0,16},{8,24},{16,0},{24,8},{1,17},{9,25},{17,1},{25,9},{2,18},{10... | collective-permute-start | bytes 1622024 | tf_op jit(solution)/shard_map/ppermute | solution.py:309
  173.0 26.4 %collective-permute-start.41 = (bf16[192,1408]{1,0:T(8,128)(2,1)S(1)}, bf16[192,1408]{1,0:T(8,128)(2,1)S(1)}, u32[]{:S(2)}, u32[]{:S(2)}) collective-permute-start(bf16[192,1408]{1,0:T(8,128)(2,1)S(1)} %get-tuple-element.80), channel_id=1, source_target_pairs={{0,24},{8,16},{16,8},{24,0},{1,25},{9,17},{17,9},{25,1},{2,26},{10... | collective-permute-start | bytes 1622024 | tf_op jit(solution)/shard_map/ppermute | solution.py:309
  174.5 9.0 %collective-permute-start.23 = (bf16[144,640]{1,0:T(8,128)(2,1)S(1)}, bf16[144,640]{1,0:T(8,128)(2,1)S(1)}, u32[]{:S(2)}, u32[]{:S(2)}) collective-permute-start(bf16[144,640]{1,0:T(8,128)(2,1)S(1)} %get-tuple-element.64), channel_id=1, source_target_pairs={{0,2},{2,0},{4,6},{6,4},{1,3},{3,1},{5,7},{7,5},{8,10},{10,8},{12,... | collective-permute-start | bytes 552968 | tf_op jit(solution)/shard_map/ppermute | solution.py:309
  175.8 26.0 %collective-permute-start.24 = (bf16[144,640]{1,0:T(8,128)(2,1)S(1)}, bf16[144,640]{1,0:T(8,128)(2,1)S(1)}, u32[]{:S(2)}, u32[]{:S(2)}) collective-permute-start(bf16[144,640]{1,0:T(8,128)(2,1)S(1)} %get-tuple-element.65), channel_id=1, source_target_pairs={{0,4},{2,6},{4,0},{6,2},{1,5},{3,7},{5,1},{7,3},{8,12},{10,14},{12... | collective-permute-start | bytes 552968 | tf_op jit(solution)/shard_map/ppermute | solution.py:309
  183.4 18.5 %collective-permute-start.25 = (bf16[144,640]{1,0:T(8,128)(2,1)S(1)}, bf16[144,640]{1,0:T(8,128)(2,1)S(1)}, u32[]{:S(2)}, u32[]{:S(2)}) collective-permute-start(bf16[144,640]{1,0:T(8,128)(2,1)S(1)} %get-tuple-element.66), channel_id=1, source_target_pairs={{0,6},{2,4},{4,2},{6,0},{1,7},{3,5},{5,3},{7,1},{8,14},{10,12},{12... | collective-permute-start | bytes 552968 | tf_op jit(solution)/shard_map/ppermute | solution.py:309
  185.3 19.6 %collective-permute-start.33 = (bf16[48,640]{1,0:T(8,128)(2,1)S(1)}, bf16[48,640]{1,0:T(8,128)(2,1)S(1)}, u32[]{:S(2)}, u32[]{:S(2)}) collective-permute-start(bf16[48,640]{1,0:T(8,128)(2,1)S(1)} %get-tuple-element.70), channel_id=1, source_target_pairs={{0,2},{2,0},{4,6},{6,4},{1,3},{3,1},{5,7},{7,5},{8,10},{10,8},{12,... | collective-permute-start | bytes 184328 | tf_op jit(solution)/shard_map/ppermute | solution.py:309
  197.0 9.3 %collective-permute-start.34 = (bf16[48,640]{1,0:T(8,128)(2,1)S(1)}, bf16[48,640]{1,0:T(8,128)(2,1)S(1)}, u32[]{:S(2)}, u32[]{:S(2)}) collective-permute-start(bf16[48,640]{1,0:T(8,128)(2,1)S(1)} %get-tuple-element.71), channel_id=1, source_target_pairs={{0,4},{2,6},{4,0},{6,2},{1,5},{3,7},{5,1},{7,3},{8,12},{10,14},{12... | collective-permute-start | bytes 184328 | tf_op jit(solution)/shard_map/ppermute | solution.py:309
  199.4 6.9 %collective-permute-start.35 = (bf16[48,640]{1,0:T(8,128)(2,1)S(1)}, bf16[48,640]{1,0:T(8,128)(2,1)S(1)}, u32[]{:S(2)}, u32[]{:S(2)}) collective-permute-start(bf16[48,640]{1,0:T(8,128)(2,1)S(1)} %get-tuple-element.72), channel_id=1, source_target_pairs={{0,6},{2,4},{4,2},{6,0},{1,7},{3,5},{5,3},{7,1},{8,14},{10,12},{12... | collective-permute-start | bytes 184328 | tf_op jit(solution)/shard_map/ppermute | solution.py:309
  201.8 14.0 %collective-permute-start.42 = (bf16[64,1408]{1,0:T(8,128)(2,1)S(1)}, bf16[64,1408]{1,0:T(8,128)(2,1)S(1)}, u32[]{:S(2)}, u32[]{:S(2)}) collective-permute-start(bf16[64,1408]{1,0:T(8,128)(2,1)S(1)} %get-tuple-element.82), channel_id=1, source_target_pairs={{0,2},{2,0},{4,6},{6,4},{1,3},{3,1},{5,7},{7,5},{8,10},{10,8},{12,... | collective-permute-start | bytes 540680 | tf_op jit(solution)/shard_map/ppermute | solution.py:309
  201.9 15.0 %collective-permute-start.43 = (bf16[64,1408]{1,0:T(8,128)(2,1)S(1)}, bf16[64,1408]{1,0:T(8,128)(2,1)S(1)}, u32[]{:S(2)}, u32[]{:S(2)}) collective-permute-start(bf16[64,1408]{1,0:T(8,128)(2,1)S(1)} %get-tuple-element.83), channel_id=1, source_target_pairs={{0,4},{2,6},{4,0},{6,2},{1,5},{3,7},{5,1},{7,3},{8,12},{10,14},{12... | collective-permute-start | bytes 540680 | tf_op jit(solution)/shard_map/ppermute | solution.py:309
  204.9 12.0 %collective-permute-start.44 = (bf16[64,1408]{1,0:T(8,128)(2,1)S(1)}, bf16[64,1408]{1,0:T(8,128)(2,1)S(1)}, u32[]{:S(2)}, u32[]{:S(2)}) collective-permute-start(bf16[64,1408]{1,0:T(8,128)(2,1)S(1)} %get-tuple-element.84), channel_id=1, source_target_pairs={{0,6},{2,4},{4,2},{6,0},{1,7},{3,5},{5,3},{7,1},{8,14},{10,12},{12... | collective-permute-start | bytes 540680 | tf_op jit(solution)/shard_map/ppermute | solution.py:309
  206.4 4.3 %collective-permute-start.36 = (bf16[48,640]{1,0:T(8,128)(2,1)S(1)}, bf16[48,640]{1,0:T(8,128)(2,1)S(1)}, u32[]{:S(2)}, u32[]{:S(2)}) collective-permute-start(bf16[48,640]{1,0:T(8,128)(2,1)S(1)} %get-tuple-element.74), channel_id=1, source_target_pairs={{0,8},{8,0},{16,24},{24,16},{1,9},{9,1},{17,25},{25,17},{2,10},{10... | collective-permute-start | bytes 184328 | tf_op jit(solution)/shard_map/ppermute | solution.py:309
  207.8 5.4 %collective-permute-start.37 = (bf16[48,640]{1,0:T(8,128)(2,1)S(1)}, bf16[48,640]{1,0:T(8,128)(2,1)S(1)}, u32[]{:S(2)}, u32[]{:S(2)}) collective-permute-start(bf16[48,640]{1,0:T(8,128)(2,1)S(1)} %get-tuple-element.75), channel_id=1, source_target_pairs={{0,16},{8,24},{16,0},{24,8},{1,17},{9,25},{17,1},{25,9},{2,18},{10... | collective-permute-start | bytes 184328 | tf_op jit(solution)/shard_map/ppermute | solution.py:309
  210.7 5.1 %collective-permute-start.38 = (bf16[48,640]{1,0:T(8,128)(2,1)S(1)}, bf16[48,640]{1,0:T(8,128)(2,1)S(1)}, u32[]{:S(2)}, u32[]{:S(2)}) collective-permute-start(bf16[48,640]{1,0:T(8,128)(2,1)S(1)} %get-tuple-element.76), channel_id=1, source_target_pairs={{0,24},{8,16},{16,8},{24,0},{1,25},{9,17},{17,9},{25,1},{2,26},{10... | collective-permute-start | bytes 184328 | tf_op jit(solution)/shard_map/ppermute | solution.py:309
  (12 other events, 144.9 us)
where the time goes:
time: 219 us; the launch traced here: 218 us
  waiting for transfers between devices  101 us (46%)
  starting transfers between devices  68.5 us (31%)
  Pallas kernels  39.6 us (18%)
  local copies, waits for them, and re-layouts  5.39 us (2%)
  other arithmetic  2.76 us (1%)
    ppermute x45, waiting for transfers between devices, mirrored(): lax.ppermute(value, axis, [(i, i ^ apart) for i in range(lax.axis_size(ax...  92.5 us
    ppermute x45, starting transfers between devices, mirrored(): lax.ppermute(value, axis, [(i, i ^ apart) for i in range(lax.axis_size(ax...  64.1 us
    pallas_call x16, Pallas kernels, whole_call(): pl.pallas_call(body, in_specs=[pl.BlockSpec(memory_space=pltpu.SMEM)] * l...  24.5 us
    pallas_call x1, Pallas kernels, exchanged_heads(): pl.pallas_call(lambda *refs: attend_kernel(*refs, step=seq_rows, width=wi...  15.1 us
    all_to_all x1, waiting for transfers between devices, exchanged_heads(): lax.all_to_all(flat, ('sp', 'c'), split_axis=0, concat_axis=0, tiled=True)  8.72 us
    all_to_all x1, starting transfers between devices, exchanged_heads(): lax.all_to_all(flat, ('sp', 'c'), split_axis=0, concat_axis=0, tiled=True)  4.41 us
  transfers between devices with their start and end apart: 46, of which 19 were waited for; matrix products, arithmetic and copies ran while one was open for 1% of the time, Pallas kernels for 12%

commit v1 on v0

--- a/solution.py
+++ b/solution.py
@@ -504,7 +504,7 @@
     capacity = 3 * top_count * tok_rows // (2 * ways)
     slots_all = ways * capacity
     low = jnp.bfloat16
-    head_cols, back_cols = (width * part // 16 // 128 * 128 for part in (6, 5))
+    head_cols, back_cols = (width * part // 16 // 128 * 128 for part in (5, 4))
     tail_cols, rest_cols = width - head_cols, width - back_cols
 
     heads = exchanged_heads(
@@ -561,12 +561,8 @@
     tails = mirrored_all([tail] * lines, "z")
     heads_in = mirrored_all(heads_out, "sp")
     groups = {"near": list(range(ways - 1)), "far": [ways - 1]}
-    head_blocks = {}
-    for group, members in groups.items():
-        block = heads_in[members[0]]
-        if len(members) > 1:
-            block = jnp.concatenate([heads_in[far] for far in members], axis=0)
-        head_blocks[group] = mirrored_all([block] * lines, "z")
+    head_own = jnp.concatenate(heads_in, axis=0)
+    head_blocks = mirrored_all([head_own] * lines, "z")
 
     weights = (expert_gate[0], expert_up[0], down_w[0])
 
@@ -579,12 +575,7 @@
 
     tail_blocks = list(
         whole_call(
-            spread_body,
-            [((lines * capacity, tail_cols), low)] * ways,
-            *tails,
-            *line_routes,
-            head_blocks["near"][0],
-            *weights[:2],
+            spread_body, [((lines * capacity, tail_cols), low)] * ways, *tails, *line_routes, head_own, *weights[:2]
         )
     )
     for members in groups.values():
@@ -598,58 +589,59 @@
         def body(*refs):
             head_refs, tail_refs, out = refs[:lines], refs[lines : lines + len(members)], refs[-1]
             for line in range(lines):
-                for at in range(len(members)):
+                for at, far in enumerate(members):
                     first = (line * len(members) + at) * capacity
-                    out[first : first + capacity, :head_cols] = head_refs[line][at * capacity : (at + 1) * capacity]
+                    out[first : first + capacity, :head_cols] = head_refs[line][far * capacity : (far + 1) * capacity]
                     out[first : first + capacity, head_cols:] = tail_refs[at][line * capacity : (line + 1) * capacity]
 
         (rows,) = whole_call(
             body,
             [((lines * len(members) * capacity, width), low)],
-            *head_blocks[group],
+            *head_blocks,
             *[tail_blocks[far] for far in members],
             *after,
         )
         return rows
 
-    def pair(group, own_part, other_parts):
+    def pair(group, own_part, other_part, *started):
         members = groups[group]
-
-        def body(*refs):
-            part_refs, outs = refs[:cores], refs[cores:]
+        count = len(members)
+
+        def body(own_ref, other_ref, *refs):
+            outs = refs[len(started) :]
             for line in range(lines):
-                for at in range(len(members)):
-                    first = (line * len(members) + at) * capacity
-                    total = part_refs[0][first : first + capacity].astype(jnp.float32)
-                    for part in part_refs[1:]:
-                        total = total + part[first : first + capacity].astype(jnp.float32)
+                if started:
+                    outs[line][: members[0] * capacity] = refs[line][...]
+                for at, far in enumerate(members):
+                    span = slice((line * count + at) * capacity, (line * count + at + 1) * capacity)
+                    total = own_ref[span].astype(jnp.float32) + other_ref[span].astype(jnp.float32)
                     total = total.astype(low)
-                    outs[line][at * capacity : (at + 1) * capacity] = total[:, :back_cols]
+                    outs[line][far * capacity : (far + 1) * capacity] = total[:, :back_cols]
                     outs[lines + at][line * capacity : (line + 1) * capacity] = total[:, back_cols:]
 
-        count = len(members)
         return whole_call(
             body,
-            [((count * capacity, back_cols), low)] * lines + [((lines * capacity, rest_cols), low)] * count,
+            [(((members[-1] + 1) * capacity, back_cols), low)] * lines
+            + [((lines * capacity, rest_cols), low)] * count,
             own_part,
-            *other_parts,
+            other_part,
+            *started,
         )
 
     assert cores == 2
-    tail_back, head_back, before = {}, {}, ()
+    tail_back, started, before, after = {}, (), (), ()
     for group, members in groups.items():
         rows = join(group, *before)
         other_rows = mirrored(rows, "c", 1)
         hidden = expert_call(rows, weights[:2], weights[0].shape[1])
-        after = (hidden,) + tuple(head_back[done][0] for done in head_back)
-        other_part = expert_call(other_rows, weights, width, after)
+        other_part = expert_call(other_rows, weights, width, (hidden,) + after)
         own_part = expert_call(hidden, weights[2:], width)
-        back = pair(group, own_part, [mirrored(other_part, "c", 1)])
-        for at, far in reversed(list(enumerate(members))):
+        back = pair(group, own_part, mirrored(other_part, "c", 1), *started)
+        for at, far in enumerate(members):
             tail_back[far] = mirrored(back[lines + at], "sp", far) if far else back[lines + at]
-        head_back[group] = mirrored_all(back[:lines], "z")
-        before = (other_part,)
+        started, before, after = back[:lines], (other_part,), (back[0],)
     tail_back = [tail_back[far] for far in range(ways)]
+    head_back = mirrored_all(started, "z")
 
     def blend_body(*refs):
         tail_refs, routes_refs, outs = refs[:ways], refs[ways : ways + lines], refs[ways + lines :]
@@ -661,17 +653,12 @@
     tail_sums = mirrored_all(tail_sums, "z")
 
     def total_body(*refs):
-        at = 0
-        for members in groups.values():
-            part_refs = refs[at : at + lines]
-            at += lines
-            total = sum(part[...].astype(jnp.float32) for part in part_refs).astype(low)
-            for index, far in enumerate(members):
-                refs[far - ways][...] = total[index * capacity : (index + 1) * capacity]
-
-    head_sums = whole_call(
-        total_body, [((capacity, back_cols), low)] * ways, *[block for group in groups for block in head_back[group]]
-    )
+        part_refs, outs = refs[:lines], refs[lines:]
+        total = sum(part[...].astype(jnp.float32) for part in part_refs).astype(low)
+        for far in range(ways):
+            outs[far][...] = total[far * capacity : (far + 1) * capacity]
+
+    head_sums = whole_call(total_body, [((capacity, back_cols), low)] * ways, *head_back)
     head_sums = mirrored_all(head_sums, "sp")
 
     def final_body(mixed_ref, routes_ref, *refs):

time: 219 us -> 218 us (level)
  starting transfers between devices: 68.5 us -> 62.8 us
  other arithmetic: 2.76 us -> 5.34 us
    ppermute x45 -> x39, starting transfers between devices: 64.1 us -> 58.4 us  [mirrored(): lax.ppermute(value, axis, [(i, i ^ apart) for i in range(lax.axis_size(ax...]
    ppermute x45 -> x39, waiting for transfers between devices: 92.5 us -> 92.8 us  [mirrored(): lax.ppermute(value, axis, [(i, i ^ apart) for i in range(lax.axis_size(ax...]
  transfers between devices with their start and end apart: 46 -> 40, of which waited for: 19 -> 19; matrix products, arithmetic and copies ran while one was open for 1% -> 1% of each run, Pallas kernels for 12% -> 12%
where the time goes in v1:
time: 218 us; the launch traced here: 217 us
  waiting for transfers between devices  101 us (46%)
  starting transfers between devices  62.8 us (29%)
  Pallas kernels  39.9 us (18%)
  local copies, waits for them, and re-layouts  7.07 us (3%)
  other arithmetic  5.34 us (2%)
    ppermute x39, waiting for transfers between devices, mirrored(): lax.ppermute(value, axis, [(i, i ^ apart) for i in range(lax.axis_size(ax...  92.8 us
    ppermute x39, starting transfers between devices, mirrored(): lax.ppermute(value, axis, [(i, i ^ apart) for i in range(lax.axis_size(ax...  58.4 us
    pallas_call x16, Pallas kernels, whole_call(): pl.pallas_call(body, in_specs=[pl.BlockSpec(memory_space=pltpu.SMEM)] * l...  24.9 us
    pallas_call x1, Pallas kernels, exchanged_heads(): pl.pallas_call(lambda *refs: attend_kernel(*refs, step=seq_rows, width=wi...  15.1 us
    all_to_all x1, waiting for transfers between devices, exchanged_heads(): lax.all_to_all(flat, ('sp', 'c'), split_axis=0, concat_axis=0, tiled=True)  8.72 us
    all_to_all x1, starting transfers between devices, exchanged_heads(): lax.all_to_all(flat, ('sp', 'c'), split_axis=0, concat_axis=0, tiled=True)  4.4 us
  transfers between devices with their start and end apart: 40, of which 19 were waited for; matrix products, arithmetic and copies ran while one was open for 1% of the time, Pallas kernels for 12%

profile of v1, /device:TPU:0, one launch (start us, length us, event | category | flops | bytes accessed | tf_op | source)
XLA Modules:
  0.0 217.1 jit_solution(9284656207897649064)
XLA Ops:
  8.7 3.0 %collective-permute-start = (bf16[384,512]{1,0:T(8,128)(2,1)}, bf16[384,512]{1,0:T(8,128)(2,1)S(1)}, u32[]{:S(2)}, u32[]{:S(2)}) collective-permute-start(bf16[384,512]{1,0:T(8,128)(2,1)} %get-tuple-element.87), channel_id=1, source_target_pairs={{0,8},{8,0},{16,24},{24,16},{1,9},{9,1},{17,25},{25,17},{2,10},{10... | collective-permute-start | bytes 1179656 | tf_op jit(solution)/shard_map/ppermute | solution.py:309
  11.6 1.5 collective-permute-start.1
  15.2 6.6 %collective-permute-done.refs_4_ = bf16[384,512]{1,0:T(8,128)(2,1)S(1)} collective-permute-done((bf16[384,512]{1,0:T(8,128)(2,1)}, bf16[384,512]{1,0:T(8,128)(2,1)S(1)}, u32[]{:S(2)}, u32[]{:S(2)}) %collective-permute-start) | collective-permute-done | bytes 393248 | tf_op jit(solution)/shard_map/ppermute | solution.py:309
  21.8 7.9 %collective-permute-done.1.refs_5_ = bf16[384,512]{1,0:T(8,128)(2,1)S(1)} collective-permute-done((bf16[384,512]{1,0:T(8,128)(2,1)S(1)}, bf16[384,512]{1,0:T(8,128)(2,1)S(1)}, u32[]{:S(2)}, u32[]{:S(2)}) %collective-permute-start.1) | collective-permute-done | bytes 393248 | tf_op jit(solution)/shard_map/ppermute | solution.py:309
  30.6 15.1 %attend.1 = bf16[4,2,256,128]{3,2,1,0:T(8,128)(2,1)} custom-call(f32[3]{0:T(128)S(1)} %pad_maximum_fusion.2.refs_0_, s32[1]{0:T(128)} %bitcast.4.refs_1_, f32[1,128]{1,0:T(1,128)S(1)} %fusion.10.refs_2_, bf16[384,512]{1,0:T(8,128)(2,1)S(1)} %get-tuple-element.86.refs_3_, bf16[384,512]{1,0:T(8,128)(2,1)S(1)} %collective-permute-done.refs_4_, ...), custom_call_target="tpu_custom_call" | custom-call | flops 2013265920 | tf_op jit(solution)/shard_map/attend/pallas_call | solution.py:364
  45.7 4.4 %all-to-all-start = ((bf16[8,256,128]{2,1,0:T(8,128)(2,1)}), bf16[8,256,128]{2,1,0:T(8,128)(2,1)}, u32[]{:S(2)}, u32[]{:S(2)}) async-start(bf16[8,256,128]{2,1,0:T(8,128)(2,1)} %bitcast.50), calls=%async_computation | async-start | bytes 1048576 | tf_op jit(solution)/shard_map/all_to_all | solution.py:380
  51.1 8.7 %all-to-all-done = bf16[8,256,128]{2,1,0:T(8,128)(2,1)} async-done(((bf16[8,256,128]{2,1,0:T(8,128)(2,1)}), bf16[8,256,128]{2,1,0:T(8,128)(2,1)}, u32[]{:S(2)}, u32[]{:S(2)}) %all-to-all-start) | async-done | bytes 524320 | tf_op jit(solution)/shard_map/all_to_all | solution.py:380
  59.9 3.4 %shard_map.181 = (bf16[64,2048]{1,0:T(8,128)(2,1)S(1)}, bf16[64,2048]{1,0:T(8,128)(2,1)S(1)}, bf16[64,2048]{1,0:T(8,128)(2,1)S(1)}, bf16[64,2048]{1,0:T(8,128)(2,1)S(1)}) custom-call(s32[2]{0:T(128)S(1)} %pad_add_fusion.at, bf16[4,2,256,128]{3,2,1,0:T(8,128)(2,1)} %bitcast.17.heads_ref, bf16[256,2048]{1,0:T(8,128)(2,1)} %refs_0_.1, ...), custom_call_target="tpu_custom_call" | custom-call | flops 805306368 | tf_op jit(solution)/shard_map/pallas_call | solution.py:319
  63.3 1.6 collective-permute-start.5
  64.9 2.6 %collective-permute-start.6 = (bf16[64,2048]{1,0:T(8,128)(2,1)S(1)}, bf16[64,2048]{1,0:T(8,128)(2,1)S(1)}, u32[]{:S(2)}, u32[]{:S(2)}) collective-permute-start(bf16[64,2048]{1,0:T(8,128)(2,1)S(1)} %get-tuple-element.53), channel_id=1, source_target_pairs={{0,4},{2,6},{4,0},{6,2},{1,5},{3,7},{5,1},{7,3},{8,12},{10,14},{12... | collective-permute-start | bytes 786440 | tf_op jit(solution)/shard_map/ppermute | solution.py:309
  69.1 3.7 %collective-permute-done.5.refs_1_ = bf16[64,2048]{1,0:T(8,128)(2,1)S(1)} collective-permute-done((bf16[64,2048]{1,0:T(8,128)(2,1)S(1)}, bf16[64,2048]{1,0:T(8,128)(2,1)S(1)}, u32[]{:S(2)}, u32[]{:S(2)}) %collective-permute-start.5) | collective-permute-done | bytes 262176 | tf_op jit(solution)/shard_map/ppermute | solution.py:309
  72.8 12.6 %collective-permute-done.6.refs_2_ = bf16[64,2048]{1,0:T(8,128)(2,1)S(1)} collective-permute-done((bf16[64,2048]{1,0:T(8,128)(2,1)S(1)}, bf16[64,2048]{1,0:T(8,128)(2,1)S(1)}, u32[]{:S(2)}, u32[]{:S(2)}) %collective-permute-start.6) | collective-permute-done | bytes 262176 | tf_op jit(solution)/shard_map/ppermute | solution.py:309
  85.9 3.4 %collective-permute-start.14 = (bf16[64,1408]{1,0:T(8,128)(2,1)S(1)}, bf16[64,1408]{1,0:T(8,128)(2,1)S(1)}, u32[]{:S(2)}, u32[]{:S(2)}) collective-permute-start(bf16[64,1408]{1,0:T(8,128)(2,1)S(1)} %get-tuple-element.60.refs_0_), channel_id=1, source_target_pairs={{0,2},{2,0},{4,6},{6,4},{1,3},{3,1},{5,7},{7,5},{8,10},{10,8},{12,... | collective-permute-start | bytes 540680 | tf_op jit(solution)/shard_map/ppermute | solution.py:309
  90.4 1.4 collective-permute-start.16
  91.8 3.0 %collective-permute-start.8 = (bf16[48,640]{1,0:T(8,128)(2,1)S(1)}, bf16[48,640]{1,0:T(8,128)(2,1)S(1)}, u32[]{:S(2)}, u32[]{:S(2)}) collective-permute-start(bf16[48,640]{1,0:T(8,128)(2,1)S(1)} %get-tuple-element.57), channel_id=1, source_target_pairs={{0,8},{8,0},{16,24},{24,16},{1,9},{9,1},{17,25},{25,17},{2,10},{10... | collective-permute-start | bytes 184328 | tf_op jit(solution)/shard_map/ppermute | solution.py:309
  94.9 2.2 %collective-permute-done.8 = bf16[48,640]{1,0:T(8,128)(2,1)S(1)} collective-permute-done((bf16[48,640]{1,0:T(8,128)(2,1)S(1)}, bf16[48,640]{1,0:T(8,128)(2,1)S(1)}, u32[]{:S(2)}, u32[]{:S(2)}) %collective-permute-start.8) | collective-permute-done | bytes 61472 | tf_op jit(solution)/shard_map/ppermute | solution.py:309
  97.4 3.8 %collective-permute-done.9 = bf16[48,640]{1,0:T(8,128)(2,1)S(1)} collective-permute-done((bf16[48,640]{1,0:T(8,128)(2,1)S(1)}, bf16[48,640]{1,0:T(8,128)(2,1)S(1)}, u32[]{:S(2)}, u32[]{:S(2)}) %collective-permute-start.9) | collective-permute-done | bytes 61472 | tf_op jit(solution)/shard_map/ppermute | solution.py:309
  101.3 1.8 collective-permute-start.10
  103.1 2.7 %collective-permute-start.18 = (f32[4,64]{1,0:T(4,128)S(1)}, f32[4,64]{1,0:T(4,128)S(1)}, u32[]{:S(2)}, u32[]{:S(2)}) collective-permute-start(f32[4,64]{1,0:T(4,128)S(1)} %pad_maximum_fusion.refs_6_.refs_4_.routes_ref), channel_id=1, source_target_pairs={{0,4},{2,6},{4,0},{6,2},{1,5},{3,7},{5,1},{7,3},{8,12},{10,14},{12... | collective-permute-start | bytes 3080 | tf_op jit(solution)/shard_map/ppermute | solution.py:309
  106.4 2.4 %collective-permute-start.19 = (f32[4,64]{1,0:T(4,128)S(1)}, f32[4,64]{1,0:T(4,128)S(1)}, u32[]{:S(2)}, u32[]{:S(2)}) collective-permute-start(f32[4,64]{1,0:T(4,128)S(1)} %pad_maximum_fusion.refs_6_.refs_4_.routes_ref), channel_id=1, source_target_pairs={{0,6},{2,4},{4,2},{6,0},{1,7},{3,5},{5,3},{7,1},{8,14},{10,12},{12... | collective-permute-start | bytes 3080 | tf_op jit(solution)/shard_map/ppermute | solution.py:309
  108.9 3.0 %collective-permute-done.19.refs_7_ = f32[4,64]{1,0:T(4,128)S(1)} collective-permute-done((f32[4,64]{1,0:T(4,128)S(1)}, f32[4,64]{1,0:T(4,128)S(1)}, u32[]{:S(2)}, u32[]{:S(2)}) %collective-permute-start.19) | collective-permute-done | bytes 1056 | tf_op jit(solution)/shard_map/ppermute | solution.py:309
  112.6 2.1 collective-permute-start.21
  115.1 2.9 %collective-permute-start.12 = (bf16[192,640]{1,0:T(8,128)(2,1)S(1)}, bf16[192,640]{1,0:T(8,128)(2,1)S(1)}, u32[]{:S(2)}, u32[]{:S(2)}) collective-permute-start(bf16[192,640]{1,0:T(8,128)(2,1)S(1)} %constant_dynamic-update-slice_fusion.1.refs_8_.refs_0_), channel_id=1, source_target_pairs={{0,4},{2,6},{4,0},{6,2},{1,5},{3,7},{5,1},{7,3},{8,12},{10,14},{12... | collective-permute-start | bytes 737288 | tf_op jit(solution)/shard_map/ppermute | solution.py:309
  118.0 1.5 collective-permute-start.13
  119.5 5.4 %collective-permute-done.11.refs_1_ = bf16[192,640]{1,0:T(8,128)(2,1)S(1)} collective-permute-done((bf16[192,640]{1,0:T(8,128)(2,1)S(1)}, bf16[192,640]{1,0:T(8,128)(2,1)S(1)}, u32[]{:S(2)}, u32[]{:S(2)}) %collective-permute-start.11) | collective-permute-done | bytes 245792 | tf_op jit(solution)/shard_map/ppermute | solution.py:309
  124.9 6.4 %collective-permute-done.12.refs_2_ = bf16[192,640]{1,0:T(8,128)(2,1)S(1)} collective-permute-done((bf16[192,640]{1,0:T(8,128)(2,1)S(1)}, bf16[192,640]{1,0:T(8,128)(2,1)S(1)}, u32[]{:S(2)}, u32[]{:S(2)}) %collective-permute-start.12) | collective-permute-done | bytes 245792 | tf_op jit(solution)/shard_map/ppermute | solution.py:309
  131.5 4.5 %shard_map.185.refs_3_.rows_ref = bf16[576,768]{1,0:T(8,128)(2,1)S(1)} custom-call(bf16[576,2048]{1,0:T(8,128)(2,1)S(1)} %shard_map.184.rows_ref, bf16[2048,768]{1,0:T(8,128)(2,1)S(1)} %bitcast.31, bf16[2048,768]{1,0:T(8,128)(2,1)S(1)} %bitcast.36), custom_call_target="tpu_custom_call" | custom-call | flops 3623878656 | tf_op jit(solution)/shard_map/pallas_call | solution.py:319
  136.1 6.3 %shard_map.186.refs_5_ = bf16[576,2048]{1,0:T(8,128)(2,1)S(1)} custom-call(bf16[576,2048]{1,0:T(8,128)(2,1)S(1)} %collective-permute-done.23.rows_ref, bf16[2048,768]{1,0:T(8,128)(2,1)S(1)} %bitcast.32, bf16[2048,768]{1,0:T(8,128)(2,1)S(1)} %bitcast.37, bf16[768,2048]{1,0:T(8,128)(2,1)S(1)} %bitcast.40, bf16[576,768]{1,0:T(8,128)(2,1)S(1)} %shard_map.185.refs_3_.rows_ref), custom_call_target="tpu_custom_call" | custom-call | flops 5435817984 | tf_op jit(solution)/shard_map/pallas_call | solution.py:319
  142.9 1.5 collective-permute-start.20
  144.4 13.7 %collective-permute-done.20.refs_4_ = bf16[192,1408]{1,0:T(8,128)(2,1)S(1)} collective-permute-done((bf16[192,1408]{1,0:T(8,128)(2,1)S(1)}, bf16[192,1408]{1,0:T(8,128)(2,1)S(1)}, u32[]{:S(2)}, u32[]{:S(2)}) %collective-permute-start.20) | collective-permute-done | bytes 540704 | tf_op jit(solution)/shard_map/ppermute | solution.py:309
  158.2 2.6 %shard_map.190.own_ref = bf16[576,2048]{1,0:T(8,128)(2,1)S(1)} custom-call(bf16[576,768]{1,0:T(8,128)(2,1)S(1)} %shard_map.185.refs_3_.rows_ref, bf16[768,2048]{1,0:T(8,128)(2,1)S(1)} %bitcast.41), custom_call_target="tpu_custom_call" | custom-call | flops 1811939328 | tf_op jit(solution)/shard_map/pallas_call | solution.py:319
  160.8 1.5 shard_map.188.rows_ref.refs_3_
  162.9 2.1 shard_map.192
  166.8 1.6 collective-permute-start.34
  168.6 1.5 collective-permute-start.35
  170.2 3.2 %collective-permute-start.27 = (bf16[192,512]{1,0:T(8,128)(2,1)S(1)}, bf16[192,512]{1,0:T(8,128)(2,1)S(1)}, u32[]{:S(2)}, u32[]{:S(2)}) collective-permute-start(bf16[192,512]{1,0:T(8,128)(2,1)S(1)} %get-tuple-element.70), channel_id=1, source_target_pairs={{0,2},{2,0},{4,6},{6,4},{1,3},{3,1},{5,7},{7,5},{8,10},{10,8},{12,... | collective-permute-start | bytes 589832 | tf_op jit(solution)/shard_map/ppermute | solution.py:309
  173.3 1.4 collective-permute-start.28
  174.8 7.0 %collective-permute-done.33.refs_1_ = bf16[192,1536]{1,0:T(8,128)(2,1)S(1)} collective-permute-done((bf16[192,1536]{1,0:T(8,128)(2,1)S(1)}, bf16[192,1536]{1,0:T(8,128)(2,1)S(1)}, u32[]{:S(2)}, u32[]{:S(2)}) %collective-permute-start.33) | collective-permute-done | bytes 589856 | tf_op jit(solution)/shard_map/ppermute | solution.py:309
  181.7 1.9 collective-permute-start.29
  183.6 10.0 %collective-permute-done.34.refs_2_ = bf16[192,1536]{1,0:T(8,128)(2,1)S(1)} collective-permute-done((bf16[192,1536]{1,0:T(8,128)(2,1)S(1)}, bf16[192,1536]{1,0:T(8,128)(2,1)S(1)}, u32[]{:S(2)}, u32[]{:S(2)}) %collective-permute-start.34) | collective-permute-done | bytes 589856 | tf_op jit(solution)/shard_map/ppermute | solution.py:309
  195.7 3.3 %collective-permute-start.36 = (bf16[64,1536]{1,0:T(8,128)(2,1)S(1)}, bf16[64,1536]{1,0:T(8,128)(2,1)S(1)}, u32[]{:S(2)}, u32[]{:S(2)}) collective-permute-start(bf16[64,1536]{1,0:T(8,128)(2,1)S(1)} %get-tuple-element.82), channel_id=1, source_target_pairs={{0,2},{2,0},{4,6},{6,4},{1,3},{3,1},{5,7},{7,5},{8,10},{10,8},{12,... | collective-permute-start | bytes 589832 | tf_op jit(solution)/shard_map/ppermute | solution.py:309
  198.9 1.6 collective-permute-start.37
  200.5 1.4 collective-permute-start.38
  202.0 1.5 collective-permute-start.30
  203.5 1.7 collective-permute-start.31
  206.1 2.8 %collective-permute-start.32 = (bf16[48,512]{1,0:T(8,128)(2,1)S(1)}, bf16[48,512]{1,0:T(8,128)(2,1)S(1)}, u32[]{:S(2)}, u32[]{:S(2)}) collective-permute-start(bf16[48,512]{1,0:T(8,128)(2,1)S(1)} %get-tuple-element.76), channel_id=1, source_target_pairs={{0,24},{8,16},{16,8},{24,0},{1,25},{9,17},{17,9},{25,1},{2,26},{10... | collective-permute-start | bytes 147464 | tf_op jit(solution)/shard_map/ppermute | solution.py:309
  208.9 2.2 %collective-permute-done.32.refs_3_ = bf16[48,512]{1,0:T(8,128)(2,1)S(1)} collective-permute-done((bf16[48,512]{1,0:T(8,128)(2,1)S(1)}, bf16[48,512]{1,0:T(8,128)(2,1)S(1)}, u32[]{:S(2)}, u32[]{:S(2)}) %collective-permute-start.32) | collective-permute-done | bytes 49184 | tf_op jit(solution)/shard_map/ppermute | solution.py:309
  211.1 4.9 %collective-permute-done.37.refs_6_ = bf16[64,1536]{1,0:T(8,128)(2,1)S(1)} collective-permute-done((bf16[64,1536]{1,0:T(8,128)(2,1)S(1)}, bf16[64,1536]{1,0:T(8,128)(2,1)S(1)}, u32[]{:S(2)}, u32[]{:S(2)}) %collective-permute-start.37) | collective-permute-done | bytes 196640 | tf_op jit(solution)/shard_map/ppermute | solution.py:309
  (106 shorter events, 25.2 us)
Async XLA Ops:
  0.0 7.3 %copy-start.5 = (bf16[512,2,64]{0,2,1:T(8,128)(2,1)S(1)}, bf16[512,2,64]{0,2,1:T(8,128)(2,1)}, u32[]{:S(2)}) copy-start(bf16[512,2,64]{0,2,1:T(8,128)(2,1)} %param.25) | copy-start | bytes 393220
  7.2 8.0 %copy-start.7 = (f32[128]{0:T(128)S(1)}, f32[128]{0:T(128)}, u32[]{:S(2)}) copy-start(f32[128]{0:T(128)} %param.28) | copy-start | bytes 1540
  7.2 8.0 %copy-start.8 = (f32[64]{0:T(128)S(1)}, f32[64]{0:T(128)}, u32[]{:S(2)}) copy-start(f32[64]{0:T(128)} %param.29) | copy-start | bytes 772
  8.7 13.1 %collective-permute-start = (bf16[384,512]{1,0:T(8,128)(2,1)}, bf16[384,512]{1,0:T(8,128)(2,1)S(1)}, u32[]{:S(2)}, u32[]{:S(2)}) collective-permute-start(bf16[384,512]{1,0:T(8,128)(2,1)} %get-tuple-element.87), channel_id=1, source_target_pairs={{0,8},{8,0},{16,24},{24,16},{1,9},{9,1},{17,25},{25,17},{2,10},{10... | collective-permute-start | bytes 1179656 | tf_op jit(solution)/shard_map/ppermute | solution.py:309
  11.6 18.0 %collective-permute-start.1 = (bf16[384,512]{1,0:T(8,128)(2,1)S(1)}, bf16[384,512]{1,0:T(8,128)(2,1)S(1)}, u32[]{:S(2)}, u32[]{:S(2)}) collective-permute-start(bf16[384,512]{1,0:T(8,128)(2,1)S(1)} %get-tuple-element.88), channel_id=1, source_target_pairs={{0,16},{8,24},{16,0},{24,8},{1,17},{9,25},{17,1},{25,9},{2,18},{10... | collective-permute-start | bytes 1179656 | tf_op jit(solution)/shard_map/ppermute | solution.py:309
  13.2 17.5 %collective-permute-start.2 = (bf16[384,512]{1,0:T(8,128)(2,1)S(1)}, bf16[384,512]{1,0:T(8,128)(2,1)S(1)}, u32[]{:S(2)}, u32[]{:S(2)}) collective-permute-start(bf16[384,512]{1,0:T(8,128)(2,1)S(1)} %get-tuple-element.85), channel_id=1, source_target_pairs={{0,24},{8,16},{16,8},{24,0},{1,25},{9,17},{17,9},{25,1},{2,26},{10... | collective-permute-start | bytes 1179656 | tf_op jit(solution)/shard_map/ppermute | solution.py:309
  13.2 46.7 %collective-permute-start.3 = (bf16[256,2048]{1,0:T(8,128)(2,1)}, bf16[256,2048]{1,0:T(8,128)(2,1)}, u32[]{:S(2)}, u32[]{:S(2)}) collective-permute-start(bf16[256,2048]{1,0:T(8,128)(2,1)} %refs_0_.1), channel_id=1, source_target_pairs={{0,1},{1,0},{2,3},{3,2},{4,5},{5,4},{6,7},{7,6},{8,9},{9,8},{10,11... | collective-permute-start | bytes 3145736 | tf_op jit(solution)/shard_map/ppermute | solution.py:309
  13.2 38.0 %collective-permute-start.4 = (bf16[128,2048]{1,0:T(8,128)(2,1)}, bf16[128,2048]{1,0:T(8,128)(2,1)}, u32[]{:S(2)}, u32[]{:S(2)}) collective-permute-start(bf16[128,2048]{1,0:T(8,128)(2,1)} %refs_1_.1), channel_id=1, source_target_pairs={{0,1},{1,0},{2,3},{3,2},{4,5},{5,4},{6,7},{7,6},{8,9},{9,8},{10,11... | collective-permute-start | bytes 1572872 | tf_op jit(solution)/shard_map/ppermute | solution.py:309
  30.6 19.5 %copy-start.6 = (s32[64,2]{0,1:T(2,128)S(1)}, s32[64,2]{0,1:T(2,128)}, u32[]{:S(2)}) copy-start(s32[64,2]{0,1:T(2,128)} %param.33) | copy-start | bytes 1540
  45.7 39.7 %copy-start.3 = (bf16[64,2048]{1,0:T(8,128)(2,1)S(1)}, bf16[64,2048]{1,0:T(8,128)(2,1)}, u32[]{:S(2)}) copy-start(bf16[64,2048]{1,0:T(8,128)(2,1)} %refs_4_.1) | copy-start | bytes 786436
  45.7 39.7 %copy-start.4 = (f32[2048]{0:T(1024)S(1)}, f32[2048]{0:T(1024)}, u32[]{:S(2)}) copy-start(f32[2048]{0:T(1024)} %param.32) | copy-start | bytes 24580
  45.7 66.2 %copy-start.1 = (bf16[1,2048,768]{2,1,0:T(8,128)(2,1)S(1)}, bf16[1,2048,768]{2,1,0:T(8,128)(2,1)}, u32[]{:S(2)}) copy-start(bf16[1,2048,768]{2,1,0:T(8,128)(2,1)} %param.36) | copy-start | bytes 9437188
  45.7 14.1 %all-to-all-start = ((bf16[8,256,128]{2,1,0:T(8,128)(2,1)}), bf16[8,256,128]{2,1,0:T(8,128)(2,1)}, u32[]{:S(2)}, u32[]{:S(2)}) async-start(bf16[8,256,128]{2,1,0:T(8,128)(2,1)} %bitcast.50), calls=%async_computation | async-start | bytes 1048576 | tf_op jit(solution)/shard_map/all_to_all | solution.py:380
  59.9 52.1 %copy-start = (bf16[1,2048,768]{2,1,0:T(8,128)(2,1)S(1)}, bf16[1,2048,768]{2,1,0:T(8,128)(2,1)}, u32[]{:S(2)}) copy-start(bf16[1,2048,768]{2,1,0:T(8,128)(2,1)} %param.35) | copy-start | bytes 9437188
  63.3 9.5 %collective-permute-start.5 = (bf16[64,2048]{1,0:T(8,128)(2,1)S(1)}, bf16[64,2048]{1,0:T(8,128)(2,1)S(1)}, u32[]{:S(2)}, u32[]{:S(2)}) collective-permute-start(bf16[64,2048]{1,0:T(8,128)(2,1)S(1)} %get-tuple-element.52), channel_id=1, source_target_pairs={{0,2},{2,0},{4,6},{6,4},{1,3},{3,1},{5,7},{7,5},{8,10},{10,8},{12,... | collective-permute-start | bytes 786440 | tf_op jit(solution)/shard_map/ppermute | solution.py:309
  64.9 20.5 %collective-permute-start.6 = (bf16[64,2048]{1,0:T(8,128)(2,1)S(1)}, bf16[64,2048]{1,0:T(8,128)(2,1)S(1)}, u32[]{:S(2)}, u32[]{:S(2)}) collective-permute-start(bf16[64,2048]{1,0:T(8,128)(2,1)S(1)} %get-tuple-element.53), channel_id=1, source_target_pairs={{0,4},{2,6},{4,0},{6,2},{1,5},{3,7},{5,1},{7,3},{8,12},{10,14},{12... | collective-permute-start | bytes 786440 | tf_op jit(solution)/shard_map/ppermute | solution.py:309
  67.5 17.9 %collective-permute-start.7 = (bf16[64,2048]{1,0:T(8,128)(2,1)S(1)}, bf16[64,2048]{1,0:T(8,128)(2,1)S(1)}, u32[]{:S(2)}, u32[]{:S(2)}) collective-permute-start(bf16[64,2048]{1,0:T(8,128)(2,1)S(1)} %get-tuple-element.54), channel_id=1, source_target_pairs={{0,6},{2,4},{4,2},{6,0},{1,7},{3,5},{5,3},{7,1},{8,14},{10,12},{12... | collective-permute-start | bytes 786440 | tf_op jit(solution)/shard_map/ppermute | solution.py:309
  68.4 34.7 %collective-permute-start.17 = (f32[4,64]{1,0:T(4,128)S(1)}, f32[4,64]{1,0:T(4,128)S(1)}, u32[]{:S(2)}, u32[]{:S(2)}) collective-permute-start(f32[4,64]{1,0:T(4,128)S(1)} %pad_maximum_fusion.refs_6_.refs_4_.routes_ref), channel_id=1, source_target_pairs={{0,2},{2,0},{4,6},{6,4},{1,3},{3,1},{5,7},{7,5},{8,10},{10,8},{12,... | collective-permute-start | bytes 3080 | tf_op jit(solution)/shard_map/ppermute | solution.py:309
  85.9 26.0 %collective-permute-start.14 = (bf16[64,1408]{1,0:T(8,128)(2,1)S(1)}, bf16[64,1408]{1,0:T(8,128)(2,1)S(1)}, u32[]{:S(2)}, u32[]{:S(2)}) collective-permute-start(bf16[64,1408]{1,0:T(8,128)(2,1)S(1)} %get-tuple-element.60.refs_0_), channel_id=1, source_target_pairs={{0,2},{2,0},{4,6},{6,4},{1,3},{3,1},{5,7},{7,5},{8,10},{10,8},{12,... | collective-permute-start | bytes 540680 | tf_op jit(solution)/shard_map/ppermute | solution.py:309
  89.4 22.5 %collective-permute-start.15 = (bf16[64,1408]{1,0:T(8,128)(2,1)S(1)}, bf16[64,1408]{1,0:T(8,128)(2,1)S(1)}, u32[]{:S(2)}, u32[]{:S(2)}) collective-permute-start(bf16[64,1408]{1,0:T(8,128)(2,1)S(1)} %get-tuple-element.60.refs_0_), channel_id=1, source_target_pairs={{0,4},{2,6},{4,0},{6,2},{1,5},{3,7},{5,1},{7,3},{8,12},{10,14},{12... | collective-permute-start | bytes 540680 | tf_op jit(solution)/shard_map/ppermute | solution.py:309
  90.4 21.5 %collective-permute-start.16 = (bf16[64,1408]{1,0:T(8,128)(2,1)S(1)}, bf16[64,1408]{1,0:T(8,128)(2,1)S(1)}, u32[]{:S(2)}, u32[]{:S(2)}) collective-permute-start(bf16[64,1408]{1,0:T(8,128)(2,1)S(1)} %get-tuple-element.60.refs_0_), channel_id=1, source_target_pairs={{0,6},{2,4},{4,2},{6,0},{1,7},{3,5},{5,3},{7,1},{8,14},{10,12},{12... | collective-permute-start | bytes 540680 | tf_op jit(solution)/shard_map/ppermute | solution.py:309
  91.8 5.2 %collective-permute-start.8 = (bf16[48,640]{1,0:T(8,128)(2,1)S(1)}, bf16[48,640]{1,0:T(8,128)(2,1)S(1)}, u32[]{:S(2)}, u32[]{:S(2)}) collective-permute-start(bf16[48,640]{1,0:T(8,128)(2,1)S(1)} %get-tuple-element.57), channel_id=1, source_target_pairs={{0,8},{8,0},{16,24},{24,16},{1,9},{9,1},{17,25},{25,17},{2,10},{10... | collective-permute-start | bytes 184328 | tf_op jit(solution)/shard_map/ppermute | solution.py:309
  97.1 4.2 %collective-permute-start.9 = (bf16[48,640]{1,0:T(8,128)(2,1)S(1)}, bf16[48,640]{1,0:T(8,128)(2,1)S(1)}, u32[]{:S(2)}, u32[]{:S(2)}) collective-permute-start(bf16[48,640]{1,0:T(8,128)(2,1)S(1)} %get-tuple-element.58), channel_id=1, source_target_pairs={{0,16},{8,24},{16,0},{24,8},{1,17},{9,25},{17,1},{25,9},{2,18},{10... | collective-permute-start | bytes 184328 | tf_op jit(solution)/shard_map/ppermute | solution.py:309
  101.3 5.1 %collective-permute-start.10 = (bf16[48,640]{1,0:T(8,128)(2,1)S(1)}, bf16[48,640]{1,0:T(8,128)(2,1)S(1)}, u32[]{:S(2)}, u32[]{:S(2)}) collective-permute-start(bf16[48,640]{1,0:T(8,128)(2,1)S(1)} %get-tuple-element.59), channel_id=1, source_target_pairs={{0,24},{8,16},{16,8},{24,0},{1,25},{9,17},{17,9},{25,1},{2,26},{10... | collective-permute-start | bytes 184328 | tf_op jit(solution)/shard_map/ppermute | solution.py:309
  103.1 5.7 %collective-permute-start.18 = (f32[4,64]{1,0:T(4,128)S(1)}, f32[4,64]{1,0:T(4,128)S(1)}, u32[]{:S(2)}, u32[]{:S(2)}) collective-permute-start(f32[4,64]{1,0:T(4,128)S(1)} %pad_maximum_fusion.refs_6_.refs_4_.routes_ref), channel_id=1, source_target_pairs={{0,4},{2,6},{4,0},{6,2},{1,5},{3,7},{5,1},{7,3},{8,12},{10,14},{12... | collective-permute-start | bytes 3080 | tf_op jit(solution)/shard_map/ppermute | solution.py:309
  106.4 5.5 %collective-permute-start.19 = (f32[4,64]{1,0:T(4,128)S(1)}, f32[4,64]{1,0:T(4,128)S(1)}, u32[]{:S(2)}, u32[]{:S(2)}) collective-permute-start(f32[4,64]{1,0:T(4,128)S(1)} %pad_maximum_fusion.refs_6_.refs_4_.routes_ref), channel_id=1, source_target_pairs={{0,6},{2,4},{4,2},{6,0},{1,7},{3,5},{5,3},{7,1},{8,14},{10,12},{12... | collective-permute-start | bytes 3080 | tf_op jit(solution)/shard_map/ppermute | solution.py:309
  112.6 18.6 %collective-permute-start.21 = (bf16[192,1408]{1,0:T(8,128)(2,1)S(1)}, bf16[192,1408]{1,0:T(8,128)(2,1)S(1)}, u32[]{:S(2)}, u32[]{:S(2)}) collective-permute-start(bf16[192,1408]{1,0:T(8,128)(2,1)S(1)} %get-tuple-element.63), channel_id=1, source_target_pairs={{0,8},{8,0},{16,24},{24,16},{1,9},{9,1},{17,25},{25,17},{2,10},{10... | collective-permute-start | bytes 1622024 | tf_op jit(solution)/shard_map/ppermute | solution.py:309
  114.8 16.5 %collective-permute-start.22 = (bf16[192,1408]{1,0:T(8,128)(2,1)S(1)}, bf16[192,1408]{1,0:T(8,128)(2,1)S(1)}, u32[]{:S(2)}, u32[]{:S(2)}) collective-permute-start(bf16[192,1408]{1,0:T(8,128)(2,1)S(1)} %get-tuple-element.64), channel_id=1, source_target_pairs={{0,16},{8,24},{16,0},{24,8},{1,17},{9,25},{17,1},{25,9},{2,18},{10... | collective-permute-start | bytes 1622024 | tf_op jit(solution)/shard_map/ppermute | solution.py:309
  115.1 9.8 %collective-permute-start.11 = (bf16[192,640]{1,0:T(8,128)(2,1)S(1)}, bf16[192,640]{1,0:T(8,128)(2,1)S(1)}, u32[]{:S(2)}, u32[]{:S(2)}) collective-permute-start(bf16[192,640]{1,0:T(8,128)(2,1)S(1)} %constant_dynamic-update-slice_fusion.1.refs_8_.refs_0_), channel_id=1, source_target_pairs={{0,2},{2,0},{4,6},{6,4},{1,3},{3,1},{5,7},{7,5},{8,10},{10,8},{12,... | collective-permute-start | bytes 737288 | tf_op jit(solution)/shard_map/ppermute | solution.py:309
  115.1 16.1 %collective-permute-start.12 = (bf16[192,640]{1,0:T(8,128)(2,1)S(1)}, bf16[192,640]{1,0:T(8,128)(2,1)S(1)}, u32[]{:S(2)}, u32[]{:S(2)}) collective-permute-start(bf16[192,640]{1,0:T(8,128)(2,1)S(1)} %constant_dynamic-update-slice_fusion.1.refs_8_.refs_0_), channel_id=1, source_target_pairs={{0,4},{2,6},{4,0},{6,2},{1,5},{3,7},{5,1},{7,3},{8,12},{10,14},{12... | collective-permute-start | bytes 737288 | tf_op jit(solution)/shard_map/ppermute | solution.py:309
  118.0 13.2 %collective-permute-start.13 = (bf16[192,640]{1,0:T(8,128)(2,1)S(1)}, bf16[192,640]{1,0:T(8,128)(2,1)S(1)}, u32[]{:S(2)}, u32[]{:S(2)}) collective-permute-start(bf16[192,640]{1,0:T(8,128)(2,1)S(1)} %constant_dynamic-update-slice_fusion.1.refs_8_.refs_0_), channel_id=1, source_target_pairs={{0,6},{2,4},{4,2},{6,0},{1,7},{3,5},{5,3},{7,1},{8,14},{10,12},{12... | collective-permute-start | bytes 737288 | tf_op jit(solution)/shard_map/ppermute | solution.py:309
  131.4 4.6 %collective-permute-start.23 = (bf16[576,2048]{1,0:T(8,128)(2,1)S(1)}, bf16[576,2048]{1,0:T(8,128)(2,1)S(1)}, u32[]{:S(2)}, u32[]{:S(2)}) collective-permute-start(bf16[576,2048]{1,0:T(8,128)(2,1)S(1)} %shard_map.184.rows_ref), channel_id=1, source_target_pairs={{0,1},{1,0},{2,3},{3,2},{4,5},{5,4},{6,7},{7,6},{8,9},{9,8},{10,11... | collective-permute-start | bytes 7077896 | tf_op jit(solution)/shard_map/ppermute | solution.py:309
  142.3 20.0 %collective-permute-start.25 = (bf16[576,2048]{1,0:T(8,128)(2,1)S(1)}, bf16[576,2048]{1,0:T(8,128)(2,1)S(1)}, u32[]{:S(2)}, u32[]{:S(2)}) collective-permute-start(bf16[576,2048]{1,0:T(8,128)(2,1)S(1)} %shard_map.186.refs_5_), channel_id=1, source_target_pairs={{0,1},{1,0},{2,3},{3,2},{4,5},{5,4},{6,7},{7,6},{8,9},{9,8},{10,11... | collective-permute-start | bytes 7077896 | tf_op jit(solution)/shard_map/ppermute | solution.py:309
  142.9 15.2 %collective-permute-start.20 = (bf16[192,1408]{1,0:T(8,128)(2,1)S(1)}, bf16[192,1408]{1,0:T(8,128)(2,1)S(1)}, u32[]{:S(2)}, u32[]{:S(2)}) collective-permute-start(bf16[192,1408]{1,0:T(8,128)(2,1)S(1)} %get-tuple-element.61), channel_id=1, source_target_pairs={{0,24},{8,16},{16,8},{24,0},{1,25},{9,17},{17,9},{25,1},{2,26},{10... | collective-permute-start | bytes 1622024 | tf_op jit(solution)/shard_map/ppermute | solution.py:309
  158.1 4.7 %collective-permute-start.24 = (bf16[192,2048]{1,0:T(8,128)(2,1)S(1)}, bf16[192,2048]{1,0:T(8,128)(2,1)S(1)}, u32[]{:S(2)}, u32[]{:S(2)}) collective-permute-start(bf16[192,2048]{1,0:T(8,128)(2,1)S(1)} %shard_map.187.rows_ref), channel_id=1, source_target_pairs={{0,1},{1,0},{2,3},{3,2},{4,5},{5,4},{6,7},{7,6},{8,9},{9,8},{10,11... | collective-permute-start | bytes 2359304 | tf_op jit(solution)/shard_map/ppermute | solution.py:309
  165.0 3.5 %collective-permute-start.26 = (bf16[192,2048]{1,0:T(8,128)(2,1)S(1)}, bf16[192,2048]{1,0:T(8,128)(2,1)S(1)}, u32[]{:S(2)}, u32[]{:S(2)}) collective-permute-start(bf16[192,2048]{1,0:T(8,128)(2,1)S(1)} %shard_map.192), channel_id=1, source_target_pairs={{0,1},{1,0},{2,3},{3,2},{4,5},{5,4},{6,7},{7,6},{8,9},{9,8},{10,11... | collective-permute-start | bytes 2359304 | tf_op jit(solution)/shard_map/ppermute | solution.py:309
  165.5 16.2 %collective-permute-start.33 = (bf16[192,1536]{1,0:T(8,128)(2,1)S(1)}, bf16[192,1536]{1,0:T(8,128)(2,1)S(1)}, u32[]{:S(2)}, u32[]{:S(2)}) collective-permute-start(bf16[192,1536]{1,0:T(8,128)(2,1)S(1)} %get-tuple-element.78), channel_id=1, source_target_pairs={{0,8},{8,0},{16,24},{24,16},{1,9},{9,1},{17,25},{25,17},{2,10},{10... | collective-permute-start | bytes 1769480 | tf_op jit(solution)/shard_map/ppermute | solution.py:309
  166.8 26.8 %collective-permute-start.34 = (bf16[192,1536]{1,0:T(8,128)(2,1)S(1)}, bf16[192,1536]{1,0:T(8,128)(2,1)S(1)}, u32[]{:S(2)}, u32[]{:S(2)}) collective-permute-start(bf16[192,1536]{1,0:T(8,128)(2,1)S(1)} %get-tuple-element.79), channel_id=1, source_target_pairs={{0,16},{8,24},{16,0},{24,8},{1,17},{9,25},{17,1},{25,9},{2,18},{10... | collective-permute-start | bytes 1769480 | tf_op jit(solution)/shard_map/ppermute | solution.py:309
  168.6 26.0 %collective-permute-start.35 = (bf16[192,1536]{1,0:T(8,128)(2,1)S(1)}, bf16[192,1536]{1,0:T(8,128)(2,1)S(1)}, u32[]{:S(2)}, u32[]{:S(2)}) collective-permute-start(bf16[192,1536]{1,0:T(8,128)(2,1)S(1)} %get-tuple-element.80), channel_id=1, source_target_pairs={{0,24},{8,16},{16,8},{24,0},{1,25},{9,17},{17,9},{25,1},{2,26},{10... | collective-permute-start | bytes 1769480 | tf_op jit(solution)/shard_map/ppermute | solution.py:309
  170.2 30.3 %collective-permute-start.27 = (bf16[192,512]{1,0:T(8,128)(2,1)S(1)}, bf16[192,512]{1,0:T(8,128)(2,1)S(1)}, u32[]{:S(2)}, u32[]{:S(2)}) collective-permute-start(bf16[192,512]{1,0:T(8,128)(2,1)S(1)} %get-tuple-element.70), channel_id=1, source_target_pairs={{0,2},{2,0},{4,6},{6,4},{1,3},{3,1},{5,7},{7,5},{8,10},{10,8},{12,... | collective-permute-start | bytes 589832 | tf_op jit(solution)/shard_map/ppermute | solution.py:309
  173.3 28.5 %collective-permute-start.28 = (bf16[192,512]{1,0:T(8,128)(2,1)S(1)}, bf16[192,512]{1,0:T(8,128)(2,1)S(1)}, u32[]{:S(2)}, u32[]{:S(2)}) collective-permute-start(bf16[192,512]{1,0:T(8,128)(2,1)S(1)} %get-tuple-element.71), channel_id=1, source_target_pairs={{0,4},{2,6},{4,0},{6,2},{1,5},{3,7},{5,1},{7,3},{8,12},{10,14},{12... | collective-permute-start | bytes 589832 | tf_op jit(solution)/shard_map/ppermute | solution.py:309
  181.7 20.1 %collective-permute-start.29 = (bf16[192,512]{1,0:T(8,128)(2,1)S(1)}, bf16[192,512]{1,0:T(8,128)(2,1)S(1)}, u32[]{:S(2)}, u32[]{:S(2)}) collective-permute-start(bf16[192,512]{1,0:T(8,128)(2,1)S(1)} %get-tuple-element.72), channel_id=1, source_target_pairs={{0,6},{2,4},{4,2},{6,0},{1,7},{3,5},{5,3},{7,1},{8,14},{10,12},{12... | collective-permute-start | bytes 589832 | tf_op jit(solution)/shard_map/ppermute | solution.py:309
  195.7 15.5 %collective-permute-start.36 = (bf16[64,1536]{1,0:T(8,128)(2,1)S(1)}, bf16[64,1536]{1,0:T(8,128)(2,1)S(1)}, u32[]{:S(2)}, u32[]{:S(2)}) collective-permute-start(bf16[64,1536]{1,0:T(8,128)(2,1)S(1)} %get-tuple-element.82), channel_id=1, source_target_pairs={{0,2},{2,0},{4,6},{6,4},{1,3},{3,1},{5,7},{7,5},{8,10},{10,8},{12,... | collective-permute-start | bytes 589832 | tf_op jit(solution)/shard_map/ppermute | solution.py:309
  198.9 17.1 %collective-permute-start.37 = (bf16[64,1536]{1,0:T(8,128)(2,1)S(1)}, bf16[64,1536]{1,0:T(8,128)(2,1)S(1)}, u32[]{:S(2)}, u32[]{:S(2)}) collective-permute-start(bf16[64,1536]{1,0:T(8,128)(2,1)S(1)} %get-tuple-element.83), channel_id=1, source_target_pairs={{0,4},{2,6},{4,0},{6,2},{1,5},{3,7},{5,1},{7,3},{8,12},{10,14},{12... | collective-permute-start | bytes 589832 | tf_op jit(solution)/shard_map/ppermute | solution.py:309
  200.5 15.5 %collective-permute-start.38 = (bf16[64,1536]{1,0:T(8,128)(2,1)S(1)}, bf16[64,1536]{1,0:T(8,128)(2,1)S(1)}, u32[]{:S(2)}, u32[]{:S(2)}) collective-permute-start(bf16[64,1536]{1,0:T(8,128)(2,1)S(1)} %get-tuple-element.84), channel_id=1, source_target_pairs={{0,6},{2,4},{4,2},{6,0},{1,7},{3,5},{5,3},{7,1},{8,14},{10,12},{12... | collective-permute-start | bytes 589832 | tf_op jit(solution)/shard_map/ppermute | solution.py:309
  202.0 4.2 %collective-permute-start.30 = (bf16[48,512]{1,0:T(8,128)(2,1)S(1)}, bf16[48,512]{1,0:T(8,128)(2,1)S(1)}, u32[]{:S(2)}, u32[]{:S(2)}) collective-permute-start(bf16[48,512]{1,0:T(8,128)(2,1)S(1)} %get-tuple-element.74), channel_id=1, source_target_pairs={{0,8},{8,0},{16,24},{24,16},{1,9},{9,1},{17,25},{25,17},{2,10},{10... | collective-permute-start | bytes 147464 | tf_op jit(solution)/shard_map/ppermute | solution.py:309
  203.5 5.4 %collective-permute-start.31 = (bf16[48,512]{1,0:T(8,128)(2,1)S(1)}, bf16[48,512]{1,0:T(8,128)(2,1)S(1)}, u32[]{:S(2)}, u32[]{:S(2)}) collective-permute-start(bf16[48,512]{1,0:T(8,128)(2,1)S(1)} %get-tuple-element.75), channel_id=1, source_target_pairs={{0,16},{8,24},{16,0},{24,8},{1,17},{9,25},{17,1},{25,9},{2,18},{10... | collective-permute-start | bytes 147464 | tf_op jit(solution)/shard_map/ppermute | solution.py:309
  206.1 5.0 %collective-permute-start.32 = (bf16[48,512]{1,0:T(8,128)(2,1)S(1)}, bf16[48,512]{1,0:T(8,128)(2,1)S(1)}, u32[]{:S(2)}, u32[]{:S(2)}) collective-permute-start(bf16[48,512]{1,0:T(8,128)(2,1)S(1)} %get-tuple-element.76), channel_id=1, source_target_pairs={{0,24},{8,16},{16,8},{24,0},{1,25},{9,17},{17,9},{25,1},{2,26},{10... | collective-permute-start | bytes 147464 | tf_op jit(solution)/shard_map/ppermute | solution.py:309
  (3 other events, 17.6 us)

commit v2 on v0

--- a/solution.py
+++ b/solution.py
@@ -290,10 +290,10 @@
     mixed = outputs[0] - scalars[1] * outputs[1]
     square = jnp.sum(mixed * mixed, axis=1, keepdims=True) * scalars[2]
     normed = (mixed * lax.rsqrt(square + EPS) * gain[...]).astype(jnp.bfloat16)
-    cores = out.shape[1]
+    pairs, cores = out.shape[1:3]
     for at in range(step // block):
-        begin = at // cores * block
-        out[0, at % cores, begin : begin + block] = normed[at * block : (at + 1) * block]
+        begin = at // (pairs * cores) * block
+        out[0, at // cores % pairs, at % cores, begin : begin + block] = normed[at * block : (at + 1) * block]
 
 
 def widen(values, width):
@@ -330,7 +330,7 @@
 def exchanged_heads(query_a, key_a, value_a, query_b, key_b, value_b, mix_a, mix_b, head_gain_a, head_gain_b, block):
     seq_rows, heads_a, _ = query_a.shape
     ways = lax.axis_size("sp")
-    cores = lax.axis_size("c")
+    cores, pair_lines = lax.axis_size("c"), lax.axis_size("zl")
     place = lax.axis_index("sp")
     groups = ((query_a, key_a, value_a), (query_b, key_b, value_b))
     width = -(-max(group[2].shape[2] for group in groups) // 128) * 128
@@ -359,14 +359,14 @@
         ]
     )
     pairs = (ways * seq_rows) * (ways + 1) * seq_rows
-    shape = (ways, cores, seq_rows // cores, width)
+    shape = (ways, pair_lines, cores, seq_rows // (pair_lines * cores), width)
     smem = pl.BlockSpec(memory_space=pltpu.SMEM)
     mixed = pl.pallas_call(
         lambda *refs: attend_kernel(*refs, step=seq_rows, width=width, maps=maps, block=block),
         grid=(ways,),
         in_specs=[smem, smem, pl.BlockSpec((1, width), lambda index: (0, 0))]
         + [pl.BlockSpec(piece.shape, lambda index: (0, 0)) for piece in pieces],
-        out_specs=pl.BlockSpec((1,) + shape[1:], lambda index: (index, 0, 0, 0)),
+        out_specs=pl.BlockSpec((1,) + shape[1:], lambda index: (index, 0, 0, 0, 0)),
         out_shape=pltpu.HBM(shape, jnp.bfloat16),
         scratch_shapes=[
             pltpu.VMEM((2, ways, seq_rows, seq_rows), jnp.float32),
@@ -376,29 +376,35 @@
         cost_estimate=pl.CostEstimate(flops=2 * pairs * (maps + width), bytes_accessed=0, transcendentals=pairs),
         name="attend",
     )(scalars, place[None].astype(jnp.int32), gain[None, :], *pieces)
-    flat = mixed.reshape((ways * cores,) + shape[2:])
-    return lax.all_to_all(flat, ("sp", "c"), split_axis=0, concat_axis=0, tiled=True).reshape(shape)
-
-
-def project(heads, proj_a, proj_b, lines, block, heads_a):
-    ways, cores, rows, _ = heads.shape
+    flat = mixed.reshape((-1,) + shape[3:])
+    return lax.all_to_all(flat, ("sp", "zl", "c"), split_axis=0, concat_axis=0, tiled=True).reshape(shape)
+
+
+def project(heads, proj_a, proj_b, block, heads_a):
+    ways, pair_lines, cores, rows, _ = heads.shape
     model = proj_a.shape[1]
+    lines = rows // block
     weights = []
-    for apart in range(cores):
-        weights += [proj_a, proj_b] if apart == 0 else [mirrored(proj_a, "c", apart), mirrored(proj_b, "c", apart)]
-    where = jnp.stack([lax.axis_index("c"), lax.axis_index("z")]).astype(jnp.int32)
+    for line in range(pair_lines):
+        found = (proj_a, proj_b)
+        if line > 0:
+            found = [mirrored(array, "zl", line) for array in found]
+        weights += found
+        for apart in range(1, cores):
+            weights += [mirrored(array, "c", apart) for array in found]
+    where = jnp.stack([lax.axis_index(axis) for axis in ("c", "zl", "zh")]).astype(jnp.int32)
     step = math.gcd(model, 512)
     narrow = proj_b.shape[0] // (ways - heads_a)
     wide = proj_a.shape[0] // heads_a
 
     def body(at, heads_ref, *refs):
-        sets, outs = refs[: 2 * cores], refs[2 * cores :]
+        sets, outs = refs[: len(weights)], refs[len(weights) :]
         pairs = []
-        for apart in range(cores):
-            core = at[0] ^ apart
+        for apart in range(pair_lines * cores):
+            core, line = at[0] ^ apart % cores, at[1] ^ apart // cores
 
             def taken(head, used):
-                found = [heads_ref[head, core, pl.ds((at[1] ^ far) * block, block), :] for far in range(lines)]
+                found = [heads_ref[head, line, core, pl.ds((at[2] ^ far) * block, block), :] for far in range(lines)]
                 return jnp.concatenate(found, axis=0)[:, :used]
 
             left_a = jnp.concatenate([taken(head, wide) for head in range(heads_a)], axis=1)
@@ -419,7 +425,7 @@
         heads,
         *weights,
         scalars=(where,),
-        flops=2 * rows * model * (proj_a.shape[0] + proj_b.shape[0]) * cores,
+        flops=rows * model * (proj_a.shape[0] + proj_b.shape[0]) * len(weights),
     )
 
 
@@ -497,14 +503,15 @@
     expert_up,
     down_w,
 ):
-    ways, lines, cores = (lax.axis_size(axis) for axis in ("sp", "z", "c"))
+    line_axes = ("zh", "zl")
+    ways, cores, line_pairs, lines = (lax.axis_size(axis) for axis in ("sp", "c", "zh", line_axes))
     place = lax.axis_index("sp")
     tok_rows, width = resid.shape
     top_count = route_ids.shape[1]
     capacity = 3 * top_count * tok_rows // (2 * ways)
     slots_all = ways * capacity
     low = jnp.bfloat16
-    head_cols, back_cols = (width * part // 16 // 128 * 128 for part in (6, 5))
+    head_cols, back_cols = (width * part // 16 // 128 * 128 for part in (4, 5))
     tail_cols, rest_cols = width - head_cols, width - back_cols
 
     heads = exchanged_heads(
@@ -513,7 +520,7 @@
 
     slots = slot_numbers(route_ids ^ place, ways, capacity)
     routes = jnp.concatenate([jnp.transpose(slots).astype(jnp.float32), jnp.transpose(route_weights)], axis=0)
-    line_routes = mirrored_all([routes] * lines, "z")
+    line_routes = mirrored_all([routes] * lines, line_axes)
 
     def hits(routes_ref, which):
         lookup = lax.broadcasted_iota(jnp.int32, (slots_all, tok_rows), 0)
@@ -535,11 +542,12 @@
             total = piece if total is None else total + piece
         return total
 
-    parts = project(heads, proj_a, proj_b, lines, tok_rows, query_a.shape[1])
-    parts = mirrored_all(parts, "z")
+    parts = project(heads, proj_a, proj_b, tok_rows, query_a.shape[1])
+    parts = mirrored_all(parts, "zh")
 
     def norm_body(*refs):
-        part_refs, (resid_ref, gain_ref, routes_ref), outs = refs[:lines], refs[lines : lines + 3], refs[lines + 3 :]
+        part_refs, outs = refs[:line_pairs], refs[line_pairs + 3 :]
+        resid_ref, gain_ref, routes_ref = refs[line_pairs : line_pairs + 3]
         mixed = resid_ref[...].astype(jnp.float32)
         for part in part_refs:
             mixed = mixed + part[...].astype(jnp.float32)
@@ -558,15 +566,11 @@
         norm_gain[None, :],
         routes,
     )
-    tails = mirrored_all([tail] * lines, "z")
+    tails = mirrored_all([tail] * lines, line_axes)
     heads_in = mirrored_all(heads_out, "sp")
     groups = {"near": list(range(ways - 1)), "far": [ways - 1]}
-    head_blocks = {}
-    for group, members in groups.items():
-        block = heads_in[members[0]]
-        if len(members) > 1:
-            block = jnp.concatenate([heads_in[far] for far in members], axis=0)
-        head_blocks[group] = mirrored_all([block] * lines, "z")
+    head_own = jnp.concatenate(heads_in, axis=0)
+    head_blocks = mirrored_all([head_own] * lines, line_axes)
 
     weights = (expert_gate[0], expert_up[0], down_w[0])
 
@@ -579,12 +583,7 @@
 
     tail_blocks = list(
         whole_call(
-            spread_body,
-            [((lines * capacity, tail_cols), low)] * ways,
-            *tails,
-            *line_routes,
-            head_blocks["near"][0],
-            *weights[:2],
+            spread_body, [((lines * capacity, tail_cols), low)] * ways, *tails, *line_routes, head_own, *weights[:2]
         )
     )
     for members in groups.values():
@@ -598,15 +597,15 @@
         def body(*refs):
             head_refs, tail_refs, out = refs[:lines], refs[lines : lines + len(members)], refs[-1]
             for line in range(lines):
-                for at in range(len(members)):
+                for at, far in enumerate(members):
                     first = (line * len(members) + at) * capacity
-                    out[first : first + capacity, :head_cols] = head_refs[line][at * capacity : (at + 1) * capacity]
+                    out[first : first + capacity, :head_cols] = head_refs[line][far * capacity : (far + 1) * capacity]
                     out[first : first + capacity, head_cols:] = tail_refs[at][line * capacity : (line + 1) * capacity]
 
         (rows,) = whole_call(
             body,
             [((lines * len(members) * capacity, width), low)],
-            *head_blocks[group],
+            *head_blocks,
             *[tail_blocks[far] for far in members],
             *after,
         )
@@ -647,7 +646,7 @@
         back = pair(group, own_part, [mirrored(other_part, "c", 1)])
         for at, far in reversed(list(enumerate(members))):
             tail_back[far] = mirrored(back[lines + at], "sp", far) if far else back[lines + at]
-        head_back[group] = mirrored_all(back[:lines], "z")
+        head_back[group] = mirrored_all(back[:lines], line_axes)
         before = (other_part,)
     tail_back = [tail_back[far] for far in range(ways)]
 
@@ -658,7 +657,7 @@
             outs[line][...] = blend_rows(routes_refs[line], block).astype(low)
 
     tail_sums = whole_call(blend_body, [((tok_rows, rest_cols), low)] * lines, *tail_back, *line_routes)
-    tail_sums = mirrored_all(tail_sums, "z")
+    tail_sums = mirrored_all(tail_sums, line_axes)
 
     def total_body(*refs):
         at = 0
@@ -726,9 +725,10 @@
         heads = (query_a.shape[1] + query_b.shape[1]) // tp_ways
         capacity = 3 * route_ids.shape[1] * block // (2 * sp_ways)
         fits = heads == sp_ways and capacity % 16 == 0 and block % 16 == 0 and resid.shape[1] % 2048 == 0
+        fits = fits and tp_ways % (2 * cores) == 0
         if fits:
-            devices = mesh.devices.reshape(sp_ways, tp_ways // cores, cores)
-            inner, axes = Mesh(devices, ("sp", "z", "c")), ("z", "c")
+            devices = mesh.devices.reshape(sp_ways, tp_ways // (2 * cores), 2, cores)
+            inner, axes = Mesh(devices, ("sp", "zh", "zl", "c")), ("zh", "zl", "c")
 
             def body(*parts):
                 return exchanged_device(*parts)

time: 219 us -> 211 us (0.963)
  starting transfers between devices: 68.5 us -> 57.1 us
  local copies, waits for them, and re-layouts: 5.39 us -> 11 us
  waiting for transfers between devices: 101 us -> 95.4 us
  other arithmetic: 2.76 us -> 5.65 us
    ppermute x45 -> x44, starting transfers between devices: 64.1 us -> 53.3 us  [mirrored(): lax.ppermute(value, axis, [(i, i ^ apart) for i in range(lax.axis_size(ax...]
    ppermute x45 -> x44, waiting for transfers between devices: 92.5 us -> 88 us  [mirrored(): lax.ppermute(value, axis, [(i, i ^ apart) for i in range(lax.axis_size(ax...]
    unnamed x40 -> x49, local copies, waits for them, and re-layouts: 4.24 us -> 8.08 us
    squeeze x1, other arithmetic: 0.59 us -> 2.8 us  [exchanged_heads(): lax.dynamic_index_in_dim(outgoing, place ^ far, 0, False)]
  transfers between devices with their start and end apart: 46 -> 45, of which waited for: 19 -> 19; matrix products, arithmetic and copies ran while one was open for 1% -> 7% of each run, Pallas kernels for 12% -> 13%
where the time goes in v2:
time: 211 us; the launch traced here: 210 us
  waiting for transfers between devices  95.4 us (45%)
  starting transfers between devices  57.1 us (27%)
  Pallas kernels  40.4 us (19%)
  local copies, waits for them, and re-layouts  11 us (5%)
  other arithmetic  5.65 us (3%)
    ppermute x44, waiting for transfers between devices, mirrored(): lax.ppermute(value, axis, [(i, i ^ apart) for i in range(lax.axis_size(ax...  88 us
    ppermute x44, starting transfers between devices, mirrored(): lax.ppermute(value, axis, [(i, i ^ apart) for i in range(lax.axis_size(ax...  53.3 us
    pallas_call x16, Pallas kernels, whole_call(): pl.pallas_call(body, in_specs=[pl.BlockSpec(memory_space=pltpu.SMEM)] * l...  24.7 us
    pallas_call x1, Pallas kernels, exchanged_heads(): pl.pallas_call(lambda *refs: attend_kernel(*refs, step=seq_rows, width=wi...  15.7 us
    unnamed x49, local copies, waits for them, and re-layouts  8.08 us
    all_to_all x1, waiting for transfers between devices, exchanged_heads(): lax.all_to_all(flat, ('sp', 'zl', 'c'), split_axis=0, concat_axis=0, tile...  7.44 us
  transfers between devices with their start and end apart: 45, of which 19 were waited for; matrix products, arithmetic and copies ran while one was open for 7% of the time, Pallas kernels for 13%

profile of v2, /device:TPU:0, one launch (start us, length us, event | category | flops | bytes accessed | tf_op | source)
XLA Modules:
  0.0 209.9 jit_solution(7853925023772404597)
XLA Ops:
  0.0 3.1 %collective-permute-start.5 = (bf16[256,2048]{1,0:T(8,128)(2,1)}, bf16[256,2048]{1,0:T(8,128)(2,1)S(1)}, u32[]{:S(2)}, u32[]{:S(2)}) collective-permute-start(bf16[256,2048]{1,0:T(8,128)(2,1)} %refs_0_.1), channel_id=1, source_target_pairs={{0,2},{2,0},{1,3},{3,1},{4,6},{6,4},{5,7},{7,5},{8,10},{10,8},{9,1... | collective-permute-start | bytes 3145736 | tf_op jit(solution)/shard_map/ppermute | solution.py:309
  4.2 1.1 copy.26
  5.4 1.9 copy.27
  11.1 1.8 pad_dynamic-update-slice_fusion
  13.8 2.8 %fusion.1 = (bf16[384,512]{1,0:T(8,128)(2,1)}, bf16[384,512]{1,0:T(8,128)(2,1)S(1)}, bf16[384,512]{1,0:T(8,128)(2,1)}, bf16[384,512]{1,0:T(8,128)(2,1)}) fusion(s32[]{:T(128)S(6)} %select_n.37, bf16[2,384,512]{2,1,0:T(8,128)(2,1)} %copy-done.7, bf16[2,384,512]{2,1,0:T(8,128)(2,1)} %get-tuple-element.85, s32[]{:T(128)S(6)} %select_n.31, s32[]{:T(128)S(6)} %select_n.35, ...), kind=kLoop, calls=%fused_computation.9 | loop fusion | flops 786432 | bytes 3145744 | tf_op jit(solution)/shard_map/jit(dynamic_index_in_dim)/squeeze | solution.py:349
  16.6 1.5 collective-permute-start
  18.1 1.5 collective-permute-start.1
  21.7 7.1 %collective-permute-done.refs_4_ = bf16[384,512]{1,0:T(8,128)(2,1)S(1)} collective-permute-done((bf16[384,512]{1,0:T(8,128)(2,1)}, bf16[384,512]{1,0:T(8,128)(2,1)S(1)}, u32[]{:S(2)}, u32[]{:S(2)}) %collective-permute-start) | collective-permute-done | bytes 393248 | tf_op jit(solution)/shard_map/ppermute | solution.py:309
  29.3 7.8 %collective-permute-done.1.refs_5_ = bf16[384,512]{1,0:T(8,128)(2,1)} collective-permute-done((bf16[384,512]{1,0:T(8,128)(2,1)}, bf16[384,512]{1,0:T(8,128)(2,1)}, u32[]{:S(2)}, u32[]{:S(2)}) %collective-permute-start.1) | collective-permute-done | bytes 393248 | tf_op jit(solution)/shard_map/ppermute | solution.py:309
  37.1 15.7 %attend.1 = bf16[4,2,2,128,128]{4,3,2,1,0:T(8,128)(2,1)} custom-call(f32[3]{0:T(128)S(1)} %pad_maximum_fusion.2.refs_0_, s32[1]{0:T(128)} %bitcast.5.refs_1_, f32[1,128]{1,0:T(1,128)S(1)} %fusion.10.refs_2_, bf16[384,512]{1,0:T(8,128)(2,1)S(1)} %get-tuple-element.82.refs_3_, bf16[384,512]{1,0:T(8,128)(2,1)S(1)} %collective-permute-done.refs_4_, ...), custom_call_target="tpu_custom_call" | custom-call | flops 2013265920 | tf_op jit(solution)/shard_map/attend/pallas_call | solution.py:364
  52.8 3.8 %all-to-all-start = ((bf16[16,128,128]{2,1,0:T(8,128)(2,1)}), bf16[16,128,128]{2,1,0:T(8,128)(2,1)S(1)}, u32[]{:S(2)}, u32[]{:S(2)}) async-start(bf16[16,128,128]{2,1,0:T(8,128)(2,1)} %bitcast.52), calls=%async_computation | async-start | bytes 1048576 | tf_op jit(solution)/shard_map/all_to_all | solution.py:380
  59.4 7.4 %all-to-all-done = bf16[16,128,128]{2,1,0:T(8,128)(2,1)S(1)} async-done(((bf16[16,128,128]{2,1,0:T(8,128)(2,1)}), bf16[16,128,128]{2,1,0:T(8,128)(2,1)S(1)}, u32[]{:S(2)}, u32[]{:S(2)}) %all-to-all-start) | async-done | bytes 524320 | tf_op jit(solution)/shard_map/all_to_all | solution.py:380
  66.9 3.5 %shard_map.181 = (bf16[64,2048]{1,0:T(8,128)(2,1)S(1)}, bf16[64,2048]{1,0:T(8,128)(2,1)S(1)}) custom-call(s32[3]{0:T(128)S(1)} %pad_add_fusion.at, bf16[4,2,2,128,128]{4,3,2,1,0:T(8,128)(2,1)S(1)} %bitcast.45, bf16[256,2048]{1,0:T(8,128)(2,1)S(1)} %copy-done.3, bf16[128,2048]{1,0:T(8,128)(2,1)S(1)} %copy-done.4, ...), custom_call_target="tpu_custom_call" | custom-call | flops 805306368 | tf_op jit(solution)/shard_map/pallas_call | solution.py:319
  70.4 2.7 %collective-permute-start.9 = (bf16[64,2048]{1,0:T(8,128)(2,1)S(1)}, bf16[64,2048]{1,0:T(8,128)(2,1)S(1)}, u32[]{:S(2)}, u32[]{:S(2)}) collective-permute-start(bf16[64,2048]{1,0:T(8,128)(2,1)S(1)} %get-tuple-element.50), channel_id=1, source_target_pairs={{0,4},{4,0},{1,5},{5,1},{2,6},{6,2},{3,7},{7,3},{8,12},{12,8},{9,1... | collective-permute-start | bytes 786440 | tf_op jit(solution)/shard_map/ppermute | solution.py:309
  73.1 11.0 %collective-permute-done.9.refs_1_ = bf16[64,2048]{1,0:T(8,128)(2,1)S(1)} collective-permute-done((bf16[64,2048]{1,0:T(8,128)(2,1)S(1)}, bf16[64,2048]{1,0:T(8,128)(2,1)S(1)}, u32[]{:S(2)}, u32[]{:S(2)}) %collective-permute-start.9) | collective-permute-done | bytes 262176 | tf_op jit(solution)/shard_map/ppermute | solution.py:309
  84.6 3.1 %collective-permute-start.17 = (bf16[64,1536]{1,0:T(8,128)(2,1)S(1)}, bf16[64,1536]{1,0:T(8,128)(2,1)S(1)}, u32[]{:S(2)}, u32[]{:S(2)}) collective-permute-start(bf16[64,1536]{1,0:T(8,128)(2,1)S(1)} %get-tuple-element.56.refs_0_), channel_id=1, source_target_pairs={{0,4},{2,6},{4,0},{6,2},{1,5},{3,7},{5,1},{7,3},{8,12},{10,14},{12... | collective-permute-start | bytes 589832 | tf_op jit(solution)/shard_map/ppermute | solution.py:309
  87.8 1.2 collective-permute-start.18
  89.7 3.4 %collective-permute-done.10 = bf16[48,512]{1,0:T(8,128)(2,1)S(1)} collective-permute-done((bf16[48,512]{1,0:T(8,128)(2,1)S(1)}, bf16[48,512]{1,0:T(8,128)(2,1)S(1)}, u32[]{:S(2)}, u32[]{:S(2)}) %collective-permute-start.10) | collective-permute-done | bytes 49184 | tf_op jit(solution)/shard_map/ppermute | solution.py:309
  93.9 3.3 %collective-permute-done.11 = bf16[48,512]{1,0:T(8,128)(2,1)S(1)} collective-permute-done((bf16[48,512]{1,0:T(8,128)(2,1)S(1)}, bf16[48,512]{1,0:T(8,128)(2,1)S(1)}, u32[]{:S(2)}, u32[]{:S(2)}) %collective-permute-start.11) | collective-permute-done | bytes 49184 | tf_op jit(solution)/shard_map/ppermute | solution.py:309
  97.2 1.4 collective-permute-start.12
  99.2 3.0 %collective-permute-done.12 = bf16[48,512]{1,0:T(8,128)(2,1)S(1)} collective-permute-done((bf16[48,512]{1,0:T(8,128)(2,1)S(1)}, bf16[48,512]{1,0:T(8,128)(2,1)S(1)}, u32[]{:S(2)}, u32[]{:S(2)}) %collective-permute-start.12) | collective-permute-done | bytes 49184 | tf_op jit(solution)/shard_map/ppermute | solution.py:309
  102.2 2.6 %collective-permute-start.21 = (f32[4,64]{1,0:T(4,128)S(1)}, f32[4,64]{1,0:T(4,128)S(1)}, u32[]{:S(2)}, u32[]{:S(2)}) collective-permute-start(f32[4,64]{1,0:T(4,128)S(1)} %pad_maximum_fusion.refs_4_.routes_ref), channel_id=1, source_target_pairs={{0,6},{2,4},{4,2},{6,0},{1,7},{3,5},{5,3},{7,1},{8,14},{10,12},{12... | collective-permute-start | bytes 3080 | tf_op jit(solution)/shard_map/ppermute | solution.py:309
  105.2 2.3 %collective-permute-done.21.refs_7_ = f32[4,64]{1,0:T(4,128)S(1)} collective-permute-done((f32[4,64]{1,0:T(4,128)S(1)}, f32[4,64]{1,0:T(4,128)S(1)}, u32[]{:S(2)}, u32[]{:S(2)}) %collective-permute-start.21) | collective-permute-done | bytes 1056 | tf_op jit(solution)/shard_map/ppermute | solution.py:309
  109.1 1.2 collective-permute-start.23
  110.3 3.5 %collective-permute-start.14 = (bf16[192,512]{1,0:T(8,128)(2,1)S(1)}, bf16[192,512]{1,0:T(8,128)(2,1)S(1)}, u32[]{:S(2)}, u32[]{:S(2)}) collective-permute-start(bf16[192,512]{1,0:T(8,128)(2,1)S(1)} %constant_dynamic-update-slice_fusion.1.refs_8_.refs_0_), channel_id=1, source_target_pairs={{0,4},{2,6},{4,0},{6,2},{1,5},{3,7},{5,1},{7,3},{8,12},{10,14},{12... | collective-permute-start | bytes 589832 | tf_op jit(solution)/shard_map/ppermute | solution.py:309
  114.7 4.5 %collective-permute-done.13.refs_1_ = bf16[192,512]{1,0:T(8,128)(2,1)S(1)} collective-permute-done((bf16[192,512]{1,0:T(8,128)(2,1)S(1)}, bf16[192,512]{1,0:T(8,128)(2,1)S(1)}, u32[]{:S(2)}, u32[]{:S(2)}) %collective-permute-start.13) | collective-permute-done | bytes 196640 | tf_op jit(solution)/shard_map/ppermute | solution.py:309
  119.2 5.7 %collective-permute-done.14.refs_2_ = bf16[192,512]{1,0:T(8,128)(2,1)S(1)} collective-permute-done((bf16[192,512]{1,0:T(8,128)(2,1)S(1)}, bf16[192,512]{1,0:T(8,128)(2,1)S(1)}, u32[]{:S(2)}, u32[]{:S(2)}) %collective-permute-start.14) | collective-permute-done | bytes 196640 | tf_op jit(solution)/shard_map/ppermute | solution.py:309
  125.1 4.4 %shard_map.185.rows_ref.refs_3_ = bf16[576,768]{1,0:T(8,128)(2,1)S(1)} custom-call(bf16[576,2048]{1,0:T(8,128)(2,1)S(1)} %shard_map.184.rows_ref, bf16[2048,768]{1,0:T(8,128)(2,1)S(1)} %bitcast.32, bf16[2048,768]{1,0:T(8,128)(2,1)S(1)} %bitcast.37), custom_call_target="tpu_custom_call" | custom-call | flops 3623878656 | tf_op jit(solution)/shard_map/pallas_call | solution.py:319
  129.7 6.3 %shard_map.187.refs_5_ = bf16[576,2048]{1,0:T(8,128)(2,1)S(1)} custom-call(bf16[576,2048]{1,0:T(8,128)(2,1)S(1)} %collective-permute-done.24.rows_ref, bf16[2048,768]{1,0:T(8,128)(2,1)S(1)} %bitcast.33, bf16[2048,768]{1,0:T(8,128)(2,1)S(1)} %bitcast.38, bf16[768,2048]{1,0:T(8,128)(2,1)S(1)} %bitcast.41, bf16[576,768]{1,0:T(8,128)(2,1)S(1)} %shard_map.185.rows_ref.refs_3_), custom_call_target="tpu_custom_call" | custom-call | flops 5435817984 | tf_op jit(solution)/shard_map/pallas_call | solution.py:319
  136.4 1.6 collective-permute-start.29
  138.0 14.6 %collective-permute-done.29.refs_4_ = bf16[192,1536]{1,0:T(8,128)(2,1)S(1)} collective-permute-done((bf16[192,1536]{1,0:T(8,128)(2,1)S(1)}, bf16[192,1536]{1,0:T(8,128)(2,1)S(1)}, u32[]{:S(2)}, u32[]{:S(2)}) %collective-permute-start.29) | collective-permute-done | bytes 589856 | tf_op jit(solution)/shard_map/ppermute | solution.py:309
  152.8 2.6 %shard_map.186.refs_0_ = bf16[576,2048]{1,0:T(8,128)(2,1)S(1)} custom-call(bf16[576,768]{1,0:T(8,128)(2,1)S(1)} %shard_map.185.rows_ref.refs_3_, bf16[768,2048]{1,0:T(8,128)(2,1)S(1)} %bitcast.42), custom_call_target="tpu_custom_call" | custom-call | flops 1811939328 | tf_op jit(solution)/shard_map/pallas_call | solution.py:319
  155.4 1.5 shard_map.190.rows_ref.refs_3_
  157.4 2.1 shard_map.192
  160.1 1.7 collective-permute-start.38
  163.4 1.4 collective-permute-start.40
  164.7 2.7 %collective-permute-start.26 = (bf16[144,640]{1,0:T(8,128)(2,1)S(1)}, bf16[144,640]{1,0:T(8,128)(2,1)S(1)}, u32[]{:S(2)}, u32[]{:S(2)}) collective-permute-start(bf16[144,640]{1,0:T(8,128)(2,1)S(1)} %get-tuple-element.61), channel_id=1, source_target_pairs={{0,2},{2,0},{4,6},{6,4},{1,3},{3,1},{5,7},{7,5},{8,10},{10,8},{12,... | collective-permute-start | bytes 552968 | tf_op jit(solution)/shard_map/ppermute | solution.py:309
  168.4 6.3 %collective-permute-done.26.refs_1_ = bf16[144,640]{1,0:T(8,128)(2,1)S(1)} collective-permute-done((bf16[144,640]{1,0:T(8,128)(2,1)S(1)}, bf16[144,640]{1,0:T(8,128)(2,1)S(1)}, u32[]{:S(2)}, u32[]{:S(2)}) %collective-permute-start.26) | collective-permute-done | bytes 184352 | tf_op jit(solution)/shard_map/ppermute | solution.py:309
  174.7 1.9 collective-permute-start.28
  176.6 1.4 collective-permute-start.32
  177.9 10.3 %collective-permute-done.39.refs_2_ = bf16[192,1408]{1,0:T(8,128)(2,1)S(1)} collective-permute-done((bf16[192,1408]{1,0:T(8,128)(2,1)S(1)}, bf16[192,1408]{1,0:T(8,128)(2,1)S(1)}, u32[]{:S(2)}, u32[]{:S(2)}) %collective-permute-start.39) | collective-permute-done | bytes 540704 | tf_op jit(solution)/shard_map/ppermute | solution.py:309
  188.2 3.6 %collective-permute-start.33 = (bf16[48,640]{1,0:T(8,128)(2,1)S(1)}, bf16[48,640]{1,0:T(8,128)(2,1)S(1)}, u32[]{:S(2)}, u32[]{:S(2)}) collective-permute-start(bf16[48,640]{1,0:T(8,128)(2,1)S(1)} %get-tuple-element.67), channel_id=1, source_target_pairs={{0,4},{2,6},{4,0},{6,2},{1,5},{3,7},{5,1},{7,3},{8,12},{10,14},{12... | collective-permute-start | bytes 184328 | tf_op jit(solution)/shard_map/ppermute | solution.py:309
  191.8 1.4 collective-permute-start.34
  194.4 3.0 %collective-permute-start.42 = (bf16[64,1408]{1,0:T(8,128)(2,1)S(1)}, bf16[64,1408]{1,0:T(8,128)(2,1)S(1)}, u32[]{:S(2)}, u32[]{:S(2)}) collective-permute-start(bf16[64,1408]{1,0:T(8,128)(2,1)S(1)} %get-tuple-element.79), channel_id=1, source_target_pairs={{0,4},{2,6},{4,0},{6,2},{1,5},{3,7},{5,1},{7,3},{8,12},{10,14},{12... | collective-permute-start | bytes 540680 | tf_op jit(solution)/shard_map/ppermute | solution.py:309
  197.4 1.4 collective-permute-start.43
  199.4 1.7 collective-permute-start.36
  201.0 2.7 %collective-permute-done.35.refs_1_ = bf16[48,640]{1,0:T(8,128)(2,1)S(1)} collective-permute-done((bf16[48,640]{1,0:T(8,128)(2,1)S(1)}, bf16[48,640]{1,0:T(8,128)(2,1)S(1)}, u32[]{:S(2)}, u32[]{:S(2)}) %collective-permute-start.35) | collective-permute-done | bytes 61472 | tf_op jit(solution)/shard_map/ppermute | solution.py:309
  204.7 4.2 %collective-permute-done.37.refs_3_ = bf16[48,640]{1,0:T(8,128)(2,1)S(1)} collective-permute-done((bf16[48,640]{1,0:T(8,128)(2,1)S(1)}, bf16[48,640]{1,0:T(8,128)(2,1)S(1)}, u32[]{:S(2)}, u32[]{:S(2)}) %collective-permute-start.37) | collective-permute-done | bytes 61472 | tf_op jit(solution)/shard_map/ppermute | solution.py:309
  (130 shorter events, 25.3 us)
Async XLA Ops:
  0.0 28.8 %collective-permute-start.5 = (bf16[256,2048]{1,0:T(8,128)(2,1)}, bf16[256,2048]{1,0:T(8,128)(2,1)S(1)}, u32[]{:S(2)}, u32[]{:S(2)}) collective-permute-start(bf16[256,2048]{1,0:T(8,128)(2,1)} %refs_0_.1), channel_id=1, source_target_pairs={{0,2},{2,0},{1,3},{3,1},{4,6},{6,4},{5,7},{7,5},{8,10},{10,8},{9,1... | collective-permute-start | bytes 3145736 | tf_op jit(solution)/shard_map/ppermute | solution.py:309
  16.6 12.2 %collective-permute-start = (bf16[384,512]{1,0:T(8,128)(2,1)}, bf16[384,512]{1,0:T(8,128)(2,1)S(1)}, u32[]{:S(2)}, u32[]{:S(2)}) collective-permute-start(bf16[384,512]{1,0:T(8,128)(2,1)} %get-tuple-element.83), channel_id=1, source_target_pairs={{0,8},{8,0},{16,24},{24,16},{1,9},{9,1},{17,25},{25,17},{2,10},{10... | collective-permute-start | bytes 1179656 | tf_op jit(solution)/shard_map/ppermute | solution.py:309
  18.1 19.0 %collective-permute-start.1 = (bf16[384,512]{1,0:T(8,128)(2,1)}, bf16[384,512]{1,0:T(8,128)(2,1)}, u32[]{:S(2)}, u32[]{:S(2)}) collective-permute-start(bf16[384,512]{1,0:T(8,128)(2,1)} %get-tuple-element.84), channel_id=1, source_target_pairs={{0,16},{8,24},{16,0},{24,8},{1,17},{9,25},{17,1},{25,9},{2,18},{10... | collective-permute-start | bytes 1179656 | tf_op jit(solution)/shard_map/ppermute | solution.py:309
  19.6 17.5 %collective-permute-start.2 = (bf16[384,512]{1,0:T(8,128)(2,1)}, bf16[384,512]{1,0:T(8,128)(2,1)}, u32[]{:S(2)}, u32[]{:S(2)}) collective-permute-start(bf16[384,512]{1,0:T(8,128)(2,1)} %get-tuple-element.81), channel_id=1, source_target_pairs={{0,24},{8,16},{16,8},{24,0},{1,25},{9,17},{17,9},{25,1},{2,26},{10... | collective-permute-start | bytes 1179656 | tf_op jit(solution)/shard_map/ppermute | solution.py:309
  20.1 36.7 %collective-permute-start.6 = (bf16[128,2048]{1,0:T(8,128)(2,1)S(1)}, bf16[128,2048]{1,0:T(8,128)(2,1)}, u32[]{:S(2)}, u32[]{:S(2)}) collective-permute-start(bf16[128,2048]{1,0:T(8,128)(2,1)S(1)} %copy-done.4), channel_id=1, source_target_pairs={{0,2},{2,0},{1,3},{3,1},{4,6},{6,4},{5,7},{7,5},{8,10},{10,8},{9,1... | collective-permute-start | bytes 1572872 | tf_op jit(solution)/shard_map/ppermute | solution.py:309
  28.8 30.6 %collective-permute-start.3 = (bf16[256,2048]{1,0:T(8,128)(2,1)S(1)}, bf16[256,2048]{1,0:T(8,128)(2,1)}, u32[]{:S(2)}, u32[]{:S(2)}) collective-permute-start(bf16[256,2048]{1,0:T(8,128)(2,1)S(1)} %copy-done.3), channel_id=1, source_target_pairs={{0,1},{1,0},{2,3},{3,2},{4,5},{5,4},{6,7},{7,6},{8,9},{9,8},{10,11... | collective-permute-start | bytes 3145736 | tf_op jit(solution)/shard_map/ppermute | solution.py:309
  28.8 38.1 %collective-permute-start.7 = (bf16[256,2048]{1,0:T(8,128)(2,1)S(1)}, bf16[256,2048]{1,0:T(8,128)(2,1)}, u32[]{:S(2)}, u32[]{:S(2)}) collective-permute-start(bf16[256,2048]{1,0:T(8,128)(2,1)S(1)} %collective-permute-done.5.refs_4_), channel_id=1, source_target_pairs={{0,1},{1,0},{2,3},{3,2},{4,5},{5,4},{6,7},{7,6},{8,9},{9,8},{10,11... | collective-permute-start | bytes 3145736 | tf_op jit(solution)/shard_map/ppermute | solution.py:309
  37.1 20.0 %copy-start.11 = (s32[64,2]{0,1:T(2,128)S(1)}, s32[64,2]{0,1:T(2,128)}, u32[]{:S(2)}) copy-start(s32[64,2]{0,1:T(2,128)} %param.33) | copy-start | bytes 1540
  52.8 14.1 %all-to-all-start = ((bf16[16,128,128]{2,1,0:T(8,128)(2,1)}), bf16[16,128,128]{2,1,0:T(8,128)(2,1)S(1)}, u32[]{:S(2)}, u32[]{:S(2)}) async-start(bf16[16,128,128]{2,1,0:T(8,128)(2,1)} %bitcast.52), calls=%async_computation | async-start | bytes 1048576 | tf_op jit(solution)/shard_map/all_to_all | solution.py:380
  56.6 2.1 %collective-permute-start.4 = (bf16[128,2048]{1,0:T(8,128)(2,1)S(1)}, bf16[128,2048]{1,0:T(8,128)(2,1)}, u32[]{:S(2)}, u32[]{:S(2)}) collective-permute-start(bf16[128,2048]{1,0:T(8,128)(2,1)S(1)} %copy-done.4), channel_id=1, source_target_pairs={{0,1},{1,0},{2,3},{3,2},{4,5},{5,4},{6,7},{7,6},{8,9},{9,8},{10,11... | collective-permute-start | bytes 1572872 | tf_op jit(solution)/shard_map/ppermute | solution.py:309
  56.7 2.7 %collective-permute-start.8 = (bf16[128,2048]{1,0:T(8,128)(2,1)}, bf16[128,2048]{1,0:T(8,128)(2,1)}, u32[]{:S(2)}, u32[]{:S(2)}) collective-permute-start(bf16[128,2048]{1,0:T(8,128)(2,1)} %collective-permute-done.6.refs_5_), channel_id=1, source_target_pairs={{0,1},{1,0},{2,3},{3,2},{4,5},{5,4},{6,7},{7,6},{8,9},{9,8},{10,11... | collective-permute-start | bytes 1572872 | tf_op jit(solution)/shard_map/ppermute | solution.py:309
  66.9 40.7 %copy-start = (bf16[1,2048,768]{2,1,0:T(8,128)(2,1)S(1)}, bf16[1,2048,768]{2,1,0:T(8,128)(2,1)}, u32[]{:S(2)}) copy-start(bf16[1,2048,768]{2,1,0:T(8,128)(2,1)} %param.35) | copy-start | bytes 9437188
  66.9 40.7 %copy-start.1 = (bf16[1,2048,768]{2,1,0:T(8,128)(2,1)S(1)}, bf16[1,2048,768]{2,1,0:T(8,128)(2,1)}, u32[]{:S(2)}) copy-start(bf16[1,2048,768]{2,1,0:T(8,128)(2,1)} %param.36) | copy-start | bytes 9437188
  70.4 13.8 %collective-permute-start.9 = (bf16[64,2048]{1,0:T(8,128)(2,1)S(1)}, bf16[64,2048]{1,0:T(8,128)(2,1)S(1)}, u32[]{:S(2)}, u32[]{:S(2)}) collective-permute-start(bf16[64,2048]{1,0:T(8,128)(2,1)S(1)} %get-tuple-element.50), channel_id=1, source_target_pairs={{0,4},{4,0},{1,5},{5,1},{2,6},{6,2},{3,7},{7,3},{8,12},{12,8},{9,1... | collective-permute-start | bytes 786440 | tf_op jit(solution)/shard_map/ppermute | solution.py:309
  73.0 25.5 %collective-permute-start.19 = (f32[4,64]{1,0:T(4,128)S(1)}, f32[4,64]{1,0:T(4,128)S(1)}, u32[]{:S(2)}, u32[]{:S(2)}) collective-permute-start(f32[4,64]{1,0:T(4,128)S(1)} %pad_maximum_fusion.refs_4_.routes_ref), channel_id=1, source_target_pairs={{0,2},{2,0},{4,6},{6,4},{1,3},{3,1},{5,7},{7,5},{8,10},{10,8},{12,... | collective-permute-start | bytes 3080 | tf_op jit(solution)/shard_map/ppermute | solution.py:309
  84.6 23.0 %collective-permute-start.16 = (bf16[64,1536]{1,0:T(8,128)(2,1)S(1)}, bf16[64,1536]{1,0:T(8,128)(2,1)S(1)}, u32[]{:S(2)}, u32[]{:S(2)}) collective-permute-start(bf16[64,1536]{1,0:T(8,128)(2,1)S(1)} %get-tuple-element.56.refs_0_), channel_id=1, source_target_pairs={{0,2},{2,0},{4,6},{6,4},{1,3},{3,1},{5,7},{7,5},{8,10},{10,8},{12,... | collective-permute-start | bytes 589832 | tf_op jit(solution)/shard_map/ppermute | solution.py:309
  84.6 22.9 %collective-permute-start.17 = (bf16[64,1536]{1,0:T(8,128)(2,1)S(1)}, bf16[64,1536]{1,0:T(8,128)(2,1)S(1)}, u32[]{:S(2)}, u32[]{:S(2)}) collective-permute-start(bf16[64,1536]{1,0:T(8,128)(2,1)S(1)} %get-tuple-element.56.refs_0_), channel_id=1, source_target_pairs={{0,4},{2,6},{4,0},{6,2},{1,5},{3,7},{5,1},{7,3},{8,12},{10,14},{12... | collective-permute-start | bytes 589832 | tf_op jit(solution)/shard_map/ppermute | solution.py:309
  87.8 19.8 %collective-permute-start.18 = (bf16[64,1536]{1,0:T(8,128)(2,1)S(1)}, bf16[64,1536]{1,0:T(8,128)(2,1)S(1)}, u32[]{:S(2)}, u32[]{:S(2)}) collective-permute-start(bf16[64,1536]{1,0:T(8,128)(2,1)S(1)} %get-tuple-element.56.refs_0_), channel_id=1, source_target_pairs={{0,6},{2,4},{4,2},{6,0},{1,7},{3,5},{5,3},{7,1},{8,14},{10,12},{12... | collective-permute-start | bytes 589832 | tf_op jit(solution)/shard_map/ppermute | solution.py:309
  89.0 4.1 %collective-permute-start.10 = (bf16[48,512]{1,0:T(8,128)(2,1)S(1)}, bf16[48,512]{1,0:T(8,128)(2,1)S(1)}, u32[]{:S(2)}, u32[]{:S(2)}) collective-permute-start(bf16[48,512]{1,0:T(8,128)(2,1)S(1)} %get-tuple-element.53), channel_id=1, source_target_pairs={{0,8},{8,0},{16,24},{24,16},{1,9},{9,1},{17,25},{25,17},{2,10},{10... | collective-permute-start | bytes 147464 | tf_op jit(solution)/shard_map/ppermute | solution.py:309
  93.1 4.1 %collective-permute-start.11 = (bf16[48,512]{1,0:T(8,128)(2,1)S(1)}, bf16[48,512]{1,0:T(8,128)(2,1)S(1)}, u32[]{:S(2)}, u32[]{:S(2)}) collective-permute-start(bf16[48,512]{1,0:T(8,128)(2,1)S(1)} %get-tuple-element.54), channel_id=1, source_target_pairs={{0,16},{8,24},{16,0},{24,8},{1,17},{9,25},{17,1},{25,9},{2,18},{10... | collective-permute-start | bytes 147464 | tf_op jit(solution)/shard_map/ppermute | solution.py:309
  97.2 5.0 %collective-permute-start.12 = (bf16[48,512]{1,0:T(8,128)(2,1)S(1)}, bf16[48,512]{1,0:T(8,128)(2,1)S(1)}, u32[]{:S(2)}, u32[]{:S(2)}) collective-permute-start(bf16[48,512]{1,0:T(8,128)(2,1)S(1)} %get-tuple-element.55), channel_id=1, source_target_pairs={{0,24},{8,16},{16,8},{24,0},{1,25},{9,17},{17,9},{25,1},{2,26},{10... | collective-permute-start | bytes 147464 | tf_op jit(solution)/shard_map/ppermute | solution.py:309
  98.6 6.7 %collective-permute-start.20 = (f32[4,64]{1,0:T(4,128)S(1)}, f32[4,64]{1,0:T(4,128)S(1)}, u32[]{:S(2)}, u32[]{:S(2)}) collective-permute-start(f32[4,64]{1,0:T(4,128)S(1)} %pad_maximum_fusion.refs_4_.routes_ref), channel_id=1, source_target_pairs={{0,4},{2,6},{4,0},{6,2},{1,5},{3,7},{5,1},{7,3},{8,12},{10,14},{12... | collective-permute-start | bytes 3080 | tf_op jit(solution)/shard_map/ppermute | solution.py:309
  102.2 5.4 %collective-permute-start.21 = (f32[4,64]{1,0:T(4,128)S(1)}, f32[4,64]{1,0:T(4,128)S(1)}, u32[]{:S(2)}, u32[]{:S(2)}) collective-permute-start(f32[4,64]{1,0:T(4,128)S(1)} %pad_maximum_fusion.refs_4_.routes_ref), channel_id=1, source_target_pairs={{0,6},{2,4},{4,2},{6,0},{1,7},{3,5},{5,3},{7,1},{8,14},{10,12},{12... | collective-permute-start | bytes 3080 | tf_op jit(solution)/shard_map/ppermute | solution.py:309
  108.4 16.5 %collective-permute-start.22 = (bf16[192,1536]{1,0:T(8,128)(2,1)S(1)}, bf16[192,1536]{1,0:T(8,128)(2,1)S(1)}, u32[]{:S(2)}, u32[]{:S(2)}) collective-permute-start(bf16[192,1536]{1,0:T(8,128)(2,1)S(1)} %get-tuple-element.58), channel_id=1, source_target_pairs={{0,8},{8,0},{16,24},{24,16},{1,9},{9,1},{17,25},{25,17},{2,10},{10... | collective-permute-start | bytes 1769480 | tf_op jit(solution)/shard_map/ppermute | solution.py:309
  109.1 15.7 %collective-permute-start.23 = (bf16[192,1536]{1,0:T(8,128)(2,1)S(1)}, bf16[192,1536]{1,0:T(8,128)(2,1)S(1)}, u32[]{:S(2)}, u32[]{:S(2)}) collective-permute-start(bf16[192,1536]{1,0:T(8,128)(2,1)S(1)} %get-tuple-element.59), channel_id=1, source_target_pairs={{0,16},{8,24},{16,0},{24,8},{1,17},{9,25},{17,1},{25,9},{2,18},{10... | collective-permute-start | bytes 1769480 | tf_op jit(solution)/shard_map/ppermute | solution.py:309
  110.3 8.8 %collective-permute-start.13 = (bf16[192,512]{1,0:T(8,128)(2,1)S(1)}, bf16[192,512]{1,0:T(8,128)(2,1)S(1)}, u32[]{:S(2)}, u32[]{:S(2)}) collective-permute-start(bf16[192,512]{1,0:T(8,128)(2,1)S(1)} %constant_dynamic-update-slice_fusion.1.refs_8_.refs_0_), channel_id=1, source_target_pairs={{0,2},{2,0},{4,6},{6,4},{1,3},{3,1},{5,7},{7,5},{8,10},{10,8},{12,... | collective-permute-start | bytes 589832 | tf_op jit(solution)/shard_map/ppermute | solution.py:309
  110.3 14.5 %collective-permute-start.14 = (bf16[192,512]{1,0:T(8,128)(2,1)S(1)}, bf16[192,512]{1,0:T(8,128)(2,1)S(1)}, u32[]{:S(2)}, u32[]{:S(2)}) collective-permute-start(bf16[192,512]{1,0:T(8,128)(2,1)S(1)} %constant_dynamic-update-slice_fusion.1.refs_8_.refs_0_), channel_id=1, source_target_pairs={{0,4},{2,6},{4,0},{6,2},{1,5},{3,7},{5,1},{7,3},{8,12},{10,14},{12... | collective-permute-start | bytes 589832 | tf_op jit(solution)/shard_map/ppermute | solution.py:309
  113.8 11.1 %collective-permute-start.15 = (bf16[192,512]{1,0:T(8,128)(2,1)S(1)}, bf16[192,512]{1,0:T(8,128)(2,1)S(1)}, u32[]{:S(2)}, u32[]{:S(2)}) collective-permute-start(bf16[192,512]{1,0:T(8,128)(2,1)S(1)} %constant_dynamic-update-slice_fusion.1.refs_8_.refs_0_), channel_id=1, source_target_pairs={{0,6},{2,4},{4,2},{6,0},{1,7},{3,5},{5,3},{7,1},{8,14},{10,12},{12... | collective-permute-start | bytes 589832 | tf_op jit(solution)/shard_map/ppermute | solution.py:309
  125.1 4.6 %collective-permute-start.24 = (bf16[576,2048]{1,0:T(8,128)(2,1)S(1)}, bf16[576,2048]{1,0:T(8,128)(2,1)S(1)}, u32[]{:S(2)}, u32[]{:S(2)}) collective-permute-start(bf16[576,2048]{1,0:T(8,128)(2,1)S(1)} %shard_map.184.rows_ref), channel_id=1, source_target_pairs={{0,1},{1,0},{2,3},{3,2},{4,5},{5,4},{6,7},{7,6},{8,9},{9,8},{10,11... | collective-permute-start | bytes 7077896 | tf_op jit(solution)/shard_map/ppermute | solution.py:309
  135.9 20.9 %collective-permute-start.25 = (bf16[576,2048]{1,0:T(8,128)(2,1)S(1)}, bf16[576,2048]{1,0:T(8,128)(2,1)S(1)}, u32[]{:S(2)}, u32[]{:S(2)}) collective-permute-start(bf16[576,2048]{1,0:T(8,128)(2,1)S(1)} %shard_map.187.refs_5_), channel_id=1, source_target_pairs={{0,1},{1,0},{2,3},{3,2},{4,5},{5,4},{6,7},{7,6},{8,9},{9,8},{10,11... | collective-permute-start | bytes 7077896 | tf_op jit(solution)/shard_map/ppermute | solution.py:309
  136.4 16.2 %collective-permute-start.29 = (bf16[192,1536]{1,0:T(8,128)(2,1)S(1)}, bf16[192,1536]{1,0:T(8,128)(2,1)S(1)}, u32[]{:S(2)}, u32[]{:S(2)}) collective-permute-start(bf16[192,1536]{1,0:T(8,128)(2,1)S(1)} %get-tuple-element.64), channel_id=1, source_target_pairs={{0,24},{8,16},{16,8},{24,0},{1,25},{9,17},{17,9},{25,1},{2,26},{10... | collective-permute-start | bytes 1769480 | tf_op jit(solution)/shard_map/ppermute | solution.py:309
  152.7 4.7 %collective-permute-start.30 = (bf16[192,2048]{1,0:T(8,128)(2,1)S(1)}, bf16[192,2048]{1,0:T(8,128)(2,1)S(1)}, u32[]{:S(2)}, u32[]{:S(2)}) collective-permute-start(bf16[192,2048]{1,0:T(8,128)(2,1)S(1)} %shard_map.189.rows_ref), channel_id=1, source_target_pairs={{0,1},{1,0},{2,3},{3,2},{4,5},{5,4},{6,7},{7,6},{8,9},{9,8},{10,11... | collective-permute-start | bytes 2359304 | tf_op jit(solution)/shard_map/ppermute | solution.py:309
  159.5 3.6 %collective-permute-start.31 = (bf16[192,2048]{1,0:T(8,128)(2,1)S(1)}, bf16[192,2048]{1,0:T(8,128)(2,1)S(1)}, u32[]{:S(2)}, u32[]{:S(2)}) collective-permute-start(bf16[192,2048]{1,0:T(8,128)(2,1)S(1)} %shard_map.192), channel_id=1, source_target_pairs={{0,1},{1,0},{2,3},{3,2},{4,5},{5,4},{6,7},{7,6},{8,9},{9,8},{10,11... | collective-permute-start | bytes 2359304 | tf_op jit(solution)/shard_map/ppermute | solution.py:309
  160.1 16.5 %collective-permute-start.38 = (bf16[192,1408]{1,0:T(8,128)(2,1)S(1)}, bf16[192,1408]{1,0:T(8,128)(2,1)S(1)}, u32[]{:S(2)}, u32[]{:S(2)}) collective-permute-start(bf16[192,1408]{1,0:T(8,128)(2,1)S(1)} %get-tuple-element.74), channel_id=1, source_target_pairs={{0,8},{8,0},{16,24},{24,16},{1,9},{9,1},{17,25},{25,17},{2,10},{10... | collective-permute-start | bytes 1622024 | tf_op jit(solution)/shard_map/ppermute | solution.py:309
  162.6 25.6 %collective-permute-start.39 = (bf16[192,1408]{1,0:T(8,128)(2,1)S(1)}, bf16[192,1408]{1,0:T(8,128)(2,1)S(1)}, u32[]{:S(2)}, u32[]{:S(2)}) collective-permute-start(bf16[192,1408]{1,0:T(8,128)(2,1)S(1)} %get-tuple-element.75), channel_id=1, source_target_pairs={{0,16},{8,24},{16,0},{24,8},{1,17},{9,25},{17,1},{25,9},{2,18},{10... | collective-permute-start | bytes 1622024 | tf_op jit(solution)/shard_map/ppermute | solution.py:309
  163.4 28.5 %collective-permute-start.40 = (bf16[192,1408]{1,0:T(8,128)(2,1)S(1)}, bf16[192,1408]{1,0:T(8,128)(2,1)S(1)}, u32[]{:S(2)}, u32[]{:S(2)}) collective-permute-start(bf16[192,1408]{1,0:T(8,128)(2,1)S(1)} %get-tuple-element.76), channel_id=1, source_target_pairs={{0,24},{8,16},{16,8},{24,0},{1,25},{9,17},{17,9},{25,1},{2,26},{10... | collective-permute-start | bytes 1622024 | tf_op jit(solution)/shard_map/ppermute | solution.py:309
  164.7 9.9 %collective-permute-start.26 = (bf16[144,640]{1,0:T(8,128)(2,1)S(1)}, bf16[144,640]{1,0:T(8,128)(2,1)S(1)}, u32[]{:S(2)}, u32[]{:S(2)}) collective-permute-start(bf16[144,640]{1,0:T(8,128)(2,1)S(1)} %get-tuple-element.61), channel_id=1, source_target_pairs={{0,2},{2,0},{4,6},{6,4},{1,3},{3,1},{5,7},{7,5},{8,10},{10,8},{12,... | collective-permute-start | bytes 552968 | tf_op jit(solution)/shard_map/ppermute | solution.py:309
  167.4 26.9 %collective-permute-start.27 = (bf16[144,640]{1,0:T(8,128)(2,1)S(1)}, bf16[144,640]{1,0:T(8,128)(2,1)S(1)}, u32[]{:S(2)}, u32[]{:S(2)}) collective-permute-start(bf16[144,640]{1,0:T(8,128)(2,1)S(1)} %get-tuple-element.62), channel_id=1, source_target_pairs={{0,4},{2,6},{4,0},{6,2},{1,5},{3,7},{5,1},{7,3},{8,12},{10,14},{12... | collective-permute-start | bytes 552968 | tf_op jit(solution)/shard_map/ppermute | solution.py:309
  174.7 19.7 %collective-permute-start.28 = (bf16[144,640]{1,0:T(8,128)(2,1)S(1)}, bf16[144,640]{1,0:T(8,128)(2,1)S(1)}, u32[]{:S(2)}, u32[]{:S(2)}) collective-permute-start(bf16[144,640]{1,0:T(8,128)(2,1)S(1)} %get-tuple-element.63), channel_id=1, source_target_pairs={{0,6},{2,4},{4,2},{6,0},{1,7},{3,5},{5,3},{7,1},{8,14},{10,12},{12... | collective-permute-start | bytes 552968 | tf_op jit(solution)/shard_map/ppermute | solution.py:309
  176.6 20.8 %collective-permute-start.32 = (bf16[48,640]{1,0:T(8,128)(2,1)S(1)}, bf16[48,640]{1,0:T(8,128)(2,1)S(1)}, u32[]{:S(2)}, u32[]{:S(2)}) collective-permute-start(bf16[48,640]{1,0:T(8,128)(2,1)S(1)} %get-tuple-element.66), channel_id=1, source_target_pairs={{0,2},{2,0},{4,6},{6,4},{1,3},{3,1},{5,7},{7,5},{8,10},{10,8},{12,... | collective-permute-start | bytes 184328 | tf_op jit(solution)/shard_map/ppermute | solution.py:309
  188.2 10.6 %collective-permute-start.33 = (bf16[48,640]{1,0:T(8,128)(2,1)S(1)}, bf16[48,640]{1,0:T(8,128)(2,1)S(1)}, u32[]{:S(2)}, u32[]{:S(2)}) collective-permute-start(bf16[48,640]{1,0:T(8,128)(2,1)S(1)} %get-tuple-element.67), channel_id=1, source_target_pairs={{0,4},{2,6},{4,0},{6,2},{1,5},{3,7},{5,1},{7,3},{8,12},{10,14},{12... | collective-permute-start | bytes 184328 | tf_op jit(solution)/shard_map/ppermute | solution.py:309
  191.8 6.9 %collective-permute-start.34 = (bf16[48,640]{1,0:T(8,128)(2,1)S(1)}, bf16[48,640]{1,0:T(8,128)(2,1)S(1)}, u32[]{:S(2)}, u32[]{:S(2)}) collective-permute-start(bf16[48,640]{1,0:T(8,128)(2,1)S(1)} %get-tuple-element.68), channel_id=1, source_target_pairs={{0,6},{2,4},{4,2},{6,0},{1,7},{3,5},{5,3},{7,1},{8,14},{10,12},{12... | collective-permute-start | bytes 184328 | tf_op jit(solution)/shard_map/ppermute | solution.py:309
  194.3 14.6 %collective-permute-start.41 = (bf16[64,1408]{1,0:T(8,128)(2,1)S(1)}, bf16[64,1408]{1,0:T(8,128)(2,1)S(1)}, u32[]{:S(2)}, u32[]{:S(2)}) collective-permute-start(bf16[64,1408]{1,0:T(8,128)(2,1)S(1)} %get-tuple-element.78), channel_id=1, source_target_pairs={{0,2},{2,0},{4,6},{6,4},{1,3},{3,1},{5,7},{7,5},{8,10},{10,8},{12,... | collective-permute-start | bytes 540680 | tf_op jit(solution)/shard_map/ppermute | solution.py:309
  194.4 14.5 %collective-permute-start.42 = (bf16[64,1408]{1,0:T(8,128)(2,1)S(1)}, bf16[64,1408]{1,0:T(8,128)(2,1)S(1)}, u32[]{:S(2)}, u32[]{:S(2)}) collective-permute-start(bf16[64,1408]{1,0:T(8,128)(2,1)S(1)} %get-tuple-element.79), channel_id=1, source_target_pairs={{0,4},{2,6},{4,0},{6,2},{1,5},{3,7},{5,1},{7,3},{8,12},{10,14},{12... | collective-permute-start | bytes 540680 | tf_op jit(solution)/shard_map/ppermute | solution.py:309
  197.4 11.5 %collective-permute-start.43 = (bf16[64,1408]{1,0:T(8,128)(2,1)S(1)}, bf16[64,1408]{1,0:T(8,128)(2,1)S(1)}, u32[]{:S(2)}, u32[]{:S(2)}) collective-permute-start(bf16[64,1408]{1,0:T(8,128)(2,1)S(1)} %get-tuple-element.80), channel_id=1, source_target_pairs={{0,6},{2,4},{4,2},{6,0},{1,7},{3,5},{5,3},{7,1},{8,14},{10,12},{12... | collective-permute-start | bytes 540680 | tf_op jit(solution)/shard_map/ppermute | solution.py:309
  198.9 4.8 %collective-permute-start.35 = (bf16[48,640]{1,0:T(8,128)(2,1)S(1)}, bf16[48,640]{1,0:T(8,128)(2,1)S(1)}, u32[]{:S(2)}, u32[]{:S(2)}) collective-permute-start(bf16[48,640]{1,0:T(8,128)(2,1)S(1)} %get-tuple-element.70), channel_id=1, source_target_pairs={{0,8},{8,0},{16,24},{24,16},{1,9},{9,1},{17,25},{25,17},{2,10},{10... | collective-permute-start | bytes 184328 | tf_op jit(solution)/shard_map/ppermute | solution.py:309
  199.4 5.4 %collective-permute-start.36 = (bf16[48,640]{1,0:T(8,128)(2,1)S(1)}, bf16[48,640]{1,0:T(8,128)(2,1)S(1)}, u32[]{:S(2)}, u32[]{:S(2)}) collective-permute-start(bf16[48,640]{1,0:T(8,128)(2,1)S(1)} %get-tuple-element.71), channel_id=1, source_target_pairs={{0,16},{8,24},{16,0},{24,8},{1,17},{9,25},{17,1},{25,9},{2,18},{10... | collective-permute-start | bytes 184328 | tf_op jit(solution)/shard_map/ppermute | solution.py:309
  203.7 5.1 %collective-permute-start.37 = (bf16[48,640]{1,0:T(8,128)(2,1)S(1)}, bf16[48,640]{1,0:T(8,128)(2,1)S(1)}, u32[]{:S(2)}, u32[]{:S(2)}) collective-permute-start(bf16[48,640]{1,0:T(8,128)(2,1)S(1)} %get-tuple-element.72), channel_id=1, source_target_pairs={{0,24},{8,16},{16,8},{24,0},{1,25},{9,17},{17,9},{25,1},{2,26},{10... | collective-permute-start | bytes 184328 | tf_op jit(solution)/shard_map/ppermute | solution.py:309
  (15 other events, 149.5 us)

commit v3 on v2

--- a/solution.py
+++ b/solution.py
@@ -227,15 +227,31 @@
     return output.astype(jnp.bfloat16)
 
 
-def attend_kernel(scalars, own, gain, *refs, step, width, maps, block):
+def attend_kernel(scalars, own, gain, *refs, step, width, maps, block, part_rows):
     pieces, (out, scores, packed) = refs[:-3], refs[-3:]
+    ways = len(pieces) // 2
     place = pl.program_id(0)
     coef = scalars[0]
 
-    @pl.when(place == 0)
+    def unpack(group):
+        found = pieces[group * ways : (group + 1) * ways]
+        value_rows = found[0].shape[0] - 4 * part_rows[group]
+        for far, piece in enumerate(found):
+            at = own[0] ^ far
+            if part_rows[group] < maps or value_rows < width:
+                packed[at] = jnp.zeros(packed.shape[1:], packed.dtype)
+            for which in range(4):
+                begin = which * part_rows[group]
+                packed[at, which * maps : which * maps + part_rows[group], :] = piece[begin : begin + part_rows[group], :]
+            packed[at, 4 * maps : 4 * maps + value_rows, :] = piece[4 * part_rows[group] :, :]
+
+    @pl.when((place == 0) & (own[1] == 0))
     def _():
-        for far, piece in enumerate(pieces):
-            packed[own[0] ^ far] = piece[...]
+        unpack(0)
+
+    @pl.when((place == 0) & (own[1] == 1))
+    def _():
+        unpack(1)
 
     queries = [jnp.transpose(packed[place, 2 * which * maps : (2 * which + 1) * maps, :]) for which in range(2)]
 
@@ -314,13 +330,13 @@
     return [values[0]] + [found[far] for far in range(1, len(values))]
 
 
-def whole_call(body, outs, *operands, scalars=(), flops=0, scratch=(), limit=8):
+def whole_call(body, outs, *operands, scalars=(), flops=0, scratch=(), limit=8, kept=()):
     vmem = pl.BlockSpec(memory_space=pltpu.VMEM)
     return pl.pallas_call(
         body,
         in_specs=[pl.BlockSpec(memory_space=pltpu.SMEM)] * len(scalars) + [vmem] * len(operands),
         out_specs=[vmem] * len(outs),
-        out_shape=[pltpu.VMEM(shape, dtype) for shape, dtype in outs],
+        out_shape=[(pltpu.HBM if at in kept else pltpu.VMEM)(*out) for at, out in enumerate(outs)],
         scratch_shapes=scratch,
         compiler_params=fast_memory(limit),
         cost_estimate=pl.CostEstimate(flops=flops, bytes_accessed=0, transcendentals=0),
@@ -336,46 +352,87 @@
     width = -(-max(group[2].shape[2] for group in groups) // 128) * 128
     maps = -(-max(group[0].shape[2] // 2 for group in groups) // 16) * 16
 
-    def filled(array, size):
-        return jnp.pad(array, ((0, 0), (0, size - array.shape[1]), (0, 0)))
-
     turned = lax.optimization_barrier([[jnp.transpose(array, (1, 2, 0)) for array in group] for group in groups])
-    outgoing = []
-    for query, key, value in turned:
-        half = query.shape[1] // 2
-        split = [array[:, first : first + half] for first in (0, half) for array in (query, key)]
-        outgoing.append(jnp.concatenate([filled(array, maps) for array in split] + [filled(value, width)], axis=1))
-    outgoing = jnp.concatenate(outgoing, axis=0)
-    pieces = [lax.dynamic_index_in_dim(outgoing, place ^ far, 0, False) for far in range(ways)]
-    pieces = mirrored_all(pieces, "sp")
-    first = place < heads_a
+    core = lax.axis_index("c")
+    part_rows = [query.shape[1] // 2 for query, _, _ in turned]
+    piece_rows = [4 * part + group[2].shape[1] for part, group in zip(part_rows, turned)]
+
+    def kind_of(index, core):
+        return (index + heads_a * core) % ways
+
+    def pack_body(at, *refs):
+        arrays, outs = (refs[:3], refs[3:6]), (refs[6 : 6 + ways], refs[6 + ways :])
+        for far in range(ways):
+            kind = kind_of(at[0] ^ far, at[1])
+
+            def fill(group, head):
+                query, key, value = arrays[group]
+                out, part = outs[group][far], part_rows[group]
+                for which in range(2):
+                    for second, array in enumerate((query, key)):
+                        begin = (2 * which + second) * part
+                        out[begin : begin + part, :] = array[head, which * part : (which + 1) * part, :]
+                out[4 * part :, :] = value[head]
+
+            @pl.when(kind < heads_a)
+            def _():
+                fill(0, kind)
+
+            @pl.when(kind >= heads_a)
+            def _():
+                fill(1, kind - heads_a)
+
+    packed = whole_call(
+        pack_body,
+        [((rows, seq_rows), jnp.bfloat16) for rows in piece_rows for _ in range(ways)],
+        *turned[0],
+        *turned[1],
+        scalars=(jnp.stack([place, core]).astype(jnp.int32),),
+        kept=(0, ways),
+    )
+    pieces = []
+    for group in range(2):
+        pieces.append(packed[group * ways])
+        for far in range(1, ways):
+            ends = [(index, core) for index in range(ways) for core in range(cores)]
+            ends = [(index, core) for index, core in ends if (kind_of(index, core) >= heads_a) == (group == 1)]
+            route = [((index ^ far) * cores + core, index * cores + core) for index, core in ends]
+            pieces.append(lax.ppermute(packed[group * ways + far], ("sp", "c"), route))
+    kind = kind_of(place, core)
+    first = kind < heads_a
     gain = jnp.where(first, widen(head_gain_a, width), widen(head_gain_b, width)) * HEAD_SCALE
     coef_a, coef_b = [math.log2(math.e) / math.sqrt(group[0].shape[2] // 2) for group in groups]
     scalars = jnp.stack(
         [
             jnp.where(first, coef_a, coef_b).astype(jnp.float32),
-            lax.dynamic_index_in_dim(jnp.concatenate([mix_a, mix_b]), place, 0, False),
+            lax.dynamic_index_in_dim(jnp.concatenate([mix_a, mix_b]), kind, 0, False),
             jnp.where(first, 1.0 / value_a.shape[2], 1.0 / value_b.shape[2]).astype(jnp.float32),
         ]
     )
     pairs = (ways * seq_rows) * (ways + 1) * seq_rows
     shape = (ways, pair_lines, cores, seq_rows // (pair_lines * cores), width)
     smem = pl.BlockSpec(memory_space=pltpu.SMEM)
+    pieces_in = [
+        pltpu.with_memory_space_constraint(piece, pltpu.VMEM if at % ways else pltpu.HBM)
+        for at, piece in enumerate(pieces)
+    ]
     mixed = pl.pallas_call(
-        lambda *refs: attend_kernel(*refs, step=seq_rows, width=width, maps=maps, block=block),
+        lambda *refs: attend_kernel(
+            *refs, step=seq_rows, width=width, maps=maps, block=block, part_rows=part_rows
+        ),
         grid=(ways,),
         in_specs=[smem, smem, pl.BlockSpec((1, width), lambda index: (0, 0))]
-        + [pl.BlockSpec(piece.shape, lambda index: (0, 0)) for piece in pieces],
+        + [pl.BlockSpec(memory_space=pltpu.VMEM)] * len(pieces),
         out_specs=pl.BlockSpec((1,) + shape[1:], lambda index: (index, 0, 0, 0, 0)),
         out_shape=pltpu.HBM(shape, jnp.bfloat16),
         scratch_shapes=[
             pltpu.VMEM((2, ways, seq_rows, seq_rows), jnp.float32),
-            pltpu.VMEM((ways,) + pieces[0].shape, jnp.bfloat16),
+            pltpu.VMEM((ways, 4 * maps + width, seq_rows), jnp.bfloat16),
         ],
-        compiler_params=pltpu.CompilerParams(dimension_semantics=("arbitrary",), vmem_limit_bytes=24 << 20),
+        compiler_params=pltpu.CompilerParams(dimension_semantics=("arbitrary",), vmem_limit_bytes=16 << 20),
         cost_estimate=pl.CostEstimate(flops=2 * pairs * (maps + width), bytes_accessed=0, transcendentals=pairs),
         name="attend",
-    )(scalars, place[None].astype(jnp.int32), gain[None, :], *pieces)
+    )(scalars, jnp.stack([place, jnp.where(first, 0, 1)]).astype(jnp.int32), gain[None, :], *pieces_in)
     flat = mixed.reshape((-1,) + shape[3:])
     return lax.all_to_all(flat, ("sp", "zl", "c"), split_axis=0, concat_axis=0, tiled=True).reshape(shape)
 
@@ -404,7 +461,8 @@
             core, line = at[0] ^ apart % cores, at[1] ^ apart // cores
 
             def taken(head, used):
-                found = [heads_ref[head, line, core, pl.ds((at[2] ^ far) * block, block), :] for far in range(lines)]
+                index = (head + heads_a * core) % ways
+                found = [heads_ref[index, line, core, pl.ds((at[2] ^ far) * block, block), :] for far in range(lines)]
                 return jnp.concatenate(found, axis=0)[:, :used]
 
             left_a = jnp.concatenate([taken(head, wide) for head in range(heads_a)], axis=1)

time: 211 us -> 213 us (level)
  starting transfers between devices: 57.1 us -> 73.5 us
  waiting for transfers between devices: 95.4 us -> 84.5 us
  other arithmetic: 5.65 us -> 1.47 us
    ppermute x0 -> x6, starting transfers between devices: none -> 17.2 us  [exchanged_heads(): pieces.append(lax.ppermute(packed[group * ways + far], ('sp', 'c'), route))]
    ppermute x44 -> x41, waiting for transfers between devices: 88 us -> 72.6 us  [mirrored(): lax.ppermute(value, axis, [(i, i ^ apart) for i in range(lax.axis_size(ax...]
    ppermute x0 -> x6, waiting for transfers between devices: none -> 4.28 us  [exchanged_heads(): pieces.append(lax.ppermute(packed[group * ways + far], ('sp', 'c'), route))]
    squeeze x1 -> x0, other arithmetic: 2.8 us -> none  [exchanged_heads(): lax.dynamic_index_in_dim(outgoing, place ^ far, 0, False)]
    pallas_call x16 -> x17, Pallas kernels: 24.7 us -> 26.6 us  [whole_call(): pl.pallas_call(body, in_specs=[pl.BlockSpec(memory_space=pltpu.SMEM)] * l...]
    ppermute x44 -> x41, starting transfers between devices: 53.3 us -> 52.3 us  [mirrored(): lax.ppermute(value, axis, [(i, i ^ apart) for i in range(lax.axis_size(ax...]
    unnamed x49 -> x43, local copies, waits for them, and re-layouts: 8.08 us -> 8.25 us
  transfers between devices with their start and end apart: 45 -> 48, of which waited for: 19 -> 19; matrix products, arithmetic and copies ran while one was open for 7% -> 3% of each run, Pallas kernels for 13% -> 14%
where the time goes in v3:
time: 213 us; the launch traced here: 212 us
  waiting for transfers between devices  84.5 us (40%)
  starting transfers between devices  73.5 us (35%)
  Pallas kernels  42.5 us (20%)
  local copies, waits for them, and re-layouts  9.31 us (4%)
    ppermute x41, waiting for transfers between devices, mirrored(): lax.ppermute(value, axis, [(i, i ^ apart) for i in range(lax.axis_size(ax...  72.6 us
    ppermute x41, starting transfers between devices, mirrored(): lax.ppermute(value, axis, [(i, i ^ apart) for i in range(lax.axis_size(ax...  52.3 us
    pallas_call x17, Pallas kernels, whole_call(): pl.pallas_call(body, in_specs=[pl.BlockSpec(memory_space=pltpu.SMEM)] * l...  26.6 us
    ppermute x6, starting transfers between devices, exchanged_heads(): pieces.append(lax.ppermute(packed[group * ways + far], ('sp', 'c'), route))  17.2 us
    pallas_call x1, Pallas kernels, exchanged_heads(): pl.pallas_call(lambda *refs: attend_kernel(*refs, step=seq_rows, width=wi...  16 us
    unnamed x43, local copies, waits for them, and re-layouts  8.25 us
    all_to_all x1, waiting for transfers between devices, exchanged_heads(): lax.all_to_all(flat, ('sp', 'zl', 'c'), split_axis=0, concat_axis=0, tile...  7.56 us
    ppermute x6, waiting for transfers between devices, exchanged_heads(): pieces.append(lax.ppermute(packed[group * ways + far], ('sp', 'c'), route))  4.28 us
  transfers between devices with their start and end apart: 48, of which 19 were waited for; matrix products, arithmetic and copies ran while one was open for 3% of the time, Pallas kernels for 14%

profile of v3, /device:TPU:0, one launch (start us, length us, event | category | flops | bytes accessed | tf_op | source)
XLA Modules:
  0.0 211.6 jit_solution(17531874444008564707)
XLA Ops:
  0.0 3.1 %collective-permute-start.8 = (bf16[256,2048]{1,0:T(8,128)(2,1)}, bf16[256,2048]{1,0:T(8,128)(2,1)S(1)}, u32[]{:S(2)}, u32[]{:S(2)}) collective-permute-start(bf16[256,2048]{1,0:T(8,128)(2,1)} %refs_0_.1), channel_id=1, source_target_pairs={{0,2},{2,0},{1,3},{3,1},{4,6},{6,4},{5,7},{7,5},{8,10},{10,8},{9,1... | collective-permute-start | bytes 3145736 | tf_op jit(solution)/shard_map/ppermute | solution.py:325
  9.3 1.9 shard_map.181
  12.6 1.3 collective-permute-start.3
  13.9 3.4 %collective-permute-start = (bf16[384,512]{1,0:T(8,128)(2,1)}, bf16[384,512]{1,0:T(8,128)(2,1)S(1)}, u32[]{:S(2)}, u32[]{:S(2)}) collective-permute-start(bf16[384,512]{1,0:T(8,128)(2,1)} %get-tuple-element.58), channel_id=1, source_target_pairs={{8,0},{0,8},{25,17},{17,25},{10,2},{2,10},{27,19},{19,27},{12,4},{... | collective-permute-start | bytes 1179656 | tf_op jit(solution)/shard_map/ppermute | solution.py:400
  17.3 1.3 collective-permute-start.1
  18.6 5.2 %collective-permute-start.4 = (bf16[192,512]{1,0:T(8,128)(2,1)}, bf16[192,512]{1,0:T(8,128)(2,1)}, u32[]{:S(2)}, u32[]{:S(2)}) collective-permute-start(bf16[192,512]{1,0:T(8,128)(2,1)} %get-tuple-element.63), channel_id=1, source_target_pairs={{17,1},{25,9},{0,16},{8,24},{19,3},{27,11},{2,18},{10,26},{21,5},{... | collective-permute-start | bytes 589832 | tf_op jit(solution)/shard_map/ppermute | solution.py:400
  24.6 1.3 collective-permute-start.2
  26.8 4.6 %collective-permute-start.5 = (bf16[192,512]{1,0:T(8,128)(2,1)}, bf16[192,512]{1,0:T(8,128)(2,1)S(1)}, u32[]{:S(2)}, u32[]{:S(2)}) collective-permute-start(bf16[192,512]{1,0:T(8,128)(2,1)} %copy-done.11), channel_id=1, source_target_pairs={{25,1},{17,9},{8,16},{0,24},{27,3},{19,11},{10,18},{2,26},{29,5},{... | collective-permute-start | bytes 589832 | tf_op jit(solution)/shard_map/ppermute | solution.py:400
  31.5 3.4 %collective-permute-done.5.refs_10_ = bf16[192,512]{1,0:T(8,128)(2,1)S(1)} collective-permute-done((bf16[192,512]{1,0:T(8,128)(2,1)}, bf16[192,512]{1,0:T(8,128)(2,1)S(1)}, u32[]{:S(2)}, u32[]{:S(2)}) %collective-permute-start.5) | collective-permute-done | bytes 196640 | tf_op jit(solution)/shard_map/ppermute | solution.py:400
  36.1 2.1 %collective-permute-start.6 = (bf16[256,2048]{1,0:T(8,128)(2,1)S(1)}, bf16[256,2048]{1,0:T(8,128)(2,1)}, u32[]{:S(2)}, u32[]{:S(2)}) collective-permute-start(bf16[256,2048]{1,0:T(8,128)(2,1)S(1)} %copy-done.3), channel_id=1, source_target_pairs={{0,1},{1,0},{2,3},{3,2},{4,5},{5,4},{6,7},{7,6},{8,9},{9,8},{10,11... | collective-permute-start | bytes 3145736 | tf_op jit(solution)/shard_map/ppermute | solution.py:325
  38.3 16.0 %attend.1 = bf16[4,2,2,128,128]{4,3,2,1,0:T(8,128)(2,1)} custom-call(f32[3]{0:T(128)S(1)} %pad_maximum_fusion.2.refs_0_, s32[2]{0:T(128)S(1)} %pad_add_fusion.1.refs_1_, f32[1,128]{1,0:T(1,128)S(1)} %fusion.2.refs_2_, bf16[384,512]{1,0:T(8,128)(2,1)} %get-tuple-element.57.refs_3_, bf16[384,512]{1,0:T(8,128)(2,1)S(1)} %collective-permute-done.refs_4_, ...), custom_call_target="tpu_custom_call" | custom-call | flops 2013265920 | tf_op jit(solution)/shard_map/attend/pallas_call | solution.py:419
  54.3 4.0 %all-to-all-start = ((bf16[16,128,128]{2,1,0:T(8,128)(2,1)}), bf16[16,128,128]{2,1,0:T(8,128)(2,1)S(1)}, u32[]{:S(2)}, u32[]{:S(2)}) async-start(bf16[16,128,128]{2,1,0:T(8,128)(2,1)} %bitcast.46), calls=%async_computation | async-start | bytes 1048576 | tf_op jit(solution)/shard_map/all_to_all | solution.py:437
  61.2 7.6 %all-to-all-done = bf16[16,128,128]{2,1,0:T(8,128)(2,1)S(1)} async-done(((bf16[16,128,128]{2,1,0:T(8,128)(2,1)}), bf16[16,128,128]{2,1,0:T(8,128)(2,1)S(1)}, u32[]{:S(2)}, u32[]{:S(2)}) %all-to-all-start) | async-done | bytes 524320 | tf_op jit(solution)/shard_map/all_to_all | solution.py:437
  68.8 3.5 %shard_map.182 = (bf16[64,2048]{1,0:T(8,128)(2,1)S(1)}, bf16[64,2048]{1,0:T(8,128)(2,1)S(1)}) custom-call(s32[3]{0:T(128)S(1)} %pad_add_fusion.at, bf16[4,2,2,128,128]{4,3,2,1,0:T(8,128)(2,1)S(1)} %bitcast.38, bf16[256,2048]{1,0:T(8,128)(2,1)S(1)} %copy-done.3, bf16[128,2048]{1,0:T(8,128)(2,1)S(1)} %copy-done.4, ...), custom_call_target="tpu_custom_call" | custom-call | flops 805306368 | tf_op jit(solution)/shard_map/pallas_call | solution.py:335
  72.3 2.7 %collective-permute-start.12 = (bf16[64,2048]{1,0:T(8,128)(2,1)S(1)}, bf16[64,2048]{1,0:T(8,128)(2,1)S(1)}, u32[]{:S(2)}, u32[]{:S(2)}) collective-permute-start(bf16[64,2048]{1,0:T(8,128)(2,1)S(1)} %get-tuple-element.66), channel_id=1, source_target_pairs={{0,4},{4,0},{1,5},{5,1},{2,6},{6,2},{3,7},{7,3},{8,12},{12,8},{9,1... | collective-permute-start | bytes 786440 | tf_op jit(solution)/shard_map/ppermute | solution.py:325
  75.0 11.0 %collective-permute-done.12.refs_1_ = bf16[64,2048]{1,0:T(8,128)(2,1)S(1)} collective-permute-done((bf16[64,2048]{1,0:T(8,128)(2,1)S(1)}, bf16[64,2048]{1,0:T(8,128)(2,1)S(1)}, u32[]{:S(2)}, u32[]{:S(2)}) %collective-permute-start.12) | collective-permute-done | bytes 262176 | tf_op jit(solution)/shard_map/ppermute | solution.py:325
  86.6 3.1 %collective-permute-start.20 = (bf16[64,1536]{1,0:T(8,128)(2,1)S(1)}, bf16[64,1536]{1,0:T(8,128)(2,1)S(1)}, u32[]{:S(2)}, u32[]{:S(2)}) collective-permute-start(bf16[64,1536]{1,0:T(8,128)(2,1)S(1)} %get-tuple-element.72.refs_0_), channel_id=1, source_target_pairs={{0,4},{2,6},{4,0},{6,2},{1,5},{3,7},{5,1},{7,3},{8,12},{10,14},{12... | collective-permute-start | bytes 589832 | tf_op jit(solution)/shard_map/ppermute | solution.py:325
  91.7 3.4 %collective-permute-done.13 = bf16[48,512]{1,0:T(8,128)(2,1)S(1)} collective-permute-done((bf16[48,512]{1,0:T(8,128)(2,1)S(1)}, bf16[48,512]{1,0:T(8,128)(2,1)S(1)}, u32[]{:S(2)}, u32[]{:S(2)}) %collective-permute-start.13) | collective-permute-done | bytes 49184 | tf_op jit(solution)/shard_map/ppermute | solution.py:325
  95.9 3.3 %collective-permute-done.14 = bf16[48,512]{1,0:T(8,128)(2,1)S(1)} collective-permute-done((bf16[48,512]{1,0:T(8,128)(2,1)S(1)}, bf16[48,512]{1,0:T(8,128)(2,1)S(1)}, u32[]{:S(2)}, u32[]{:S(2)}) %collective-permute-start.14) | collective-permute-done | bytes 49184 | tf_op jit(solution)/shard_map/ppermute | solution.py:325
  99.1 1.3 collective-permute-start.15
  101.0 3.1 %collective-permute-done.15 = bf16[48,512]{1,0:T(8,128)(2,1)S(1)} collective-permute-done((bf16[48,512]{1,0:T(8,128)(2,1)S(1)}, bf16[48,512]{1,0:T(8,128)(2,1)S(1)}, u32[]{:S(2)}, u32[]{:S(2)}) %collective-permute-start.15) | collective-permute-done | bytes 49184 | tf_op jit(solution)/shard_map/ppermute | solution.py:325
  104.1 2.6 %collective-permute-start.24 = (f32[4,64]{1,0:T(4,128)S(1)}, f32[4,64]{1,0:T(4,128)S(1)}, u32[]{:S(2)}, u32[]{:S(2)}) collective-permute-start(f32[4,64]{1,0:T(4,128)S(1)} %pad_maximum_fusion.refs_4_.routes_ref), channel_id=1, source_target_pairs={{0,6},{2,4},{4,2},{6,0},{1,7},{3,5},{5,3},{7,1},{8,14},{10,12},{12... | collective-permute-start | bytes 3080 | tf_op jit(solution)/shard_map/ppermute | solution.py:325
  107.2 2.3 %collective-permute-done.24.refs_7_ = f32[4,64]{1,0:T(4,128)S(1)} collective-permute-done((f32[4,64]{1,0:T(4,128)S(1)}, f32[4,64]{1,0:T(4,128)S(1)}, u32[]{:S(2)}, u32[]{:S(2)}) %collective-permute-start.24) | collective-permute-done | bytes 1056 | tf_op jit(solution)/shard_map/ppermute | solution.py:325
  112.3 3.3 %collective-permute-start.17 = (bf16[192,512]{1,0:T(8,128)(2,1)S(1)}, bf16[192,512]{1,0:T(8,128)(2,1)S(1)}, u32[]{:S(2)}, u32[]{:S(2)}) collective-permute-start(bf16[192,512]{1,0:T(8,128)(2,1)S(1)} %constant_dynamic-update-slice_fusion.refs_8_.refs_0_), channel_id=1, source_target_pairs={{0,4},{2,6},{4,0},{6,2},{1,5},{3,7},{5,1},{7,3},{8,12},{10,14},{12... | collective-permute-start | bytes 589832 | tf_op jit(solution)/shard_map/ppermute | solution.py:325
  116.6 4.4 %collective-permute-done.16.refs_1_ = bf16[192,512]{1,0:T(8,128)(2,1)S(1)} collective-permute-done((bf16[192,512]{1,0:T(8,128)(2,1)S(1)}, bf16[192,512]{1,0:T(8,128)(2,1)S(1)}, u32[]{:S(2)}, u32[]{:S(2)}) %collective-permute-start.16) | collective-permute-done | bytes 196640 | tf_op jit(solution)/shard_map/ppermute | solution.py:325
  121.1 5.8 %collective-permute-done.17.refs_2_ = bf16[192,512]{1,0:T(8,128)(2,1)S(1)} collective-permute-done((bf16[192,512]{1,0:T(8,128)(2,1)S(1)}, bf16[192,512]{1,0:T(8,128)(2,1)S(1)}, u32[]{:S(2)}, u32[]{:S(2)}) %collective-permute-start.17) | collective-permute-done | bytes 196640 | tf_op jit(solution)/shard_map/ppermute | solution.py:325
  127.1 4.4 %shard_map.186.rows_ref.refs_3_ = bf16[576,768]{1,0:T(8,128)(2,1)S(1)} custom-call(bf16[576,2048]{1,0:T(8,128)(2,1)S(1)} %shard_map.185.rows_ref, bf16[2048,768]{1,0:T(8,128)(2,1)S(1)} %bitcast.25, bf16[2048,768]{1,0:T(8,128)(2,1)S(1)} %bitcast.30), custom_call_target="tpu_custom_call" | custom-call | flops 3623878656 | tf_op jit(solution)/shard_map/pallas_call | solution.py:335
  131.6 6.3 %shard_map.188.refs_5_ = bf16[576,2048]{1,0:T(8,128)(2,1)S(1)} custom-call(bf16[576,2048]{1,0:T(8,128)(2,1)S(1)} %collective-permute-done.27.rows_ref, bf16[2048,768]{1,0:T(8,128)(2,1)S(1)} %bitcast.26, bf16[2048,768]{1,0:T(8,128)(2,1)S(1)} %bitcast.31, bf16[768,2048]{1,0:T(8,128)(2,1)S(1)} %bitcast.34, bf16[576,768]{1,0:T(8,128)(2,1)S(1)} %shard_map.186.rows_ref.refs_3_), custom_call_target="tpu_custom_call" | custom-call | flops 5435817984 | tf_op jit(solution)/shard_map/pallas_call | solution.py:335
  138.4 1.7 collective-permute-start.32
  140.0 14.6 %collective-permute-done.32.refs_4_ = bf16[192,1536]{1,0:T(8,128)(2,1)S(1)} collective-permute-done((bf16[192,1536]{1,0:T(8,128)(2,1)S(1)}, bf16[192,1536]{1,0:T(8,128)(2,1)S(1)}, u32[]{:S(2)}, u32[]{:S(2)}) %collective-permute-start.32) | collective-permute-done | bytes 589856 | tf_op jit(solution)/shard_map/ppermute | solution.py:325
  154.8 2.6 %shard_map.187.refs_0_ = bf16[576,2048]{1,0:T(8,128)(2,1)S(1)} custom-call(bf16[576,768]{1,0:T(8,128)(2,1)S(1)} %shard_map.186.rows_ref.refs_3_, bf16[768,2048]{1,0:T(8,128)(2,1)S(1)} %bitcast.35), custom_call_target="tpu_custom_call" | custom-call | flops 1811939328 | tf_op jit(solution)/shard_map/pallas_call | solution.py:335
  157.3 1.5 shard_map.191.rows_ref.refs_3_
  159.4 2.1 shard_map.193
  162.1 1.5 collective-permute-start.41
  165.4 1.3 collective-permute-start.43
  166.7 2.6 %collective-permute-start.29 = (bf16[144,640]{1,0:T(8,128)(2,1)S(1)}, bf16[144,640]{1,0:T(8,128)(2,1)S(1)}, u32[]{:S(2)}, u32[]{:S(2)}) collective-permute-start(bf16[144,640]{1,0:T(8,128)(2,1)S(1)} %get-tuple-element.77), channel_id=1, source_target_pairs={{0,2},{2,0},{4,6},{6,4},{1,3},{3,1},{5,7},{7,5},{8,10},{10,8},{12,... | collective-permute-start | bytes 552968 | tf_op jit(solution)/shard_map/ppermute | solution.py:325
  170.3 6.2 %collective-permute-done.29.refs_1_ = bf16[144,640]{1,0:T(8,128)(2,1)S(1)} collective-permute-done((bf16[144,640]{1,0:T(8,128)(2,1)S(1)}, bf16[144,640]{1,0:T(8,128)(2,1)S(1)}, u32[]{:S(2)}, u32[]{:S(2)}) %collective-permute-start.29) | collective-permute-done | bytes 184352 | tf_op jit(solution)/shard_map/ppermute | solution.py:325
  176.6 1.9 collective-permute-start.31
  178.4 1.4 collective-permute-start.35
  179.9 10.2 %collective-permute-done.42.refs_2_ = bf16[192,1408]{1,0:T(8,128)(2,1)S(1)} collective-permute-done((bf16[192,1408]{1,0:T(8,128)(2,1)S(1)}, bf16[192,1408]{1,0:T(8,128)(2,1)S(1)}, u32[]{:S(2)}, u32[]{:S(2)}) %collective-permute-start.42) | collective-permute-done | bytes 540704 | tf_op jit(solution)/shard_map/ppermute | solution.py:325
  190.0 3.6 %collective-permute-start.36 = (bf16[48,640]{1,0:T(8,128)(2,1)S(1)}, bf16[48,640]{1,0:T(8,128)(2,1)S(1)}, u32[]{:S(2)}, u32[]{:S(2)}) collective-permute-start(bf16[48,640]{1,0:T(8,128)(2,1)S(1)} %get-tuple-element.83), channel_id=1, source_target_pairs={{0,4},{2,6},{4,0},{6,2},{1,5},{3,7},{5,1},{7,3},{8,12},{10,14},{12... | collective-permute-start | bytes 184328 | tf_op jit(solution)/shard_map/ppermute | solution.py:325
  193.7 1.4 collective-permute-start.37
  196.2 3.0 %collective-permute-start.45 = (bf16[64,1408]{1,0:T(8,128)(2,1)S(1)}, bf16[64,1408]{1,0:T(8,128)(2,1)S(1)}, u32[]{:S(2)}, u32[]{:S(2)}) collective-permute-start(bf16[64,1408]{1,0:T(8,128)(2,1)S(1)} %get-tuple-element.95), channel_id=1, source_target_pairs={{0,4},{2,6},{4,0},{6,2},{1,5},{3,7},{5,1},{7,3},{8,12},{10,14},{12... | collective-permute-start | bytes 540680 | tf_op jit(solution)/shard_map/ppermute | solution.py:325
  199.2 1.4 collective-permute-start.46
  201.3 1.7 collective-permute-start.39
  203.0 2.4 %collective-permute-done.38.refs_1_ = bf16[48,640]{1,0:T(8,128)(2,1)S(1)} collective-permute-done((bf16[48,640]{1,0:T(8,128)(2,1)S(1)}, bf16[48,640]{1,0:T(8,128)(2,1)S(1)}, u32[]{:S(2)}, u32[]{:S(2)}) %collective-permute-start.38) | collective-permute-done | bytes 61472 | tf_op jit(solution)/shard_map/ppermute | solution.py:325
  205.4 1.2 collective-permute-start.40
  206.7 3.9 %collective-permute-done.40.refs_3_ = bf16[48,640]{1,0:T(8,128)(2,1)S(1)} collective-permute-done((bf16[48,640]{1,0:T(8,128)(2,1)S(1)}, bf16[48,640]{1,0:T(8,128)(2,1)S(1)}, u32[]{:S(2)}, u32[]{:S(2)}) %collective-permute-start.40) | collective-permute-done | bytes 61472 | tf_op jit(solution)/shard_map/ppermute | solution.py:325
  (127 shorter events, 29.3 us)
Async XLA Ops:
  0.0 38.2 %collective-permute-start.8 = (bf16[256,2048]{1,0:T(8,128)(2,1)}, bf16[256,2048]{1,0:T(8,128)(2,1)S(1)}, u32[]{:S(2)}, u32[]{:S(2)}) collective-permute-start(bf16[256,2048]{1,0:T(8,128)(2,1)} %refs_0_.1), channel_id=1, source_target_pairs={{0,2},{2,0},{1,3},{3,1},{4,6},{6,4},{5,7},{7,5},{8,10},{10,8},{9,1... | collective-permute-start | bytes 3145736 | tf_op jit(solution)/shard_map/ppermute | solution.py:325
  12.6 12.0 %collective-permute-start.3 = (bf16[192,512]{1,0:T(8,128)(2,1)}, bf16[192,512]{1,0:T(8,128)(2,1)}, u32[]{:S(2)}, u32[]{:S(2)}) collective-permute-start(bf16[192,512]{1,0:T(8,128)(2,1)} %get-tuple-element.62), channel_id=1, source_target_pairs={{9,1},{1,9},{24,16},{16,24},{11,3},{3,11},{26,18},{18,26},{13,5},{... | collective-permute-start | bytes 589832 | tf_op jit(solution)/shard_map/ppermute | solution.py:400
  13.9 22.1 %collective-permute-start = (bf16[384,512]{1,0:T(8,128)(2,1)}, bf16[384,512]{1,0:T(8,128)(2,1)S(1)}, u32[]{:S(2)}, u32[]{:S(2)}) collective-permute-start(bf16[384,512]{1,0:T(8,128)(2,1)} %get-tuple-element.58), channel_id=1, source_target_pairs={{8,0},{0,8},{25,17},{17,25},{10,2},{2,10},{27,19},{19,27},{12,4},{... | collective-permute-start | bytes 1179656 | tf_op jit(solution)/shard_map/ppermute | solution.py:400
  17.3 21.0 %collective-permute-start.1 = (bf16[384,512]{1,0:T(8,128)(2,1)}, bf16[384,512]{1,0:T(8,128)(2,1)S(1)}, u32[]{:S(2)}, u32[]{:S(2)}) collective-permute-start(bf16[384,512]{1,0:T(8,128)(2,1)} %get-tuple-element.59), channel_id=1, source_target_pairs={{16,0},{24,8},{1,17},{9,25},{18,2},{26,10},{3,19},{11,27},{20,4},{... | collective-permute-start | bytes 1179656 | tf_op jit(solution)/shard_map/ppermute | solution.py:400
  18.6 8.1 %collective-permute-start.4 = (bf16[192,512]{1,0:T(8,128)(2,1)}, bf16[192,512]{1,0:T(8,128)(2,1)}, u32[]{:S(2)}, u32[]{:S(2)}) collective-permute-start(bf16[192,512]{1,0:T(8,128)(2,1)} %get-tuple-element.63), channel_id=1, source_target_pairs={{17,1},{25,9},{0,16},{8,24},{19,3},{27,11},{2,18},{10,26},{21,5},{... | collective-permute-start | bytes 589832 | tf_op jit(solution)/shard_map/ppermute | solution.py:400
  24.6 13.7 %collective-permute-start.2 = (bf16[384,512]{1,0:T(8,128)(2,1)}, bf16[384,512]{1,0:T(8,128)(2,1)S(1)}, u32[]{:S(2)}, u32[]{:S(2)}) collective-permute-start(bf16[384,512]{1,0:T(8,128)(2,1)} %copy-done.10), channel_id=1, source_target_pairs={{24,0},{16,8},{9,17},{1,25},{26,2},{18,10},{11,19},{3,27},{28,4},{... | collective-permute-start | bytes 1179656 | tf_op jit(solution)/shard_map/ppermute | solution.py:400
  26.8 8.1 %collective-permute-start.5 = (bf16[192,512]{1,0:T(8,128)(2,1)}, bf16[192,512]{1,0:T(8,128)(2,1)S(1)}, u32[]{:S(2)}, u32[]{:S(2)}) collective-permute-start(bf16[192,512]{1,0:T(8,128)(2,1)} %copy-done.11), channel_id=1, source_target_pairs={{25,1},{17,9},{8,16},{0,24},{27,3},{19,11},{10,18},{2,26},{29,5},{... | collective-permute-start | bytes 589832 | tf_op jit(solution)/shard_map/ppermute | solution.py:400
  34.9 23.8 %collective-permute-start.9 = (bf16[128,2048]{1,0:T(8,128)(2,1)S(1)}, bf16[128,2048]{1,0:T(8,128)(2,1)}, u32[]{:S(2)}, u32[]{:S(2)}) collective-permute-start(bf16[128,2048]{1,0:T(8,128)(2,1)S(1)} %copy-done.4), channel_id=1, source_target_pairs={{0,2},{2,0},{1,3},{3,1},{4,6},{6,4},{5,7},{7,5},{8,10},{10,8},{9,1... | collective-permute-start | bytes 1572872 | tf_op jit(solution)/shard_map/ppermute | solution.py:325
  36.1 25.2 %collective-permute-start.6 = (bf16[256,2048]{1,0:T(8,128)(2,1)S(1)}, bf16[256,2048]{1,0:T(8,128)(2,1)}, u32[]{:S(2)}, u32[]{:S(2)}) collective-permute-start(bf16[256,2048]{1,0:T(8,128)(2,1)S(1)} %copy-done.3), channel_id=1, source_target_pairs={{0,1},{1,0},{2,3},{3,2},{4,5},{5,4},{6,7},{7,6},{8,9},{9,8},{10,11... | collective-permute-start | bytes 3145736 | tf_op jit(solution)/shard_map/ppermute | solution.py:325
  38.2 30.6 %collective-permute-start.10 = (bf16[256,2048]{1,0:T(8,128)(2,1)S(1)}, bf16[256,2048]{1,0:T(8,128)(2,1)}, u32[]{:S(2)}, u32[]{:S(2)}) collective-permute-start(bf16[256,2048]{1,0:T(8,128)(2,1)S(1)} %collective-permute-done.8.refs_4_), channel_id=1, source_target_pairs={{0,1},{1,0},{2,3},{3,2},{4,5},{5,4},{6,7},{7,6},{8,9},{9,8},{10,11... | collective-permute-start | bytes 3145736 | tf_op jit(solution)/shard_map/ppermute | solution.py:325
  54.3 14.5 %all-to-all-start = ((bf16[16,128,128]{2,1,0:T(8,128)(2,1)}), bf16[16,128,128]{2,1,0:T(8,128)(2,1)S(1)}, u32[]{:S(2)}, u32[]{:S(2)}) async-start(bf16[16,128,128]{2,1,0:T(8,128)(2,1)} %bitcast.46), calls=%async_computation | async-start | bytes 1048576 | tf_op jit(solution)/shard_map/all_to_all | solution.py:437
  58.3 2.2 %collective-permute-start.7 = (bf16[128,2048]{1,0:T(8,128)(2,1)S(1)}, bf16[128,2048]{1,0:T(8,128)(2,1)}, u32[]{:S(2)}, u32[]{:S(2)}) collective-permute-start(bf16[128,2048]{1,0:T(8,128)(2,1)S(1)} %copy-done.4), channel_id=1, source_target_pairs={{0,1},{1,0},{2,3},{3,2},{4,5},{5,4},{6,7},{7,6},{8,9},{9,8},{10,11... | collective-permute-start | bytes 1572872 | tf_op jit(solution)/shard_map/ppermute | solution.py:325
  58.7 2.5 %collective-permute-start.11 = (bf16[128,2048]{1,0:T(8,128)(2,1)}, bf16[128,2048]{1,0:T(8,128)(2,1)}, u32[]{:S(2)}, u32[]{:S(2)}) collective-permute-start(bf16[128,2048]{1,0:T(8,128)(2,1)} %collective-permute-done.9.refs_5_), channel_id=1, source_target_pairs={{0,1},{1,0},{2,3},{3,2},{4,5},{5,4},{6,7},{7,6},{8,9},{9,8},{10,11... | collective-permute-start | bytes 1572872 | tf_op jit(solution)/shard_map/ppermute | solution.py:325
  72.3 13.8 %collective-permute-start.12 = (bf16[64,2048]{1,0:T(8,128)(2,1)S(1)}, bf16[64,2048]{1,0:T(8,128)(2,1)S(1)}, u32[]{:S(2)}, u32[]{:S(2)}) collective-permute-start(bf16[64,2048]{1,0:T(8,128)(2,1)S(1)} %get-tuple-element.66), channel_id=1, source_target_pairs={{0,4},{4,0},{1,5},{5,1},{2,6},{6,2},{3,7},{7,3},{8,12},{12,8},{9,1... | collective-permute-start | bytes 786440 | tf_op jit(solution)/shard_map/ppermute | solution.py:325
  75.0 25.5 %collective-permute-start.22 = (f32[4,64]{1,0:T(4,128)S(1)}, f32[4,64]{1,0:T(4,128)S(1)}, u32[]{:S(2)}, u32[]{:S(2)}) collective-permute-start(f32[4,64]{1,0:T(4,128)S(1)} %pad_maximum_fusion.refs_4_.routes_ref), channel_id=1, source_target_pairs={{0,2},{2,0},{4,6},{6,4},{1,3},{3,1},{5,7},{7,5},{8,10},{10,8},{12,... | collective-permute-start | bytes 3080 | tf_op jit(solution)/shard_map/ppermute | solution.py:325
  86.5 23.0 %collective-permute-start.19 = (bf16[64,1536]{1,0:T(8,128)(2,1)S(1)}, bf16[64,1536]{1,0:T(8,128)(2,1)S(1)}, u32[]{:S(2)}, u32[]{:S(2)}) collective-permute-start(bf16[64,1536]{1,0:T(8,128)(2,1)S(1)} %get-tuple-element.72.refs_0_), channel_id=1, source_target_pairs={{0,2},{2,0},{4,6},{6,4},{1,3},{3,1},{5,7},{7,5},{8,10},{10,8},{12,... | collective-permute-start | bytes 589832 | tf_op jit(solution)/shard_map/ppermute | solution.py:325
  86.6 22.9 %collective-permute-start.20 = (bf16[64,1536]{1,0:T(8,128)(2,1)S(1)}, bf16[64,1536]{1,0:T(8,128)(2,1)S(1)}, u32[]{:S(2)}, u32[]{:S(2)}) collective-permute-start(bf16[64,1536]{1,0:T(8,128)(2,1)S(1)} %get-tuple-element.72.refs_0_), channel_id=1, source_target_pairs={{0,4},{2,6},{4,0},{6,2},{1,5},{3,7},{5,1},{7,3},{8,12},{10,14},{12... | collective-permute-start | bytes 589832 | tf_op jit(solution)/shard_map/ppermute | solution.py:325
  89.7 19.8 %collective-permute-start.21 = (bf16[64,1536]{1,0:T(8,128)(2,1)S(1)}, bf16[64,1536]{1,0:T(8,128)(2,1)S(1)}, u32[]{:S(2)}, u32[]{:S(2)}) collective-permute-start(bf16[64,1536]{1,0:T(8,128)(2,1)S(1)} %get-tuple-element.72.refs_0_), channel_id=1, source_target_pairs={{0,6},{2,4},{4,2},{6,0},{1,7},{3,5},{5,3},{7,1},{8,14},{10,12},{12... | collective-permute-start | bytes 589832 | tf_op jit(solution)/shard_map/ppermute | solution.py:325
  90.9 4.1 %collective-permute-start.13 = (bf16[48,512]{1,0:T(8,128)(2,1)S(1)}, bf16[48,512]{1,0:T(8,128)(2,1)S(1)}, u32[]{:S(2)}, u32[]{:S(2)}) collective-permute-start(bf16[48,512]{1,0:T(8,128)(2,1)S(1)} %get-tuple-element.69), channel_id=1, source_target_pairs={{0,8},{8,0},{16,24},{24,16},{1,9},{9,1},{17,25},{25,17},{2,10},{10... | collective-permute-start | bytes 147464 | tf_op jit(solution)/shard_map/ppermute | solution.py:325
  95.0 4.1 %collective-permute-start.14 = (bf16[48,512]{1,0:T(8,128)(2,1)S(1)}, bf16[48,512]{1,0:T(8,128)(2,1)S(1)}, u32[]{:S(2)}, u32[]{:S(2)}) collective-permute-start(bf16[48,512]{1,0:T(8,128)(2,1)S(1)} %get-tuple-element.70), channel_id=1, source_target_pairs={{0,16},{8,24},{16,0},{24,8},{1,17},{9,25},{17,1},{25,9},{2,18},{10... | collective-permute-start | bytes 147464 | tf_op jit(solution)/shard_map/ppermute | solution.py:325
  99.1 5.0 %collective-permute-start.15 = (bf16[48,512]{1,0:T(8,128)(2,1)S(1)}, bf16[48,512]{1,0:T(8,128)(2,1)S(1)}, u32[]{:S(2)}, u32[]{:S(2)}) collective-permute-start(bf16[48,512]{1,0:T(8,128)(2,1)S(1)} %get-tuple-element.71), channel_id=1, source_target_pairs={{0,24},{8,16},{16,8},{24,0},{1,25},{9,17},{17,9},{25,1},{2,26},{10... | collective-permute-start | bytes 147464 | tf_op jit(solution)/shard_map/ppermute | solution.py:325
  100.5 6.7 %collective-permute-start.23 = (f32[4,64]{1,0:T(4,128)S(1)}, f32[4,64]{1,0:T(4,128)S(1)}, u32[]{:S(2)}, u32[]{:S(2)}) collective-permute-start(f32[4,64]{1,0:T(4,128)S(1)} %pad_maximum_fusion.refs_4_.routes_ref), channel_id=1, source_target_pairs={{0,4},{2,6},{4,0},{6,2},{1,5},{3,7},{5,1},{7,3},{8,12},{10,14},{12... | collective-permute-start | bytes 3080 | tf_op jit(solution)/shard_map/ppermute | solution.py:325
  104.1 5.4 %collective-permute-start.24 = (f32[4,64]{1,0:T(4,128)S(1)}, f32[4,64]{1,0:T(4,128)S(1)}, u32[]{:S(2)}, u32[]{:S(2)}) collective-permute-start(f32[4,64]{1,0:T(4,128)S(1)} %pad_maximum_fusion.refs_4_.routes_ref), channel_id=1, source_target_pairs={{0,6},{2,4},{4,2},{6,0},{1,7},{3,5},{5,3},{7,1},{8,14},{10,12},{12... | collective-permute-start | bytes 3080 | tf_op jit(solution)/shard_map/ppermute | solution.py:325
  110.3 16.6 %collective-permute-start.25 = (bf16[192,1536]{1,0:T(8,128)(2,1)S(1)}, bf16[192,1536]{1,0:T(8,128)(2,1)S(1)}, u32[]{:S(2)}, u32[]{:S(2)}) collective-permute-start(bf16[192,1536]{1,0:T(8,128)(2,1)S(1)} %get-tuple-element.74), channel_id=1, source_target_pairs={{0,8},{8,0},{16,24},{24,16},{1,9},{9,1},{17,25},{25,17},{2,10},{10... | collective-permute-start | bytes 1769480 | tf_op jit(solution)/shard_map/ppermute | solution.py:325
  111.1 15.8 %collective-permute-start.26 = (bf16[192,1536]{1,0:T(8,128)(2,1)S(1)}, bf16[192,1536]{1,0:T(8,128)(2,1)S(1)}, u32[]{:S(2)}, u32[]{:S(2)}) collective-permute-start(bf16[192,1536]{1,0:T(8,128)(2,1)S(1)} %get-tuple-element.75), channel_id=1, source_target_pairs={{0,16},{8,24},{16,0},{24,8},{1,17},{9,25},{17,1},{25,9},{2,18},{10... | collective-permute-start | bytes 1769480 | tf_op jit(solution)/shard_map/ppermute | solution.py:325
  112.2 8.8 %collective-permute-start.16 = (bf16[192,512]{1,0:T(8,128)(2,1)S(1)}, bf16[192,512]{1,0:T(8,128)(2,1)S(1)}, u32[]{:S(2)}, u32[]{:S(2)}) collective-permute-start(bf16[192,512]{1,0:T(8,128)(2,1)S(1)} %constant_dynamic-update-slice_fusion.refs_8_.refs_0_), channel_id=1, source_target_pairs={{0,2},{2,0},{4,6},{6,4},{1,3},{3,1},{5,7},{7,5},{8,10},{10,8},{12,... | collective-permute-start | bytes 589832 | tf_op jit(solution)/shard_map/ppermute | solution.py:325
  112.3 14.6 %collective-permute-start.17 = (bf16[192,512]{1,0:T(8,128)(2,1)S(1)}, bf16[192,512]{1,0:T(8,128)(2,1)S(1)}, u32[]{:S(2)}, u32[]{:S(2)}) collective-permute-start(bf16[192,512]{1,0:T(8,128)(2,1)S(1)} %constant_dynamic-update-slice_fusion.refs_8_.refs_0_), channel_id=1, source_target_pairs={{0,4},{2,6},{4,0},{6,2},{1,5},{3,7},{5,1},{7,3},{8,12},{10,14},{12... | collective-permute-start | bytes 589832 | tf_op jit(solution)/shard_map/ppermute | solution.py:325
  115.5 11.3 %collective-permute-start.18 = (bf16[192,512]{1,0:T(8,128)(2,1)S(1)}, bf16[192,512]{1,0:T(8,128)(2,1)S(1)}, u32[]{:S(2)}, u32[]{:S(2)}) collective-permute-start(bf16[192,512]{1,0:T(8,128)(2,1)S(1)} %constant_dynamic-update-slice_fusion.refs_8_.refs_0_), channel_id=1, source_target_pairs={{0,6},{2,4},{4,2},{6,0},{1,7},{3,5},{5,3},{7,1},{8,14},{10,12},{12... | collective-permute-start | bytes 589832 | tf_op jit(solution)/shard_map/ppermute | solution.py:325
  127.0 4.6 %collective-permute-start.27 = (bf16[576,2048]{1,0:T(8,128)(2,1)S(1)}, bf16[576,2048]{1,0:T(8,128)(2,1)S(1)}, u32[]{:S(2)}, u32[]{:S(2)}) collective-permute-start(bf16[576,2048]{1,0:T(8,128)(2,1)S(1)} %shard_map.185.rows_ref), channel_id=1, source_target_pairs={{0,1},{1,0},{2,3},{3,2},{4,5},{5,4},{6,7},{7,6},{8,9},{9,8},{10,11... | collective-permute-start | bytes 7077896 | tf_op jit(solution)/shard_map/ppermute | solution.py:325
  137.9 20.9 %collective-permute-start.28 = (bf16[576,2048]{1,0:T(8,128)(2,1)S(1)}, bf16[576,2048]{1,0:T(8,128)(2,1)S(1)}, u32[]{:S(2)}, u32[]{:S(2)}) collective-permute-start(bf16[576,2048]{1,0:T(8,128)(2,1)S(1)} %shard_map.188.refs_5_), channel_id=1, source_target_pairs={{0,1},{1,0},{2,3},{3,2},{4,5},{5,4},{6,7},{7,6},{8,9},{9,8},{10,11... | collective-permute-start | bytes 7077896 | tf_op jit(solution)/shard_map/ppermute | solution.py:325
  138.4 16.2 %collective-permute-start.32 = (bf16[192,1536]{1,0:T(8,128)(2,1)S(1)}, bf16[192,1536]{1,0:T(8,128)(2,1)S(1)}, u32[]{:S(2)}, u32[]{:S(2)}) collective-permute-start(bf16[192,1536]{1,0:T(8,128)(2,1)S(1)} %get-tuple-element.80), channel_id=1, source_target_pairs={{0,24},{8,16},{16,8},{24,0},{1,25},{9,17},{17,9},{25,1},{2,26},{10... | collective-permute-start | bytes 1769480 | tf_op jit(solution)/shard_map/ppermute | solution.py:325
  154.7 4.7 %collective-permute-start.33 = (bf16[192,2048]{1,0:T(8,128)(2,1)S(1)}, bf16[192,2048]{1,0:T(8,128)(2,1)S(1)}, u32[]{:S(2)}, u32[]{:S(2)}) collective-permute-start(bf16[192,2048]{1,0:T(8,128)(2,1)S(1)} %shard_map.190.rows_ref), channel_id=1, source_target_pairs={{0,1},{1,0},{2,3},{3,2},{4,5},{5,4},{6,7},{7,6},{8,9},{9,8},{10,11... | collective-permute-start | bytes 2359304 | tf_op jit(solution)/shard_map/ppermute | solution.py:325
  161.5 3.7 %collective-permute-start.34 = (bf16[192,2048]{1,0:T(8,128)(2,1)S(1)}, bf16[192,2048]{1,0:T(8,128)(2,1)S(1)}, u32[]{:S(2)}, u32[]{:S(2)}) collective-permute-start(bf16[192,2048]{1,0:T(8,128)(2,1)S(1)} %shard_map.193), channel_id=1, source_target_pairs={{0,1},{1,0},{2,3},{3,2},{4,5},{5,4},{6,7},{7,6},{8,9},{9,8},{10,11... | collective-permute-start | bytes 2359304 | tf_op jit(solution)/shard_map/ppermute | solution.py:325
  162.1 16.4 %collective-permute-start.41 = (bf16[192,1408]{1,0:T(8,128)(2,1)S(1)}, bf16[192,1408]{1,0:T(8,128)(2,1)S(1)}, u32[]{:S(2)}, u32[]{:S(2)}) collective-permute-start(bf16[192,1408]{1,0:T(8,128)(2,1)S(1)} %get-tuple-element.90), channel_id=1, source_target_pairs={{0,8},{8,0},{16,24},{24,16},{1,9},{9,1},{17,25},{25,17},{2,10},{10... | collective-permute-start | bytes 1622024 | tf_op jit(solution)/shard_map/ppermute | solution.py:325
  164.4 25.6 %collective-permute-start.42 = (bf16[192,1408]{1,0:T(8,128)(2,1)S(1)}, bf16[192,1408]{1,0:T(8,128)(2,1)S(1)}, u32[]{:S(2)}, u32[]{:S(2)}) collective-permute-start(bf16[192,1408]{1,0:T(8,128)(2,1)S(1)} %get-tuple-element.91), channel_id=1, source_target_pairs={{0,16},{8,24},{16,0},{24,8},{1,17},{9,25},{17,1},{25,9},{2,18},{10... | collective-permute-start | bytes 1622024 | tf_op jit(solution)/shard_map/ppermute | solution.py:325
  165.4 28.3 %collective-permute-start.43 = (bf16[192,1408]{1,0:T(8,128)(2,1)S(1)}, bf16[192,1408]{1,0:T(8,128)(2,1)S(1)}, u32[]{:S(2)}, u32[]{:S(2)}) collective-permute-start(bf16[192,1408]{1,0:T(8,128)(2,1)S(1)} %get-tuple-element.92), channel_id=1, source_target_pairs={{0,24},{8,16},{16,8},{24,0},{1,25},{9,17},{17,9},{25,1},{2,26},{10... | collective-permute-start | bytes 1622024 | tf_op jit(solution)/shard_map/ppermute | solution.py:325
  166.7 9.9 %collective-permute-start.29 = (bf16[144,640]{1,0:T(8,128)(2,1)S(1)}, bf16[144,640]{1,0:T(8,128)(2,1)S(1)}, u32[]{:S(2)}, u32[]{:S(2)}) collective-permute-start(bf16[144,640]{1,0:T(8,128)(2,1)S(1)} %get-tuple-element.77), channel_id=1, source_target_pairs={{0,2},{2,0},{4,6},{6,4},{1,3},{3,1},{5,7},{7,5},{8,10},{10,8},{12,... | collective-permute-start | bytes 552968 | tf_op jit(solution)/shard_map/ppermute | solution.py:325
  169.3 26.8 %collective-permute-start.30 = (bf16[144,640]{1,0:T(8,128)(2,1)S(1)}, bf16[144,640]{1,0:T(8,128)(2,1)S(1)}, u32[]{:S(2)}, u32[]{:S(2)}) collective-permute-start(bf16[144,640]{1,0:T(8,128)(2,1)S(1)} %get-tuple-element.78), channel_id=1, source_target_pairs={{0,4},{2,6},{4,0},{6,2},{1,5},{3,7},{5,1},{7,3},{8,12},{10,14},{12... | collective-permute-start | bytes 552968 | tf_op jit(solution)/shard_map/ppermute | solution.py:325
  176.6 19.6 %collective-permute-start.31 = (bf16[144,640]{1,0:T(8,128)(2,1)S(1)}, bf16[144,640]{1,0:T(8,128)(2,1)S(1)}, u32[]{:S(2)}, u32[]{:S(2)}) collective-permute-start(bf16[144,640]{1,0:T(8,128)(2,1)S(1)} %get-tuple-element.79), channel_id=1, source_target_pairs={{0,6},{2,4},{4,2},{6,0},{1,7},{3,5},{5,3},{7,1},{8,14},{10,12},{12... | collective-permute-start | bytes 552968 | tf_op jit(solution)/shard_map/ppermute | solution.py:325
  178.4 20.8 %collective-permute-start.35 = (bf16[48,640]{1,0:T(8,128)(2,1)S(1)}, bf16[48,640]{1,0:T(8,128)(2,1)S(1)}, u32[]{:S(2)}, u32[]{:S(2)}) collective-permute-start(bf16[48,640]{1,0:T(8,128)(2,1)S(1)} %get-tuple-element.82), channel_id=1, source_target_pairs={{0,2},{2,0},{4,6},{6,4},{1,3},{3,1},{5,7},{7,5},{8,10},{10,8},{12,... | collective-permute-start | bytes 184328 | tf_op jit(solution)/shard_map/ppermute | solution.py:325
  190.0 10.5 %collective-permute-start.36 = (bf16[48,640]{1,0:T(8,128)(2,1)S(1)}, bf16[48,640]{1,0:T(8,128)(2,1)S(1)}, u32[]{:S(2)}, u32[]{:S(2)}) collective-permute-start(bf16[48,640]{1,0:T(8,128)(2,1)S(1)} %get-tuple-element.83), channel_id=1, source_target_pairs={{0,4},{2,6},{4,0},{6,2},{1,5},{3,7},{5,1},{7,3},{8,12},{10,14},{12... | collective-permute-start | bytes 184328 | tf_op jit(solution)/shard_map/ppermute | solution.py:325
  193.7 6.9 %collective-permute-start.37 = (bf16[48,640]{1,0:T(8,128)(2,1)S(1)}, bf16[48,640]{1,0:T(8,128)(2,1)S(1)}, u32[]{:S(2)}, u32[]{:S(2)}) collective-permute-start(bf16[48,640]{1,0:T(8,128)(2,1)S(1)} %get-tuple-element.84), channel_id=1, source_target_pairs={{0,6},{2,4},{4,2},{6,0},{1,7},{3,5},{5,3},{7,1},{8,14},{10,12},{12... | collective-permute-start | bytes 184328 | tf_op jit(solution)/shard_map/ppermute | solution.py:325
  196.1 14.5 %collective-permute-start.44 = (bf16[64,1408]{1,0:T(8,128)(2,1)S(1)}, bf16[64,1408]{1,0:T(8,128)(2,1)S(1)}, u32[]{:S(2)}, u32[]{:S(2)}) collective-permute-start(bf16[64,1408]{1,0:T(8,128)(2,1)S(1)} %get-tuple-element.94), channel_id=1, source_target_pairs={{0,2},{2,0},{4,6},{6,4},{1,3},{3,1},{5,7},{7,5},{8,10},{10,8},{12,... | collective-permute-start | bytes 540680 | tf_op jit(solution)/shard_map/ppermute | solution.py:325
  196.2 14.4 %collective-permute-start.45 = (bf16[64,1408]{1,0:T(8,128)(2,1)S(1)}, bf16[64,1408]{1,0:T(8,128)(2,1)S(1)}, u32[]{:S(2)}, u32[]{:S(2)}) collective-permute-start(bf16[64,1408]{1,0:T(8,128)(2,1)S(1)} %get-tuple-element.95), channel_id=1, source_target_pairs={{0,4},{2,6},{4,0},{6,2},{1,5},{3,7},{5,1},{7,3},{8,12},{10,14},{12... | collective-permute-start | bytes 540680 | tf_op jit(solution)/shard_map/ppermute | solution.py:325
  199.2 11.4 %collective-permute-start.46 = (bf16[64,1408]{1,0:T(8,128)(2,1)S(1)}, bf16[64,1408]{1,0:T(8,128)(2,1)S(1)}, u32[]{:S(2)}, u32[]{:S(2)}) collective-permute-start(bf16[64,1408]{1,0:T(8,128)(2,1)S(1)} %get-tuple-element.96), channel_id=1, source_target_pairs={{0,6},{2,4},{4,2},{6,0},{1,7},{3,5},{5,3},{7,1},{8,14},{10,12},{12... | collective-permute-start | bytes 540680 | tf_op jit(solution)/shard_map/ppermute | solution.py:325
  200.7 4.7 %collective-permute-start.38 = (bf16[48,640]{1,0:T(8,128)(2,1)S(1)}, bf16[48,640]{1,0:T(8,128)(2,1)S(1)}, u32[]{:S(2)}, u32[]{:S(2)}) collective-permute-start(bf16[48,640]{1,0:T(8,128)(2,1)S(1)} %get-tuple-element.86), channel_id=1, source_target_pairs={{0,8},{8,0},{16,24},{24,16},{1,9},{9,1},{17,25},{25,17},{2,10},{10... | collective-permute-start | bytes 184328 | tf_op jit(solution)/shard_map/ppermute | solution.py:325
  201.3 5.4 %collective-permute-start.39 = (bf16[48,640]{1,0:T(8,128)(2,1)S(1)}, bf16[48,640]{1,0:T(8,128)(2,1)S(1)}, u32[]{:S(2)}, u32[]{:S(2)}) collective-permute-start(bf16[48,640]{1,0:T(8,128)(2,1)S(1)} %get-tuple-element.87), channel_id=1, source_target_pairs={{0,16},{8,24},{16,0},{24,8},{1,17},{9,25},{17,1},{25,9},{2,18},{10... | collective-permute-start | bytes 184328 | tf_op jit(solution)/shard_map/ppermute | solution.py:325
  205.4 5.1 %collective-permute-start.40 = (bf16[48,640]{1,0:T(8,128)(2,1)S(1)}, bf16[48,640]{1,0:T(8,128)(2,1)S(1)}, u32[]{:S(2)}, u32[]{:S(2)}) collective-permute-start(bf16[48,640]{1,0:T(8,128)(2,1)S(1)} %get-tuple-element.88), channel_id=1, source_target_pairs={{0,24},{8,16},{16,8},{24,0},{1,25},{9,17},{17,9},{25,1},{2,26},{10... | collective-permute-start | bytes 184328 | tf_op jit(solution)/shard_map/ppermute | solution.py:325
  (18 other events, 333.0 us)
